TPU v7x, 128 devices: a whole 4x4x4 slice. The times are simulated.
128 devices in a mesh: ep: 16 (over z, x), tp: 8 (over y, core).
Axes of the slice: x: 4, y: 4, z: 4, core: 2. Of those that a mesh axis runs over, the one named last changes fastest.
Arguments:
- residual: bfloat16 [2048, 2048], P('ep', 'tp'), may hold values from -61 to 61
- in_gain: float32 [2048], replicated, may hold values from 0.1 to 1.9
- in_weight: bfloat16 [2048, 1024], P(None, 'tp'), may hold values from -0.125 to 0.125
- state: float32 [2, 2048, 4096], P(None, 'ep', 'tp'), may hold values from -3 to 3
- decay_rate: float32 [64, 64], P('tp'), may hold values from 0.1 to 1
- frequency: float32 [64, 64], P('tp'), may hold values from 0 to 200
- log_step: float32 [64], P('tp'), may hold values from -3 to -0.7
- in_coef: float32 [2, 64, 64, 16], P(None, 'tp'), may hold values from -1 to 1
- out_coef: float32 [2, 64, 16, 64], P(None, 'tp'), may hold values from -0.75 to 0.75
- skip_gain: float32 [1024], P('tp'), may hold values from -3 to 3
- out_weight: bfloat16 [1024, 2048], replicated, may hold values from -0.1875 to 0.1875
- mid_gain: float32 [2048], replicated, may hold values from 0.1 to 1.9
- gate_vector: bfloat16 [2048], replicated, may hold values from -0.125 to 0.125
- routes: int32 [2048, 4], P('ep'), may hold values from 0 to 127, all different within a row; in each aligned block of 128 rows (0 to 127, 128 to 255, ...) at most 8 rows name the same one
- route_weight: float32 [2048, 4], P('ep'), may hold values from 0.1 to 1
- expert_gate: bfloat16 [128, 2048, 512], P(('ep', 'tp')), may hold values from -0.125 to 0.125
- expert_up: bfloat16 [128, 2048, 512], P(('ep', 'tp')), may hold values from -0.125 to 0.125
- expert_down: bfloat16 [128, 512, 2048], P(('ep', 'tp')), may hold values from -0.25 to 0.25
- shared_gate: bfloat16 [2048, 4096], P(None, 'ep'), may hold values from -0.125 to 0.125
- shared_up: bfloat16 [2048, 4096], P(None, 'ep'), may hold values from -0.125 to 0.125
- shared_down: bfloat16 [4096, 2048], P('ep'), may hold values from -0.09375 to 0.09375
Outputs:
- layer_out: bfloat16 [2048, 2048], P(('ep', 'tp'))
- new_state: float32 [2, 2048, 4096], P(None, 'ep', 'tp')
Inputs may be any that keep to these rules, and one draw needn't show every extreme that they name: `routes`: each row names 4 different experts. Among the rows of one index of ep no expert is named more than 8 times, a bound that some block reaches.
All inputs are finite; a program needn't handle non-finite values.
Results may differ from a plain program's by a relative error of at most 0.0085.
Values may be sent and summed in bfloat16 or wider, within the bound.
No kernel may reach another device: no remote copies, remote signals or barrier semaphores. Data moves between devices by JAX's collectives and lax.ppermute only.
A program may use at most 128 MiB of HBM per device.

v0:
```python
import functools
import math

import jax
import jax.numpy as jnp
from jax import lax
from jax.experimental import pallas as pl
from jax.experimental.pallas import tpu as pltpu
from jax.sharding import PartitionSpec as P


norm_eps = 1e-05
routed_scale = 2.5
f32 = jnp.float32
bf16 = jnp.bfloat16
cores = 2


def y_shift(tp_count, step):
    chips = tp_count // cores
    return [
        (y * cores + c, ((y + step) % chips) * cores + c)
        for y in range(chips)
        for c in range(cores)
    ]


def core_swap(tp_count):
    return [(i, i ^ 1) for i in range(tp_count)]


def hop_gather(array, tp_count):
    chips = tp_count // cores
    mine = [array] + [
        lax.ppermute(array, "tp", y_shift(tp_count, step)) for step in range(1, chips)
    ]
    other = [lax.ppermute(part, "tp", core_swap(tp_count)) for part in mine]
    return mine, other


def plane_shift(ep_count, z_step, x_step):
    side = math.isqrt(ep_count)
    return [
        (z * side + x, ((z + z_step) % side) * side + (x + x_step) % side)
        for z in range(side)
        for x in range(side)
    ]


def natural_blocks(mine, other, tp_count, place):
    chips = tp_count // cores
    y, c = place // cores, place % cores
    even = jnp.where(c == 0, mine, other)
    odd = jnp.where(c == 0, other, mine)
    blocks = []
    for b in range(tp_count):
        k = (y - b // cores) % chips
        blocks.append(lax.dynamic_index_in_dim(even if b % cores == 0 else odd, k, 0, False))
    return jnp.concatenate(blocks, axis=1)


def layer_norm(values, gain_vec):
    row_mean = jnp.mean(values, axis=-1, keepdims=True)
    row_square = jnp.mean(values * values, axis=-1, keepdims=True)
    return (values - row_mean) * lax.rsqrt(row_square - row_mean * row_mean + norm_eps) * gain_vec


def coefficients(decay_rate, frequency, log_step, in_coef):
    time_step = jnp.exp(log_step)[:, None]
    real_rate = -decay_rate
    magnitude = jnp.exp(real_rate * time_step)
    keep_re = magnitude * jnp.cos(frequency * time_step)
    keep_im = magnitude * jnp.sin(frequency * time_step)
    denominator = real_rate * real_rate + frequency * frequency
    factor_re = ((keep_re - 1.0) * real_rate + keep_im * frequency) / denominator
    factor_im = (keep_im * real_rate - (keep_re - 1.0) * frequency) / denominator
    push_re = factor_re[..., None] * in_coef[0] - factor_im[..., None] * in_coef[1]
    push_im = factor_re[..., None] * in_coef[1] + factor_im[..., None] * in_coef[0]
    return (keep_re, keep_im, push_re, push_im)


def mixer_step(
    normed, in_weight, state, decay_rate, frequency, log_step, in_coef, out_coef, skip_gain
):
    row_count = normed.shape[0]
    group_count, state_count = decay_rate.shape
    keep_re, keep_im, push_re, push_im = coefficients(decay_rate, frequency, log_step, in_coef)
    drive = jnp.dot(normed, in_weight, preferred_element_type=f32).astype(bf16)
    drive_f = drive.astype(f32).reshape(row_count, group_count, -1)
    input_re = jnp.einsum("tgh,gph->tgp", drive_f, push_re)
    input_im = jnp.einsum("tgh,gph->tgp", drive_f, push_im)
    old_re = state[0].reshape(row_count, group_count, state_count)
    old_im = state[1].reshape(row_count, group_count, state_count)
    new_re = keep_re * old_re - keep_im * old_im + input_re
    new_im = keep_re * old_im + keep_im * old_re + input_im
    read_out = jnp.einsum("ghp,tgp->tgh", out_coef[0], new_re) - jnp.einsum(
        "ghp,tgp->tgh", out_coef[1], new_im
    )
    read_out = read_out.reshape(row_count, -1) + skip_gain * drive_f.reshape(row_count, -1)
    mixed_rows = jax.nn.gelu(read_out, approximate=True).astype(bf16)
    updated = jnp.stack([new_re.reshape(row_count, -1), new_im.reshape(row_count, -1)])
    return (mixed_rows, updated)


def in_hbm():
    return pl.BlockSpec(memory_space=pltpu.HBM)


def in_vmem():
    return pl.BlockSpec(memory_space=pltpu.VMEM)


def in_smem():
    return pl.BlockSpec(memory_space=pltpu.SMEM)


def mm(a, b):
    return jnp.dot(a, b, preferred_element_type=f32)


def expert_body(
    rows_hbm, gate_hbm, up_hbm, down_hbm, out_hbm, rows, gate, up, down, hidden, out, sems
):
    cuts = gate.shape[0]
    load_rows = pltpu.make_async_copy(rows_hbm, rows, sems.at[0])
    load_rows.start()
    loads = []
    for i in range(cuts):
        pair = (
            pltpu.make_async_copy(gate_hbm.at[i], gate.at[i], sems.at[1 + 2 * i]),
            pltpu.make_async_copy(up_hbm.at[i], up.at[i], sems.at[2 + 2 * i]),
        )
        for copy in pair:
            copy.start()
        loads.append(pair)
    parts = down.shape[0]
    tail = [
        pltpu.make_async_copy(down_hbm.at[i], down.at[i], sems.at[1 + 2 * cuts + i])
        for i in range(parts)
    ]
    for copy in tail:
        copy.start()
    load_rows.wait()
    gate_part = up_part = None
    depth = gate.shape[1]
    for i in range(cuts):
        for copy in loads[i]:
            copy.wait()
        block = rows[:, i * depth : (i + 1) * depth]
        g, u = mm(block, gate[i]), mm(block, up[i])
        gate_part = g if gate_part is None else gate_part + g
        up_part = u if up_part is None else up_part + u
    hidden[...] = (gate_part * jax.nn.sigmoid(gate_part) * up_part).astype(bf16)
    total = None
    depth = down.shape[1]
    for i in range(parts):
        tail[i].wait()
        piece = mm(hidden[:, i * depth : (i + 1) * depth], down[i])
        total = piece if total is None else total + piece
    out[...] = total.astype(bf16)
    store = pltpu.make_async_copy(out, out_hbm, sems.at[0])
    store.start()
    store.wait()


def expert_kernel(rows, gate, up, down):
    count, width = rows.shape
    inner = gate.shape[1]
    cuts, parts = 4, 2
    return pl.pallas_call(
        expert_body,
        out_shape=jax.ShapeDtypeStruct((count, width), bf16),
        in_specs=[in_hbm()] * 4,
        out_specs=in_hbm(),
        scratch_shapes=[
            pltpu.VMEM((count, width), bf16),
            pltpu.VMEM((cuts, width // cuts, inner), bf16),
            pltpu.VMEM((cuts, width // cuts, inner), bf16),
            pltpu.VMEM((parts, inner // parts, width), bf16),
            pltpu.VMEM((count, inner), bf16),
            pltpu.VMEM((count, width), bf16),
            pltpu.SemaphoreType.DMA((1 + 2 * cuts + parts,)),
        ],
        compiler_params=pltpu.CompilerParams(vmem_limit_bytes=60 * 1024 * 1024),
        name="expert_mlp",
    )(
        rows,
        gate.reshape(cuts, width // cuts, inner),
        up.reshape(cuts, width // cuts, inner),
        down.reshape(parts, inner // parts, width),
    )


def shared_body(place, *refs, side):
    planes, refs = refs[:side], refs[side:]
    z, x = lax.div(place[0], side), lax.rem(place[0], side)
    order = [
        lax.rem(z + side - i, side) * side + lax.rem(x + side - j, side)
        for i in range(side)
        for j in range(side)
    ]
    gate_hbm, up_hbm, down_hbm, out_hbm, gate, up, down, rows, out, sems = refs
    loads = [
        pltpu.make_async_copy(gate_hbm, gate, sems.at[0]),
        pltpu.make_async_copy(up_hbm, up, sems.at[1]),
        pltpu.make_async_copy(down_hbm, down, sems.at[2]),
    ]
    moves = [
        pltpu.make_async_copy(plane, rows.at[i], sems.at[3 + i]) for i, plane in enumerate(planes)
    ]
    for copy in moves + loads:
        copy.start()
    for copy in moves + loads[:2]:
        copy.wait()
    per = rows.shape[1] // side
    for half in range(2):
        x = rows[half * 2 : half * 2 + 2].reshape(2 * rows.shape[1], rows.shape[2])
        gate_part = mm(x, gate[...])
        up_part = mm(x, up[...])
        hidden = (gate_part * jax.nn.sigmoid(gate_part) * up_part).astype(bf16)
        if half == 0:
            loads[2].wait()
        result = mm(hidden, down[...]).astype(bf16)
        for k in range(2 * side):
            block = order[half * 2 * side + k]
            out[pl.ds(pl.multiple_of(block * per, per), per), :] = result[k * per : (k + 1) * per]
    store = pltpu.make_async_copy(out, out_hbm, sems.at[0])
    store.start()
    store.wait()


def shared_kernel(place, planes, gate, up, down):
    count, width = planes[0].shape
    inner = gate.shape[1]
    side = len(planes)
    return pl.pallas_call(
        functools.partial(shared_body, side=side),
        out_shape=jax.ShapeDtypeStruct((count * side, width), bf16),
        in_specs=[in_smem()] + [in_hbm()] * (side + 3),
        out_specs=in_hbm(),
        scratch_shapes=[
            pltpu.VMEM((width, inner), bf16),
            pltpu.VMEM((width, inner), bf16),
            pltpu.VMEM((inner, width), bf16),
            pltpu.VMEM((side, count, width), bf16),
            pltpu.VMEM((count * side, width), bf16),
            pltpu.SemaphoreType.DMA((3 + side,)),
        ],
        compiler_params=pltpu.CompilerParams(vmem_limit_bytes=60 * 1024 * 1024),
        name="shared_mlp",
    )(place, *planes, gate, up, down)


def mid_body(place, *refs, tp):
    resid, mixed, refs = refs[:tp], refs[tp : 2 * tp], refs[2 * tp :]
    chips = tp // cores
    chip, core = lax.div(place[0], cores), lax.rem(place[0], cores)
    order = [
        lax.rem(chip + chips - k, chips) * cores + (core ^ other)
        for other in range(cores)
        for k in range(chips)
    ]
    weight_hbm, gain, picked, own_mid, after_hbm, outgoing_hbm, weight, rows, total, normed, outgoing, sems = refs
    cuts = weight.shape[0]
    loads = [
        pltpu.make_async_copy(weight_hbm.at[i], weight.at[i], sems.at[i]) for i in range(cuts)
    ]
    for copy in loads:
        copy.start()
    feat, chan = resid[0].shape[1], mixed[0].shape[1]
    for i in range(tp):
        at = pl.multiple_of(order[i] * feat, feat)
        total[:, pl.ds(at, feat)] = resid[i][...].astype(f32)
        at = pl.multiple_of(order[i] * chan, chan)
        rows[:, pl.ds(at, chan)] = mixed[i][...]
    depth = weight.shape[1]
    for i in range(cuts):
        loads[i].wait()
        total[...] += mm(rows[:, i * depth : (i + 1) * depth], weight[i])
    values = total[...]
    mean = jnp.mean(values, axis=-1, keepdims=True)
    square = jnp.mean(values * values, axis=-1, keepdims=True)
    scale = lax.rsqrt(square - mean * mean + norm_eps)
    normed[...] = ((values - mean) * scale * gain[...]).astype(bf16)
    per = own_mid.shape[0]
    at = pl.multiple_of(place[0] * per, per)
    own_mid[...] = normed[pl.ds(at, per), :]
    keep = pltpu.make_async_copy(total.at[pl.ds(at, per), :], after_hbm, sems.at[0])
    keep.start()
    outgoing[...] = mm(picked[...], normed[...]).astype(bf16)
    store = pltpu.make_async_copy(outgoing, outgoing_hbm, sems.at[1])
    store.start()
    keep.wait()
    store.wait()


def mid_kernel(place, resid, mixed, weight, gain, picked):
    tp = len(resid)
    rows, feat = resid[0].shape
    chan = mixed[0].shape[1]
    width = feat * tp
    cuts = 8
    per = rows // tp
    return pl.pallas_call(
        functools.partial(mid_body, tp=tp),
        out_shape=(
            jax.ShapeDtypeStruct((per, width), bf16),
            jax.ShapeDtypeStruct((per, width), f32),
            jax.ShapeDtypeStruct((picked.shape[0], width), bf16),
        ),
        in_specs=[in_smem()] + [in_vmem()] * (2 * tp) + [in_hbm()] + [in_vmem()] * 2,
        out_specs=(in_vmem(), in_hbm(), in_hbm()),
        scratch_shapes=[
            pltpu.VMEM((cuts, chan * tp // cuts, width), bf16),
            pltpu.VMEM((rows, chan * tp), bf16),
            pltpu.VMEM((rows, width), f32),
            pltpu.VMEM((rows, width), bf16),
            pltpu.VMEM((picked.shape[0], width), bf16),
            pltpu.SemaphoreType.DMA((cuts,)),
        ],
        compiler_params=pltpu.CompilerParams(vmem_limit_bytes=60 * 1024 * 1024),
        name="out_proj_norm",
    )(
        place,
        *resid,
        *mixed,
        weight.reshape(cuts, chan * tp // cuts, width),
        gain.reshape(1, width),
        picked,
    )


def join_body(*refs):
    parts, out, sems = refs[:-2], refs[-2], refs[-1]
    per = parts[0].shape[0]
    moves = [
        pltpu.make_async_copy(part, out.at[pl.ds(i * per, per), :], sems.at[i])
        for i, part in enumerate(parts)
    ]
    for copy in moves:
        copy.start()
    for copy in moves:
        copy.wait()


def join_kernel(parts):
    per, width = parts[0].shape
    return pl.pallas_call(
        join_body,
        out_shape=jax.ShapeDtypeStruct((per * len(parts), width), parts[0].dtype),
        in_specs=[in_vmem()] * len(parts),
        out_specs=in_hbm(),
        scratch_shapes=[pltpu.SemaphoreType.DMA((len(parts),))],
        compiler_params=pltpu.CompilerParams(vmem_limit_bytes=60 * 1024 * 1024),
        name="join_rows",
    )(*parts)


def tables_body(place, routes, weights, picked_out, share_out, *, experts, tp_count):
    top, rows = routes.shape
    slots = picked_out.shape[0]
    capacity = slots * tp_count // experts
    tp = place[0]
    chips = tp_count // cores
    per = rows // tp_count
    slot = lax.broadcasted_iota(jnp.int32, (slots, rows), 0)
    wanted = (slot // capacity) * tp_count + tp
    total = jnp.sum(weights[...], axis=0, keepdims=True)
    named = routes[0:1, :] == wanted
    share = jnp.where(named, weights[0:1, :] / total * routed_scale, 0.0)
    for j in range(1, top):
        hit = routes[j : j + 1, :] == wanted
        named = named | hit
        share = share + jnp.where(hit, weights[j : j + 1, :] / total * routed_scale, 0.0)
    down = lax.broadcasted_iota(jnp.int32, (rows, rows), 0)
    across = lax.broadcasted_iota(jnp.int32, (rows, rows), 1)
    rank = mm(named.astype(f32).astype(bf16), (down < across).astype(f32).astype(bf16))
    picked = named & (rank == (slot % capacity).astype(f32))
    picked_out[...] = jnp.where(picked, 1.0, 0.0).astype(bf16)
    share = jnp.where(picked, share, 0.0)
    high = share.astype(bf16)
    low = (share - high.astype(f32)).astype(bf16)
    ahead = (across // per) % chips
    core = (tp % cores) ^ (across // (per * chips))
    source = (((tp // cores + ahead) % chips) * cores + core) * per + across % per
    turn = (source == down).astype(f32).astype(bf16)
    share_out[:slots, :] = mm(high, turn).astype(bf16)
    share_out[slots:, :] = mm(low, turn).astype(bf16)


def tables_kernel(place, routes, weights, experts, tp_count):
    rows, top = routes.shape
    slots = max(2, 2 * rows * top // experts) * (experts // tp_count)
    return pl.pallas_call(
        functools.partial(tables_body, experts=experts, tp_count=tp_count),
        out_shape=(
            jax.ShapeDtypeStruct((slots, rows), bf16),
            jax.ShapeDtypeStruct((2 * slots, rows), bf16),
        ),
        in_specs=[in_smem()] + [in_vmem()] * 2,
        out_specs=(in_vmem(),) * 2,
        compiler_params=pltpu.CompilerParams(vmem_limit_bytes=60 * 1024 * 1024),
        name="slot_tables",
    )(place, routes.T, weights.T)


def layer(
    residual,
    in_gain,
    in_weight,
    state,
    decay_rate,
    frequency,
    log_step,
    in_coef,
    out_coef,
    skip_gain,
    out_weight,
    mid_gain,
    gate_vector,
    routes,
    route_weight,
    expert_gate,
    expert_up,
    expert_down,
    shared_gate,
    shared_up,
    shared_down,
):
    tp_count = lax.axis_size("tp")
    ep_count = lax.axis_size("ep")
    chips = tp_count // cores
    place = lax.axis_index("tp")
    seq_rows, feat_part = residual.shape
    width = feat_part * tp_count
    per_dev = seq_rows // tp_count
    capacity = max(2, 2 * seq_rows * routes.shape[1] // (ep_count * tp_count))
    slots = ep_count * capacity

    resid_mine, resid_other = hop_gather(residual, tp_count)
    full_resid = natural_blocks(jnp.stack(resid_mine), jnp.stack(resid_other), tp_count, place).astype(f32)
    normed = layer_norm(full_resid, in_gain).astype(bf16)
    mixed_part, new_state = mixer_step(
        normed, in_weight, state, decay_rate, frequency, log_step, in_coef, out_coef, skip_gain
    )
    picked, share = tables_kernel(
        place.reshape(1), routes, route_weight, ep_count * tp_count, tp_count
    )
    mixed_mine, mixed_other = hop_gather(mixed_part, tp_count)
    own_mid, own_after, outgoing = mid_kernel(
        place.reshape(1), resid_mine + resid_other, mixed_mine + mixed_other, out_weight, mid_gain, picked
    )

    side = math.isqrt(ep_count)
    line = [own_mid] + [
        lax.ppermute(own_mid, "ep", plane_shift(ep_count, 0, step)) for step in range(1, side)
    ]
    line = join_kernel(line)
    plane = [line] + [
        lax.ppermute(line, "ep", plane_shift(ep_count, step, 0)) for step in range(1, side)
    ]
    slot_rows = lax.all_to_all(
        outgoing.reshape(ep_count, capacity, width), "ep", split_axis=0, concat_axis=0, tiled=True
    ).reshape(slots, width)

    result = expert_kernel(slot_rows, expert_gate[0], expert_up[0], expert_down[0])
    returned = lax.all_to_all(
        result.reshape(ep_count, capacity, width), "ep", split_axis=0, concat_axis=0, tiled=True
    ).reshape(slots, width)

    partial_rows = shared_kernel(lax.axis_index("ep").reshape(1), plane, shared_gate, shared_up, shared_down)
    partial_back = lax.all_to_all(
        partial_rows.reshape(ep_count, per_dev, width), "ep", split_axis=0, concat_axis=0, tiled=True
    )
    shared = jnp.sum(partial_back.astype(f32), axis=0)

    both = lax.dot_general(
        share,
        jnp.concatenate([returned, returned], axis=0),
        (((0,), (0,)), ((), ())),
        preferred_element_type=f32,
    )
    half = per_dev * chips
    theirs = lax.ppermute(both[half:].astype(bf16), "tp", core_swap(tp_count))
    pair = both[:half] + theirs.astype(f32)
    routed = pair[:per_dev]
    pair = pair.astype(bf16)
    for step in range(1, chips):
        routed = routed + lax.ppermute(
            pair[step * per_dev : (step + 1) * per_dev], "tp", y_shift(tp_count, step)
        ).astype(f32)
    gate_value = jax.nn.sigmoid(jnp.dot(own_mid, gate_vector, preferred_element_type=f32))
    layer_out = (own_after + routed + gate_value[:, None] * shared).astype(bf16)
    return (layer_out, new_state)


def solution(mesh):
    return jax.shard_map(
        layer,
        mesh=mesh,
        in_specs=(
            P("ep", "tp"),
            P(),
            P(None, "tp"),
            P(None, "ep", "tp"),
            P("tp", None),
            P("tp", None),
            P("tp"),
            P(None, "tp", None, None),
            P(None, "tp", None, None),
            P("tp"),
            P(),
            P(),
            P(),
            P("ep", None),
            P("ep", None),
            P(("ep", "tp"), None, None),
            P(("ep", "tp"), None, None),
            P(("ep", "tp"), None, None),
            P(None, "ep"),
            P(None, "ep"),
            P("ep", None),
        ),
        out_specs=(P(("ep", "tp"), None), P(None, "ep", "tp")),
        check_vma=False,
    )
```

profile of v0, /device:TPU:0, one launch (start us, length us, event | category | flops | bytes accessed | tf_op | source)
XLA Modules:
  0.0 114.0 jit_solution(4035952853991953533)
XLA Ops:
  0.8 3.2 %collective-permute-start.2 = (bf16[128,256]{1,0:T(8,128)(2,1)}, bf16[128,256]{1,0:T(8,128)(2,1)S(1)}, u32[]{:S(2)}, u32[]{:S(2)}) collective-permute-start(bf16[128,256]{1,0:T(8,128)(2,1)} %refs_0_.1), channel_id=1, source_target_pairs={{0,6},{1,7},{2,0},{3,1},{4,2},{5,3},{6,4},{7,5},{8,14},{9,15},{10,... | collective-permute-start | bytes 196616 | tf_op jit(solution)/shard_map/ppermute | solution.py:35
  3.9 0.6 collective-permute-start.1
  4.6 1.0 collective-permute-start
  5.5 1.1 fusion.50
  6.6 0.7 exp.9
  7.3 0.3 collective-permute-done.2.refs_3_
  7.6 2.9 %collective-permute-done.1.refs_2_ = bf16[128,256]{1,0:T(8,128)(2,1)S(1)} collective-permute-done((bf16[128,256]{1,0:T(8,128)(2,1)}, bf16[128,256]{1,0:T(8,128)(2,1)S(1)}, u32[]{:S(2)}, u32[]{:S(2)}) %collective-permute-start.1) | collective-permute-done | bytes 65568 | tf_op jit(solution)/shard_map/ppermute | solution.py:35
  10.5 0.7 collective-permute-done.refs_1_
  11.2 0.8 add_divide_fusion
  13.1 0.4 convolution_convert_fusion
  13.6 0.3 fusion
  13.9 0.3 fusion.1
  14.7 0.7 collective-permute-start.9
  15.4 0.6 collective-permute-start.8
  16.0 1.1 collective-permute-start.7
  17.1 1.8 %collective-permute-done.9.refs_11_ = bf16[128,128]{1,0:T(8,128)(2,1)S(1)} collective-permute-done((bf16[128,128]{1,0:T(8,128)(2,1)S(1)}, bf16[128,128]{1,0:T(8,128)(2,1)S(1)}, u32[]{:S(2)}, u32[]{:S(2)}) %collective-permute-start.9) | collective-permute-done | bytes 32800 | tf_op jit(solution)/shard_map/ppermute | solution.py:35
  18.9 2.0 %collective-permute-done.8.refs_10_ = bf16[128,128]{1,0:T(8,128)(2,1)S(1)} collective-permute-done((bf16[128,128]{1,0:T(8,128)(2,1)S(1)}, bf16[128,128]{1,0:T(8,128)(2,1)S(1)}, u32[]{:S(2)}, u32[]{:S(2)}) %collective-permute-start.8) | collective-permute-done | bytes 32800 | tf_op jit(solution)/shard_map/ppermute | solution.py:35
  20.9 0.5 collective-permute-done.7.refs_9_
  21.4 1.6 %slot_tables.1 = (bf16[128,128]{1,0:T(8,128)(2,1)}, bf16[256,128]{1,0:T(8,128)(2,1)}) custom-call(s32[1]{0:T(128)} %bitcast.place, s32[4,128]{1,0:T(4,128)} %bitcast.123, f32[4,128]{1,0:T(4,128)} %bitcast.124), custom_call_target="tpu_custom_call" | custom-call | tf_op jit(solution)/shard_map/slot_tables/pallas_call | solution.py:394
  23.1 0.5 copy-done.24
  23.7 5.7 %out_proj_norm.1 = (bf16[16,2048]{1,0:T(8,128)(2,1)}, f32[16,2048]{1,0:T(8,128)}, bf16[128,2048]{1,0:T(8,128)(2,1)}) custom-call(s32[1]{0:T(128)} %bitcast.place, bf16[128,256]{1,0:T(8,128)(2,1)} %refs_0_.1, bf16[128,256]{1,0:T(8,128)(2,1)} %copy-done.7, bf16[128,256]{1,0:T(8,128)(2,1)} %copy-done.6, bf16[128,256]{1,0:T(8,128)(2,1)} %copy-done.5, ...), custom_call_target="tpu_custom_call" | custom-call | tf_op jit(solution)/shard_map/out_proj_norm/pallas_call | solution.py:304
  29.5 20.2 %all_to_all.15 = bf16[16,8,2048]{2,1,0:T(8,128)(2,1)} all-to-all(bf16[16,8,2048]{2,1,0:T(8,128)(2,1)} %bitcast.110), channel_id=1, replica_groups=mesh['ep'=16,'tp'=8] {'ep'}, dimensions={0} | all-to-all | bytes 1048576 | tf_op jit(solution)/shard_map/all_to_all | solution.py:462
  49.6 4.3 %expert_mlp.1 = bf16[128,2048]{1,0:T(8,128)(2,1)} custom-call(bf16[128,2048]{1,0:T(8,128)(2,1)} %bitcast.105, bf16[4,512,512]{2,1,0:T(8,128)(2,1)} %bitcast.106, bf16[4,512,512]{2,1,0:T(8,128)(2,1)} %bitcast.107, bf16[2,256,2048]{2,1,0:T(8,128)(2,1)} %bitcast.108), custom_call_target="tpu_custom_call" | custom-call | tf_op jit(solution)/shard_map/expert_mlp/pallas_call | solution.py:170
  54.0 3.7 %all-to-all-start.1 = ((bf16[16,8,2048]{2,1,0:T(8,128)(2,1)}), bf16[16,8,2048]{2,1,0:T(8,128)(2,1)S(1)}, u32[]{:S(2)}, u32[]{:S(2)}) async-start(bf16[16,8,2048]{2,1,0:T(8,128)(2,1)} %bitcast.104), calls=%async_computation.1 | async-start | bytes 1048576 | tf_op jit(solution)/shard_map/all_to_all | solution.py:467
  57.7 3.1 %collective-permute-start.20 = (bf16[16,2048]{1,0:T(8,128)(2,1)S(1)}, bf16[16,2048]{1,0:T(8,128)(2,1)S(1)}, u32[]{:S(2)}, u32[]{:S(2)}) collective-permute-start(bf16[16,2048]{1,0:T(8,128)(2,1)S(1)} %copy-done.16), channel_id=1, source_target_pairs={{0,24},{8,0},{16,8},{24,16},{32,56},{40,32},{48,40},{56,48},{64,88... | collective-permute-start | bytes 196616 | tf_op jit(solution)/shard_map/ppermute | solution.py:456
  60.8 0.8 collective-permute-start.19
  61.7 0.9 collective-permute-start.18
  62.8 4.3 %collective-permute-done.20.refs_3_ = bf16[16,2048]{1,0:T(8,128)(2,1)S(1)} collective-permute-done((bf16[16,2048]{1,0:T(8,128)(2,1)S(1)}, bf16[16,2048]{1,0:T(8,128)(2,1)S(1)}, u32[]{:S(2)}, u32[]{:S(2)}) %collective-permute-start.20) | collective-permute-done | bytes 65568 | tf_op jit(solution)/shard_map/ppermute | solution.py:456
  67.1 1.6 %collective-permute-done.19.refs_2_ = bf16[16,2048]{1,0:T(8,128)(2,1)S(1)} collective-permute-done((bf16[16,2048]{1,0:T(8,128)(2,1)S(1)}, bf16[16,2048]{1,0:T(8,128)(2,1)S(1)}, u32[]{:S(2)}, u32[]{:S(2)}) %collective-permute-start.19) | collective-permute-done | bytes 65568 | tf_op jit(solution)/shard_map/ppermute | solution.py:456
  69.0 0.3 copy-done.19
  69.3 0.6 copy-done.20
  70.0 1.7 %join_rows.1.refs_0_ = bf16[64,2048]{1,0:T(8,128)(2,1)} custom-call(bf16[16,2048]{1,0:T(8,128)(2,1)} %get-tuple-element.11.refs_0_, bf16[16,2048]{1,0:T(8,128)(2,1)} %copy-done.20, bf16[16,2048]{1,0:T(8,128)(2,1)} %copy-done.19, bf16[16,2048]{1,0:T(8,128)(2,1)} %copy-done.18), custom_call_target="tpu_custom_call" | custom-call | tf_op jit(solution)/shard_map/join_rows/pallas_call | solution.py:348
  71.6 2.8 %collective-permute-start.23 = (bf16[64,2048]{1,0:T(8,128)(2,1)}, bf16[64,2048]{1,0:T(8,128)(2,1)S(1)}, u32[]{:S(2)}, u32[]{:S(2)}) collective-permute-start(bf16[64,2048]{1,0:T(8,128)(2,1)} %join_rows.1.refs_0_), channel_id=1, source_target_pairs={{0,96},{8,104},{16,112},{24,120},{32,0},{40,8},{48,16},{56,24},{64... | collective-permute-start | bytes 786440 | tf_op jit(solution)/shard_map/ppermute | solution.py:460
  74.5 0.8 collective-permute-start.22
  75.3 0.9 collective-permute-start.21
  76.2 0.3 fusion.10
  76.6 0.8 pad_maximum_fusion
  77.4 6.5 %collective-permute-done.23.refs_3_ = bf16[64,2048]{1,0:T(8,128)(2,1)S(1)} collective-permute-done((bf16[64,2048]{1,0:T(8,128)(2,1)}, bf16[64,2048]{1,0:T(8,128)(2,1)S(1)}, u32[]{:S(2)}, u32[]{:S(2)}) %collective-permute-start.23) | collective-permute-done | bytes 262176 | tf_op jit(solution)/shard_map/ppermute | solution.py:460
  84.0 0.8 collective-permute-done.22.refs_2_
  84.8 2.9 %collective-permute-done.21.refs_1_ = bf16[64,2048]{1,0:T(8,128)(2,1)} collective-permute-done((bf16[64,2048]{1,0:T(8,128)(2,1)}, bf16[64,2048]{1,0:T(8,128)(2,1)}, u32[]{:S(2)}, u32[]{:S(2)}) %collective-permute-start.21) | collective-permute-done | bytes 262176 | tf_op jit(solution)/shard_map/ppermute | solution.py:460
  87.7 4.3 %shared_mlp.1 = bf16[256,2048]{1,0:T(8,128)(2,1)} custom-call(s32[1]{0:T(128)} %bitcast.40.place, bf16[64,2048]{1,0:T(8,128)(2,1)} %join_rows.1.refs_0_, bf16[64,2048]{1,0:T(8,128)(2,1)} %collective-permute-done.21.refs_1_, bf16[64,2048]{1,0:T(8,128)(2,1)} %copy-done.2, bf16[64,2048]{1,0:T(8,128)(2,1)} %copy-done.1, bf16[2048,256]{1,0:T(8,128)(2,1)} %refs_4_.1, ...), custom_call_target="tpu_custom_call" | custom-call | tf_op jit(solution)/shard_map/shared_mlp/pallas_call | solution.py:236
  92.0 3.8 %all-to-all-start.2 = ((bf16[16,16,2048]{2,1,0:T(8,128)(2,1)}), bf16[16,16,2048]{2,1,0:T(8,128)(2,1)S(1)}, u32[]{:S(2)}, u32[]{:S(2)}) async-start(bf16[16,16,2048]{2,1,0:T(8,128)(2,1)} %bitcast.97), calls=%async_computation.2 | async-start | bytes 2097152 | tf_op jit(solution)/shard_map/all_to_all | solution.py:472
  95.9 1.0 fusion.49
  97.0 0.5 collective-permute-start.15
  97.5 2.8 %collective-permute-start.17 = (bf16[16,2048]{1,0:T(8,128)(2,1)S(1)}, bf16[16,2048]{1,0:T(8,128)(2,1)S(1)}, u32[]{:S(2)}, u32[]{:S(2)}) collective-permute-start(bf16[16,2048]{1,0:T(8,128)(2,1)S(1)} %get-tuple-element.21), channel_id=1, source_target_pairs={{0,6},{1,7},{2,0},{3,1},{4,2},{5,3},{6,4},{7,5},{8,14},{9,15},{10,... | collective-permute-start | bytes 196616 | tf_op jit(solution)/shard_map/ppermute | solution.py:489
  100.3 0.3 collective-permute-start.16
  100.6 12.5 %all-to-all-done.2 = bf16[16,16,2048]{2,1,0:T(8,128)(2,1)S(1)} async-done(((bf16[16,16,2048]{2,1,0:T(8,128)(2,1)}), bf16[16,16,2048]{2,1,0:T(8,128)(2,1)S(1)}, u32[]{:S(2)}, u32[]{:S(2)}) %all-to-all-start.2) | async-done | bytes 1048608 | tf_op jit(solution)/shard_map/all_to_all | solution.py:472
  113.3 0.7 fusion.22
  (107 shorter events, 2.5 us)
Async XLA Ops:
  0.6 12.4 %copy-start = (bf16[2048,128]{1,0:T(8,128)(2,1)S(1)}, bf16[2048,128]{1,0:T(8,128)(2,1)}, u32[]{:S(2)}) copy-start(bf16[2048,128]{1,0:T(8,128)(2,1)} %param.23) | copy-start | bytes 1572868
  0.6 11.9 %copy-start.3 = (bf16[128,256]{1,0:T(8,128)(2,1)S(1)}, bf16[128,256]{1,0:T(8,128)(2,1)}, u32[]{:S(2)}) copy-start(bf16[128,256]{1,0:T(8,128)(2,1)} %refs_0_.1) | copy-start | bytes 196612
  0.7 11.8 %collective-permute-start.3 = (bf16[128,256]{1,0:T(8,128)(2,1)}, bf16[128,256]{1,0:T(8,128)(2,1)S(1)}, u32[]{:S(2)}, u32[]{:S(2)}) collective-permute-start(bf16[128,256]{1,0:T(8,128)(2,1)} %refs_0_.1), channel_id=1, source_target_pairs={{0,1},{1,0},{2,3},{3,2},{4,5},{5,4},{6,7},{7,6},{8,9},{9,8},{10,11... | collective-permute-start | bytes 196616 | tf_op jit(solution)/shard_map/ppermute | solution.py:37
  0.8 6.9 %collective-permute-start.2 = (bf16[128,256]{1,0:T(8,128)(2,1)}, bf16[128,256]{1,0:T(8,128)(2,1)S(1)}, u32[]{:S(2)}, u32[]{:S(2)}) collective-permute-start(bf16[128,256]{1,0:T(8,128)(2,1)} %refs_0_.1), channel_id=1, source_target_pairs={{0,6},{1,7},{2,0},{3,1},{4,2},{5,3},{6,4},{7,5},{8,14},{9,15},{10,... | collective-permute-start | bytes 196616 | tf_op jit(solution)/shard_map/ppermute | solution.py:35
  3.9 6.6 %collective-permute-start.1 = (bf16[128,256]{1,0:T(8,128)(2,1)}, bf16[128,256]{1,0:T(8,128)(2,1)S(1)}, u32[]{:S(2)}, u32[]{:S(2)}) collective-permute-start(bf16[128,256]{1,0:T(8,128)(2,1)} %refs_0_.1), channel_id=1, source_target_pairs={{0,4},{1,5},{2,6},{3,7},{4,0},{5,1},{6,2},{7,3},{8,12},{9,13},{10,... | collective-permute-start | bytes 196616 | tf_op jit(solution)/shard_map/ppermute | solution.py:35
  4.6 6.6 %collective-permute-start = (bf16[128,256]{1,0:T(8,128)(2,1)}, bf16[128,256]{1,0:T(8,128)(2,1)S(1)}, u32[]{:S(2)}, u32[]{:S(2)}) collective-permute-start(bf16[128,256]{1,0:T(8,128)(2,1)} %refs_0_.1), channel_id=1, source_target_pairs={{0,2},{1,3},{2,4},{3,5},{4,6},{5,7},{6,0},{7,1},{8,10},{9,11},{10,... | collective-permute-start | bytes 196616 | tf_op jit(solution)/shard_map/ppermute | solution.py:35
  6.6 6.4 %copy-start.30 = (f32[2048]{0:T(1024)S(1)}, f32[2048]{0:T(1024)}, u32[]{:S(2)}) copy-start(f32[2048]{0:T(1024)} %param.22) | copy-start | bytes 24580
  7.6 5.8 %copy-start.5 = (bf16[128,256]{1,0:T(8,128)(2,1)}, bf16[128,256]{1,0:T(8,128)(2,1)S(1)}, u32[]{:S(2)}) copy-start(bf16[128,256]{1,0:T(8,128)(2,1)S(1)} %collective-permute-done.2.refs_3_) | copy-start | bytes 196612
  7.6 4.8 %collective-permute-start.6 = (bf16[128,256]{1,0:T(8,128)(2,1)S(1)}, bf16[128,256]{1,0:T(8,128)(2,1)S(1)}, u32[]{:S(2)}, u32[]{:S(2)}) collective-permute-start(bf16[128,256]{1,0:T(8,128)(2,1)S(1)} %collective-permute-done.2.refs_3_), channel_id=1, source_target_pairs={{0,1},{1,0},{2,3},{3,2},{4,5},{5,4},{6,7},{7,6},{8,9},{9,8},{10,11... | collective-permute-start | bytes 196616 | tf_op jit(solution)/shard_map/ppermute | solution.py:37
  10.5 3.0 %copy-start.6 = (bf16[128,256]{1,0:T(8,128)(2,1)}, bf16[128,256]{1,0:T(8,128)(2,1)S(1)}, u32[]{:S(2)}) copy-start(bf16[128,256]{1,0:T(8,128)(2,1)S(1)} %collective-permute-done.1.refs_2_) | copy-start | bytes 196612
  10.5 2.0 %collective-permute-start.5 = (bf16[128,256]{1,0:T(8,128)(2,1)S(1)}, bf16[128,256]{1,0:T(8,128)(2,1)S(1)}, u32[]{:S(2)}, u32[]{:S(2)}) collective-permute-start(bf16[128,256]{1,0:T(8,128)(2,1)S(1)} %collective-permute-done.1.refs_2_), channel_id=1, source_target_pairs={{0,1},{1,0},{2,3},{3,2},{4,5},{5,4},{6,7},{7,6},{8,9},{9,8},{10,11... | collective-permute-start | bytes 196616 | tf_op jit(solution)/shard_map/ppermute | solution.py:37
  11.2 2.3 %copy-start.7 = (bf16[128,256]{1,0:T(8,128)(2,1)}, bf16[128,256]{1,0:T(8,128)(2,1)S(1)}, u32[]{:S(2)}) copy-start(bf16[128,256]{1,0:T(8,128)(2,1)S(1)} %collective-permute-done.refs_1_) | copy-start | bytes 196612
  11.2 1.3 %collective-permute-start.4 = (bf16[128,256]{1,0:T(8,128)(2,1)S(1)}, bf16[128,256]{1,0:T(8,128)(2,1)S(1)}, u32[]{:S(2)}, u32[]{:S(2)}) collective-permute-start(bf16[128,256]{1,0:T(8,128)(2,1)S(1)} %collective-permute-done.refs_1_), channel_id=1, source_target_pairs={{0,1},{1,0},{2,3},{3,2},{4,5},{5,4},{6,7},{7,6},{8,9},{9,8},{10,11... | collective-permute-start | bytes 196616 | tf_op jit(solution)/shard_map/ppermute | solution.py:37
  12.5 1.0 copy-start.4
  12.5 1.1 copy-start.11
  12.8 1.5 %copy-start.12 = (f32[2,8,16,64]{3,2,1,0:T(8,128)S(1)}, f32[2,8,16,64]{3,2,1,0:T(8,128)}, u32[]{:S(2)}) copy-start(f32[2,8,16,64]{3,2,1,0:T(8,128)} %param.29) | copy-start | bytes 196612
  13.1 1.6 %copy-start.29 = (f32[128]{0:T(128)S(1)}, f32[128]{0:T(128)}, u32[]{:S(2)}) copy-start(f32[128]{0:T(128)} %param.30) | copy-start | bytes 1540
  14.7 8.4 %copy-start.14 = (bf16[128,128]{1,0:T(8,128)(2,1)}, bf16[128,128]{1,0:T(8,128)(2,1)S(1)}, u32[]{:S(2)}) copy-start(bf16[128,128]{1,0:T(8,128)(2,1)S(1)} %fusion.30.refs_8_) | copy-start | bytes 98308
  14.7 4.2 %collective-permute-start.9 = (bf16[128,128]{1,0:T(8,128)(2,1)S(1)}, bf16[128,128]{1,0:T(8,128)(2,1)S(1)}, u32[]{:S(2)}, u32[]{:S(2)}) collective-permute-start(bf16[128,128]{1,0:T(8,128)(2,1)S(1)} %fusion.30.refs_8_), channel_id=1, source_target_pairs={{0,6},{1,7},{2,0},{3,1},{4,2},{5,3},{6,4},{7,5},{8,14},{9,15},{10,... | collective-permute-start | bytes 98312 | tf_op jit(solution)/shard_map/ppermute | solution.py:35
  15.4 5.5 %collective-permute-start.8 = (bf16[128,128]{1,0:T(8,128)(2,1)S(1)}, bf16[128,128]{1,0:T(8,128)(2,1)S(1)}, u32[]{:S(2)}, u32[]{:S(2)}) collective-permute-start(bf16[128,128]{1,0:T(8,128)(2,1)S(1)} %fusion.30.refs_8_), channel_id=1, source_target_pairs={{0,4},{1,5},{2,6},{3,7},{4,0},{5,1},{6,2},{7,3},{8,12},{9,13},{10,... | collective-permute-start | bytes 98312 | tf_op jit(solution)/shard_map/ppermute | solution.py:35
  16.0 5.4 %collective-permute-start.7 = (bf16[128,128]{1,0:T(8,128)(2,1)S(1)}, bf16[128,128]{1,0:T(8,128)(2,1)S(1)}, u32[]{:S(2)}, u32[]{:S(2)}) collective-permute-start(bf16[128,128]{1,0:T(8,128)(2,1)S(1)} %fusion.30.refs_8_), channel_id=1, source_target_pairs={{0,2},{1,3},{2,4},{3,5},{4,6},{5,7},{6,0},{7,1},{8,10},{9,11},{10,... | collective-permute-start | bytes 98312 | tf_op jit(solution)/shard_map/ppermute | solution.py:35
  17.1 5.9 %collective-permute-start.10 = (bf16[128,128]{1,0:T(8,128)(2,1)S(1)}, bf16[128,128]{1,0:T(8,128)(2,1)S(1)}, u32[]{:S(2)}, u32[]{:S(2)}) collective-permute-start(bf16[128,128]{1,0:T(8,128)(2,1)S(1)} %fusion.30.refs_8_), channel_id=1, source_target_pairs={{0,1},{1,0},{2,3},{3,2},{4,5},{5,4},{6,7},{7,6},{8,9},{9,8},{10,11... | collective-permute-start | bytes 98312 | tf_op jit(solution)/shard_map/ppermute | solution.py:37
  18.9 4.2 %copy-start.21 = (bf16[128,128]{1,0:T(8,128)(2,1)}, bf16[128,128]{1,0:T(8,128)(2,1)S(1)}, u32[]{:S(2)}) copy-start(bf16[128,128]{1,0:T(8,128)(2,1)S(1)} %collective-permute-done.9.refs_11_) | copy-start | bytes 98308
  18.9 4.1 %collective-permute-start.13 = (bf16[128,128]{1,0:T(8,128)(2,1)S(1)}, bf16[128,128]{1,0:T(8,128)(2,1)S(1)}, u32[]{:S(2)}, u32[]{:S(2)}) collective-permute-start(bf16[128,128]{1,0:T(8,128)(2,1)S(1)} %collective-permute-done.9.refs_11_), channel_id=1, source_target_pairs={{0,1},{1,0},{2,3},{3,2},{4,5},{5,4},{6,7},{7,6},{8,9},{9,8},{10,11... | collective-permute-start | bytes 98312 | tf_op jit(solution)/shard_map/ppermute | solution.py:37
  20.9 2.2 %copy-start.22 = (bf16[128,128]{1,0:T(8,128)(2,1)}, bf16[128,128]{1,0:T(8,128)(2,1)S(1)}, u32[]{:S(2)}) copy-start(bf16[128,128]{1,0:T(8,128)(2,1)S(1)} %collective-permute-done.8.refs_10_) | copy-start | bytes 98308
  20.9 2.2 %collective-permute-start.12 = (bf16[128,128]{1,0:T(8,128)(2,1)S(1)}, bf16[128,128]{1,0:T(8,128)(2,1)S(1)}, u32[]{:S(2)}, u32[]{:S(2)}) collective-permute-start(bf16[128,128]{1,0:T(8,128)(2,1)S(1)} %collective-permute-done.8.refs_10_), channel_id=1, source_target_pairs={{0,1},{1,0},{2,3},{3,2},{4,5},{5,4},{6,7},{7,6},{8,9},{9,8},{10,11... | collective-permute-start | bytes 98312 | tf_op jit(solution)/shard_map/ppermute | solution.py:37
  21.4 1.8 %copy-start.23 = (bf16[128,128]{1,0:T(8,128)(2,1)}, bf16[128,128]{1,0:T(8,128)(2,1)S(1)}, u32[]{:S(2)}) copy-start(bf16[128,128]{1,0:T(8,128)(2,1)S(1)} %collective-permute-done.7.refs_9_) | copy-start | bytes 98308
  21.4 1.7 %collective-permute-start.11 = (bf16[128,128]{1,0:T(8,128)(2,1)S(1)}, bf16[128,128]{1,0:T(8,128)(2,1)S(1)}, u32[]{:S(2)}, u32[]{:S(2)}) collective-permute-start(bf16[128,128]{1,0:T(8,128)(2,1)S(1)} %collective-permute-done.7.refs_9_), channel_id=1, source_target_pairs={{0,1},{1,0},{2,3},{3,2},{4,5},{5,4},{6,7},{7,6},{8,9},{9,8},{10,11... | collective-permute-start | bytes 98312 | tf_op jit(solution)/shard_map/ppermute | solution.py:37
  49.6 8.1 %copy-start.16 = (bf16[16,2048]{1,0:T(8,128)(2,1)S(1)}, bf16[16,2048]{1,0:T(8,128)(2,1)}, u32[]{:S(2)}) copy-start(bf16[16,2048]{1,0:T(8,128)(2,1)} %get-tuple-element.11.refs_0_) | copy-start | bytes 196612
  49.6 12.9 %copy-start.28 = (bf16[2048]{0:T(1024)(128)(2,1)S(1)}, bf16[2048]{0:T(1024)(128)(2,1)}, u32[]{:S(2)}) copy-start(bf16[2048]{0:T(1024)(128)(2,1)} %param.33) | copy-start | bytes 12292
  54.0 22.2 %copy-start.15 = (bf16[256,128]{1,0:T(8,128)(2,1)S(1)}, bf16[256,128]{1,0:T(8,128)(2,1)}, u32[]{:S(2)}) copy-start(bf16[256,128]{1,0:T(8,128)(2,1)} %get-tuple-element.9) | copy-start | bytes 196612
  54.0 22.2 %all-to-all-start.1 = ((bf16[16,8,2048]{2,1,0:T(8,128)(2,1)}), bf16[16,8,2048]{2,1,0:T(8,128)(2,1)S(1)}, u32[]{:S(2)}, u32[]{:S(2)}) async-start(bf16[16,8,2048]{2,1,0:T(8,128)(2,1)} %bitcast.104), calls=%async_computation.1 | async-start | bytes 1048576 | tf_op jit(solution)/shard_map/all_to_all | solution.py:467
  57.7 9.4 %collective-permute-start.20 = (bf16[16,2048]{1,0:T(8,128)(2,1)S(1)}, bf16[16,2048]{1,0:T(8,128)(2,1)S(1)}, u32[]{:S(2)}, u32[]{:S(2)}) collective-permute-start(bf16[16,2048]{1,0:T(8,128)(2,1)S(1)} %copy-done.16), channel_id=1, source_target_pairs={{0,24},{8,0},{16,8},{24,16},{32,56},{40,32},{48,40},{56,48},{64,88... | collective-permute-start | bytes 196616 | tf_op jit(solution)/shard_map/ppermute | solution.py:456
  60.8 7.9 %collective-permute-start.19 = (bf16[16,2048]{1,0:T(8,128)(2,1)S(1)}, bf16[16,2048]{1,0:T(8,128)(2,1)S(1)}, u32[]{:S(2)}, u32[]{:S(2)}) collective-permute-start(bf16[16,2048]{1,0:T(8,128)(2,1)S(1)} %copy-done.16), channel_id=1, source_target_pairs={{0,16},{8,24},{16,0},{24,8},{32,48},{40,56},{48,32},{56,40},{64,80... | collective-permute-start | bytes 196616 | tf_op jit(solution)/shard_map/ppermute | solution.py:456
  61.7 7.3 %collective-permute-start.18 = (bf16[16,2048]{1,0:T(8,128)(2,1)S(1)}, bf16[16,2048]{1,0:T(8,128)(2,1)S(1)}, u32[]{:S(2)}, u32[]{:S(2)}) collective-permute-start(bf16[16,2048]{1,0:T(8,128)(2,1)S(1)} %copy-done.16), channel_id=1, source_target_pairs={{0,8},{8,16},{16,24},{24,0},{32,40},{40,48},{48,56},{56,32},{64,72... | collective-permute-start | bytes 196616 | tf_op jit(solution)/shard_map/ppermute | solution.py:456
  67.1 1.9 %copy-start.18 = (bf16[16,2048]{1,0:T(8,128)(2,1)}, bf16[16,2048]{1,0:T(8,128)(2,1)S(1)}, u32[]{:S(2)}) copy-start(bf16[16,2048]{1,0:T(8,128)(2,1)S(1)} %collective-permute-done.20.refs_3_) | copy-start | bytes 196612
  71.6 12.3 %collective-permute-start.23 = (bf16[64,2048]{1,0:T(8,128)(2,1)}, bf16[64,2048]{1,0:T(8,128)(2,1)S(1)}, u32[]{:S(2)}, u32[]{:S(2)}) collective-permute-start(bf16[64,2048]{1,0:T(8,128)(2,1)} %join_rows.1.refs_0_), channel_id=1, source_target_pairs={{0,96},{8,104},{16,112},{24,120},{32,0},{40,8},{48,16},{56,24},{64... | collective-permute-start | bytes 786440 | tf_op jit(solution)/shard_map/ppermute | solution.py:460
  74.5 10.4 %collective-permute-start.22 = (bf16[64,2048]{1,0:T(8,128)(2,1)}, bf16[64,2048]{1,0:T(8,128)(2,1)S(1)}, u32[]{:S(2)}, u32[]{:S(2)}) collective-permute-start(bf16[64,2048]{1,0:T(8,128)(2,1)} %join_rows.1.refs_0_), channel_id=1, source_target_pairs={{0,64},{8,72},{16,80},{24,88},{32,96},{40,104},{48,112},{56,120},{... | collective-permute-start | bytes 786440 | tf_op jit(solution)/shard_map/ppermute | solution.py:460
  75.3 12.4 %collective-permute-start.21 = (bf16[64,2048]{1,0:T(8,128)(2,1)}, bf16[64,2048]{1,0:T(8,128)(2,1)}, u32[]{:S(2)}, u32[]{:S(2)}) collective-permute-start(bf16[64,2048]{1,0:T(8,128)(2,1)} %join_rows.1.refs_0_), channel_id=1, source_target_pairs={{0,32},{8,40},{16,48},{24,56},{32,64},{40,72},{48,80},{56,88},{64,... | collective-permute-start | bytes 786440 | tf_op jit(solution)/shard_map/ppermute | solution.py:460
  76.5 19.4 %collective-permute-start.14 = (bf16[64,2048]{1,0:T(8,128)(2,1)S(1)}, bf16[64,2048]{1,0:T(8,128)(2,1)}, u32[]{:S(2)}, u32[]{:S(2)}) collective-permute-start(bf16[64,2048]{1,0:T(8,128)(2,1)S(1)} %slice.94), channel_id=1, source_target_pairs={{0,1},{1,0},{2,3},{3,2},{4,5},{5,4},{6,7},{7,6},{8,9},{9,8},{10,11... | collective-permute-start | bytes 786440 | tf_op jit(solution)/shard_map/ppermute | solution.py:484
  84.0 3.7 %copy-start.1 = (bf16[64,2048]{1,0:T(8,128)(2,1)}, bf16[64,2048]{1,0:T(8,128)(2,1)S(1)}, u32[]{:S(2)}) copy-start(bf16[64,2048]{1,0:T(8,128)(2,1)S(1)} %collective-permute-done.23.refs_3_) | copy-start | bytes 786436
  84.8 2.9 %copy-start.2 = (bf16[64,2048]{1,0:T(8,128)(2,1)}, bf16[64,2048]{1,0:T(8,128)(2,1)S(1)}, u32[]{:S(2)}) copy-start(bf16[64,2048]{1,0:T(8,128)(2,1)S(1)} %collective-permute-done.22.refs_2_) | copy-start | bytes 786436
  92.0 3.8 %copy-start.17 = (bf16[16,2048]{1,0:T(8,128)(2,1)S(1)}, bf16[16,2048]{1,0:T(8,128)(2,1)}, u32[]{:S(2)}) copy-start(bf16[16,2048]{1,0:T(8,128)(2,1)} %get-tuple-element.11.refs_0_) | copy-start | bytes 196612
  92.0 21.2 %all-to-all-start.2 = ((bf16[16,16,2048]{2,1,0:T(8,128)(2,1)}), bf16[16,16,2048]{2,1,0:T(8,128)(2,1)S(1)}, u32[]{:S(2)}, u32[]{:S(2)}) async-start(bf16[16,16,2048]{2,1,0:T(8,128)(2,1)} %bitcast.97), calls=%async_computation.2 | async-start | bytes 2097152 | tf_op jit(solution)/shard_map/all_to_all | solution.py:472
  95.8 17.5 %copy-start.13 = (f32[16,2048]{1,0:T(8,128)S(1)}, f32[16,2048]{1,0:T(8,128)}, u32[]{:S(2)}) copy-start(f32[16,2048]{1,0:T(8,128)} %get-tuple-element.8) | copy-start | bytes 393220
  97.0 16.3 %collective-permute-start.15 = (bf16[16,2048]{1,0:T(8,128)(2,1)S(1)}, bf16[16,2048]{1,0:T(8,128)(2,1)S(1)}, u32[]{:S(2)}, u32[]{:S(2)}) collective-permute-start(bf16[16,2048]{1,0:T(8,128)(2,1)S(1)} %get-tuple-element.20), channel_id=1, source_target_pairs={{0,2},{1,3},{2,4},{3,5},{4,6},{5,7},{6,0},{7,1},{8,10},{9,11},{10,... | collective-permute-start | bytes 196616 | tf_op jit(solution)/shard_map/ppermute | solution.py:489
  97.5 15.8 %collective-permute-start.17 = (bf16[16,2048]{1,0:T(8,128)(2,1)S(1)}, bf16[16,2048]{1,0:T(8,128)(2,1)S(1)}, u32[]{:S(2)}, u32[]{:S(2)}) collective-permute-start(bf16[16,2048]{1,0:T(8,128)(2,1)S(1)} %get-tuple-element.21), channel_id=1, source_target_pairs={{0,6},{1,7},{2,0},{3,1},{4,2},{5,3},{6,4},{7,5},{8,14},{9,15},{10,... | collective-permute-start | bytes 196616 | tf_op jit(solution)/shard_map/ppermute | solution.py:489
  100.3 13.0 %collective-permute-start.16 = (bf16[16,2048]{1,0:T(8,128)(2,1)S(1)}, bf16[16,2048]{1,0:T(8,128)(2,1)S(1)}, u32[]{:S(2)}, u32[]{:S(2)}) collective-permute-start(bf16[16,2048]{1,0:T(8,128)(2,1)S(1)} %get-tuple-element.22), channel_id=1, source_target_pairs={{0,4},{1,5},{2,6},{3,7},{4,0},{5,1},{6,2},{7,3},{8,12},{9,13},{10,... | collective-permute-start | bytes 196616 | tf_op jit(solution)/shard_map/ppermute | solution.py:489
  (9 other events, 6.7 us)
where the time goes:
time: 115 us; the launch traced here: 114 us
  waiting for transfers between devices  37.1 us (32%)
  starting transfers between devices  27.8 us (24%)
  blocking collectives  20.2 us (18%)
  Pallas kernels  17.6 us (15%)
  local copies, waits for them, and re-layouts  4.25 us (4%)
  other arithmetic  3.91 us (3%)
  matrix products  1.72 us (1%)
  between operations  1.39 us (1%)
    all_to_all x1, blocking collectives, layer(): lax.all_to_all(outgoing.reshape(ep_count, capacity, width), 'ep', split_a...  20.2 us
    all_to_all x1, waiting for transfers between devices, layer(): lax.all_to_all(partial_rows.reshape(ep_count, per_dev, width), 'ep', spli...  12.5 us
    ppermute x3, waiting for transfers between devices, layer(): lax.ppermute(line, 'ep', plane_shift(ep_count, step, 0))  10.2 us
    ppermute x6, waiting for transfers between devices, hop_gather(): lax.ppermute(array, 'tp', y_shift(tp_count, step))  8.16 us
    ppermute x6, starting transfers between devices, hop_gather(): lax.ppermute(array, 'tp', y_shift(tp_count, step))  7.19 us
    ppermute x3, waiting for transfers between devices, layer(): lax.ppermute(own_mid, 'ep', plane_shift(ep_count, 0, step))  6.18 us
    pallas_call x1, Pallas kernels, mid_kernel(): pl.pallas_call(functools.partial(mid_body, tp=tp), out_shape=(jax.ShapeDt...  5.75 us
    ppermute x3, starting transfers between devices, layer(): lax.ppermute(own_mid, 'ep', plane_shift(ep_count, 0, step))  4.8 us
  transfers between devices with their start and end apart: 26, of which 13 were waited for; matrix products, arithmetic and copies ran while one was open for 5% of the time, Pallas kernels for 7%

commit v1 on v0

--- a/solution.py
+++ b/solution.py
@@ -45,6 +45,22 @@
         for z in range(side)
         for x in range(side)
     ]
+
+
+def weight_moves(ep_count, tp_count, core):
+    side = math.isqrt(ep_count)
+    moves = []
+    for e in range(ep_count):
+        far = (side - 1 - e // side) * side + e % side
+        for t in range(tp_count):
+            to = far if t % cores == core else e
+            moves.append((e * tp_count + t, to * tp_count + (t ^ 1)))
+    return moves
+
+
+def pair_swap(ep_count):
+    side = math.isqrt(ep_count)
+    return [(e, ((e // side) ^ 1) * side + e % side) for e in range(ep_count)]
 
 
 def natural_blocks(mine, other, tp_count, place):
@@ -121,7 +137,8 @@
 def expert_body(
     rows_hbm, gate_hbm, up_hbm, down_hbm, out_hbm, rows, gate, up, down, hidden, out, sems
 ):
-    cuts = gate.shape[0]
+    cuts, depth = gate.shape[0], gate.shape[1]
+    halves = down.shape[0]
     load_rows = pltpu.make_async_copy(rows_hbm, rows, sems.at[0])
     load_rows.start()
     loads = []
@@ -133,16 +150,17 @@
         for copy in pair:
             copy.start()
         loads.append(pair)
-    parts = down.shape[0]
+    span = down.shape[2]
     tail = [
-        pltpu.make_async_copy(down_hbm.at[i], down.at[i], sems.at[1 + 2 * cuts + i])
-        for i in range(parts)
+        pltpu.make_async_copy(
+            down_hbm.at[:, i * span : (i + 1) * span], down.at[i], sems.at[1 + 2 * cuts + i]
+        )
+        for i in range(halves)
     ]
     for copy in tail:
         copy.start()
     load_rows.wait()
     gate_part = up_part = None
-    depth = gate.shape[1]
     for i in range(cuts):
         for copy in loads[i]:
             copy.wait()
@@ -151,22 +169,23 @@
         gate_part = g if gate_part is None else gate_part + g
         up_part = u if up_part is None else up_part + u
     hidden[...] = (gate_part * jax.nn.sigmoid(gate_part) * up_part).astype(bf16)
-    total = None
-    depth = down.shape[1]
-    for i in range(parts):
+    stores = []
+    for i in range(halves):
         tail[i].wait()
-        piece = mm(hidden[:, i * depth : (i + 1) * depth], down[i])
-        total = piece if total is None else total + piece
-    out[...] = total.astype(bf16)
-    store = pltpu.make_async_copy(out, out_hbm, sems.at[0])
-    store.start()
-    store.wait()
+        out[i] = mm(hidden[...], down[i]).astype(bf16)
+        store = pltpu.make_async_copy(
+            out.at[i], out_hbm.at[:, i * span : (i + 1) * span], sems.at[1 + 2 * i]
+        )
+        store.start()
+        stores.append(store)
+    for store in stores:
+        store.wait()
 
 
 def expert_kernel(rows, gate, up, down):
     count, width = rows.shape
     inner = gate.shape[1]
-    cuts, parts = 4, 2
+    cuts, parts = 8, 2
     return pl.pallas_call(
         expert_body,
         out_shape=jax.ShapeDtypeStruct((count, width), bf16),
@@ -176,9 +195,9 @@
             pltpu.VMEM((count, width), bf16),
             pltpu.VMEM((cuts, width // cuts, inner), bf16),
             pltpu.VMEM((cuts, width // cuts, inner), bf16),
-            pltpu.VMEM((parts, inner // parts, width), bf16),
+            pltpu.VMEM((parts, inner, width // parts), bf16),
             pltpu.VMEM((count, inner), bf16),
-            pltpu.VMEM((count, width), bf16),
+            pltpu.VMEM((parts, count, width // parts), bf16),
             pltpu.SemaphoreType.DMA((1 + 2 * cuts + parts,)),
         ],
         compiler_params=pltpu.CompilerParams(vmem_limit_bytes=60 * 1024 * 1024),
@@ -187,68 +206,135 @@
         rows,
         gate.reshape(cuts, width // cuts, inner),
         up.reshape(cuts, width // cuts, inner),
-        down.reshape(parts, inner // parts, width),
-    )
-
-
-def shared_body(place, *refs, side):
-    planes, refs = refs[:side], refs[side:]
-    z, x = lax.div(place[0], side), lax.rem(place[0], side)
+        down,
+    )
+
+
+def shared_body(
+    place,
+    line_hbm,
+    pair_hbm,
+    gate_hbm,
+    up_hbm,
+    down_hbm,
+    gate_far,
+    up_far,
+    down_far,
+    gate_swap,
+    up_swap,
+    down_swap,
+    out_hbm,
+    gate,
+    up,
+    down,
+    rows,
+    out,
+    sems,
+    *,
+    side,
+):
+    here, core = place[0], lax.rem(place[1], cores)
+    z, x = lax.rem(lax.div(here, side), 2), lax.rem(here, side)
     order = [
-        lax.rem(z + side - i, side) * side + lax.rem(x + side - j, side)
-        for i in range(side)
-        for j in range(side)
-    ]
-    gate_hbm, up_hbm, down_hbm, out_hbm, gate, up, down, rows, out, sems = refs
-    loads = [
-        pltpu.make_async_copy(gate_hbm, gate, sems.at[0]),
-        pltpu.make_async_copy(up_hbm, up, sems.at[1]),
-        pltpu.make_async_copy(down_hbm, down, sems.at[2]),
+        lax.rem(z + i, 2) * side + lax.rem(x + side - j, side) for i in range(2) for j in range(side)
     ]
     moves = [
-        pltpu.make_async_copy(plane, rows.at[i], sems.at[3 + i]) for i, plane in enumerate(planes)
-    ]
-    for copy in moves + loads:
+        pltpu.make_async_copy(line_hbm, rows.at[0], sems.at[0]),
+        pltpu.make_async_copy(pair_hbm, rows.at[1], sems.at[1]),
+    ]
+    near = [
+        pltpu.make_async_copy(source, target.at[0], sems.at[2 + i])
+        for i, (source, target) in enumerate(((gate_hbm, gate), (up_hbm, up), (down_hbm, down)))
+    ]
+    for copy in moves + near:
         copy.start()
-    for copy in moves + loads[:2]:
+
+    @pl.when(core == 0)
+    def _():
+        pltpu.make_async_copy(gate_swap, gate.at[1], sems.at[5]).start()
+        pltpu.make_async_copy(up_far, up.at[1], sems.at[6]).start()
+        pltpu.make_async_copy(down_swap, down.at[1], sems.at[7]).start()
+
+    @pl.when(core != 0)
+    def _():
+        pltpu.make_async_copy(gate_far, gate.at[1], sems.at[5]).start()
+        pltpu.make_async_copy(up_swap, up.at[1], sems.at[6]).start()
+        pltpu.make_async_copy(down_far, down.at[1], sems.at[7]).start()
+
+    far = [
+        pltpu.make_async_copy(gate_far, gate.at[1], sems.at[5]),
+        pltpu.make_async_copy(up_far, up.at[1], sems.at[6]),
+        pltpu.make_async_copy(down_far, down.at[1], sems.at[7]),
+    ]
+    for copy in moves:
         copy.wait()
+    count = 2 * rows.shape[1]
+    x_all = rows[...].reshape(count, rows.shape[2])
+    hidden = []
+    for i, loads in enumerate((near, far)):
+        loads[0].wait()
+        gate_part = mm(x_all, gate[i])
+        loads[1].wait()
+        up_part = mm(x_all, up[i])
+        hidden.append((gate_part * jax.nn.sigmoid(gate_part) * up_part).astype(bf16))
+    near[2].wait()
+    far[2].wait()
     per = rows.shape[1] // side
+    stores = []
     for half in range(2):
-        x = rows[half * 2 : half * 2 + 2].reshape(2 * rows.shape[1], rows.shape[2])
-        gate_part = mm(x, gate[...])
-        up_part = mm(x, up[...])
-        hidden = (gate_part * jax.nn.sigmoid(gate_part) * up_part).astype(bf16)
-        if half == 0:
-            loads[2].wait()
-        result = mm(hidden, down[...]).astype(bf16)
-        for k in range(2 * side):
-            block = order[half * 2 * side + k]
-            out[pl.ds(pl.multiple_of(block * per, per), per), :] = result[k * per : (k + 1) * per]
-    store = pltpu.make_async_copy(out, out_hbm, sems.at[0])
-    store.start()
-    store.wait()
-
-
-def shared_kernel(place, planes, gate, up, down):
-    count, width = planes[0].shape
-    inner = gate.shape[1]
-    side = len(planes)
+        lo = half * count // 2
+        part = slice(lo, lo + count // 2)
+        total = mm(hidden[0][part], down[0]) + mm(hidden[1][part], down[1])
+        out[part, :] = total.astype(bf16)
+        for k in range(half * side, (half + 1) * side):
+            at = pl.multiple_of(order[k] * per, per)
+            stores.append(
+                pltpu.make_async_copy(
+                    out.at[k * per : (k + 1) * per, :], out_hbm.at[pl.ds(at, per), :], sems.at[8 + k]
+                )
+            )
+            stores[-1].start()
+    for store in stores:
+        store.wait()
+
+
+def shared_kernel(place, line, pair, own, far, swap, side):
+    count, width = line.shape
+    inner = own[0].shape[1]
     return pl.pallas_call(
         functools.partial(shared_body, side=side),
-        out_shape=jax.ShapeDtypeStruct((count * side, width), bf16),
-        in_specs=[in_smem()] + [in_hbm()] * (side + 3),
+        out_shape=jax.ShapeDtypeStruct((count * 2, width), bf16),
+        in_specs=[in_smem()] + [in_hbm()] * 11,
         out_specs=in_hbm(),
         scratch_shapes=[
-            pltpu.VMEM((width, inner), bf16),
-            pltpu.VMEM((width, inner), bf16),
-            pltpu.VMEM((inner, width), bf16),
-            pltpu.VMEM((side, count, width), bf16),
-            pltpu.VMEM((count * side, width), bf16),
-            pltpu.SemaphoreType.DMA((3 + side,)),
+            pltpu.VMEM((2, width, inner), bf16),
+            pltpu.VMEM((2, width, inner), bf16),
+            pltpu.VMEM((2, inner, width), bf16),
+            pltpu.VMEM((2, count, width), bf16),
+            pltpu.VMEM((count * 2, width), bf16),
+            pltpu.SemaphoreType.DMA((8 + 2 * side,)),
         ],
         compiler_params=pltpu.CompilerParams(vmem_limit_bytes=60 * 1024 * 1024),
         name="shared_mlp",
-    )(place, *planes, gate, up, down)
+    )(place, line, pair, *own, *far, *swap)
+
+
+def pull_body(weight_hbm, out, sem):
+    copy = pltpu.make_async_copy(weight_hbm, out, sem)
+    copy.start()
+    copy.wait()
+
+
+def pull_kernel(weight):
+    return pl.pallas_call(
+        pull_body,
+        out_shape=jax.ShapeDtypeStruct(weight.shape, weight.dtype),
+        in_specs=[in_hbm()],
+        out_specs=in_vmem(),
+        scratch_shapes=[pltpu.SemaphoreType.DMA(())],
+        compiler_params=pltpu.CompilerParams(vmem_limit_bytes=8 << 20),
+        name="pull_weight",
+    )(weight)
 
 
 def mid_body(place, *refs, tp):
@@ -260,23 +346,14 @@
         for other in range(cores)
         for k in range(chips)
     ]
-    weight_hbm, gain, picked, own_mid, after_hbm, outgoing_hbm, weight, rows, total, normed, outgoing, sems = refs
-    cuts = weight.shape[0]
-    loads = [
-        pltpu.make_async_copy(weight_hbm.at[i], weight.at[i], sems.at[i]) for i in range(cuts)
-    ]
-    for copy in loads:
-        copy.start()
+    weight, gain, picked, own_mid, after_hbm, outgoing_hbm, rows, total, normed, outgoing, sems = refs
     feat, chan = resid[0].shape[1], mixed[0].shape[1]
     for i in range(tp):
         at = pl.multiple_of(order[i] * feat, feat)
         total[:, pl.ds(at, feat)] = resid[i][...].astype(f32)
         at = pl.multiple_of(order[i] * chan, chan)
         rows[:, pl.ds(at, chan)] = mixed[i][...]
-    depth = weight.shape[1]
-    for i in range(cuts):
-        loads[i].wait()
-        total[...] += mm(rows[:, i * depth : (i + 1) * depth], weight[i])
+    total[...] += mm(rows[...], weight[...])
     values = total[...]
     mean = jnp.mean(values, axis=-1, keepdims=True)
     square = jnp.mean(values * values, axis=-1, keepdims=True)
@@ -299,7 +376,6 @@
     rows, feat = resid[0].shape
     chan = mixed[0].shape[1]
     width = feat * tp
-    cuts = 8
     per = rows // tp
     return pl.pallas_call(
         functools.partial(mid_body, tp=tp),
@@ -308,23 +384,22 @@
             jax.ShapeDtypeStruct((per, width), f32),
             jax.ShapeDtypeStruct((picked.shape[0], width), bf16),
         ),
-        in_specs=[in_smem()] + [in_vmem()] * (2 * tp) + [in_hbm()] + [in_vmem()] * 2,
+        in_specs=[in_smem()] + [in_vmem()] * (2 * tp + 3),
         out_specs=(in_vmem(), in_hbm(), in_hbm()),
         scratch_shapes=[
-            pltpu.VMEM((cuts, chan * tp // cuts, width), bf16),
             pltpu.VMEM((rows, chan * tp), bf16),
             pltpu.VMEM((rows, width), f32),
             pltpu.VMEM((rows, width), bf16),
             pltpu.VMEM((picked.shape[0], width), bf16),
-            pltpu.SemaphoreType.DMA((cuts,)),
+            pltpu.SemaphoreType.DMA((2,)),
         ],
-        compiler_params=pltpu.CompilerParams(vmem_limit_bytes=60 * 1024 * 1024),
+        compiler_params=pltpu.CompilerParams(vmem_limit_bytes=24 << 20),
         name="out_proj_norm",
     )(
         place,
         *resid,
         *mixed,
-        weight.reshape(cuts, chan * tp // cuts, width),
+        weight,
         gain.reshape(1, width),
         picked,
     )
@@ -351,7 +426,7 @@
         in_specs=[in_vmem()] * len(parts),
         out_specs=in_hbm(),
         scratch_shapes=[pltpu.SemaphoreType.DMA((len(parts),))],
-        compiler_params=pltpu.CompilerParams(vmem_limit_bytes=60 * 1024 * 1024),
+        compiler_params=pltpu.CompilerParams(vmem_limit_bytes=8 << 20),
         name="join_rows",
     )(*parts)
 
@@ -399,7 +474,7 @@
         ),
         in_specs=[in_smem()] + [in_vmem()] * 2,
         out_specs=(in_vmem(),) * 2,
-        compiler_params=pltpu.CompilerParams(vmem_limit_bytes=60 * 1024 * 1024),
+        compiler_params=pltpu.CompilerParams(vmem_limit_bytes=8 << 20),
         name="slot_tables",
     )(place, routes.T, weights.T)
 
@@ -438,6 +513,12 @@
     slots = ep_count * capacity
 
     resid_mine, resid_other = hop_gather(residual, tp_count)
+    own = (shared_gate, shared_up, shared_down)
+    far = [
+        lax.ppermute(w, ("ep", "tp"), weight_moves(ep_count, tp_count, core))
+        for w, core in zip(own, (0, 1, 0))
+    ]
+    swap = [lax.ppermute(w, "tp", core_swap(tp_count)) for w in far]
     full_resid = natural_blocks(jnp.stack(resid_mine), jnp.stack(resid_other), tp_count, place).astype(f32)
     normed = layer_norm(full_resid, in_gain).astype(bf16)
     mixed_part, new_state = mixer_step(
@@ -447,18 +528,17 @@
         place.reshape(1), routes, route_weight, ep_count * tp_count, tp_count
     )
     mixed_mine, mixed_other = hop_gather(mixed_part, tp_count)
+    out_rows = pull_kernel(out_weight)
     own_mid, own_after, outgoing = mid_kernel(
-        place.reshape(1), resid_mine + resid_other, mixed_mine + mixed_other, out_weight, mid_gain, picked
+        place.reshape(1), resid_mine + resid_other, mixed_mine + mixed_other, out_rows, mid_gain, picked
     )
 
     side = math.isqrt(ep_count)
-    line = [own_mid] + [
-        lax.ppermute(own_mid, "ep", plane_shift(ep_count, 0, step)) for step in range(1, side)
-    ]
+    line = [own_mid]
+    for step in range(1, side):
+        line.append(lax.ppermute(own_mid, "ep", plane_shift(ep_count, 0, step)))
     line = join_kernel(line)
-    plane = [line] + [
-        lax.ppermute(line, "ep", plane_shift(ep_count, step, 0)) for step in range(1, side)
-    ]
+    pair = lax.ppermute(line, "ep", pair_swap(ep_count))
     slot_rows = lax.all_to_all(
         outgoing.reshape(ep_count, capacity, width), "ep", split_axis=0, concat_axis=0, tiled=True
     ).reshape(slots, width)
@@ -468,9 +548,16 @@
         result.reshape(ep_count, capacity, width), "ep", split_axis=0, concat_axis=0, tiled=True
     ).reshape(slots, width)
 
-    partial_rows = shared_kernel(lax.axis_index("ep").reshape(1), plane, shared_gate, shared_up, shared_down)
+    group = 2 * side
+    where = jnp.stack([lax.axis_index("ep"), place]).astype(jnp.int32)
+    partial_rows = shared_kernel(where, line, pair, own, far, swap, side)
     partial_back = lax.all_to_all(
-        partial_rows.reshape(ep_count, per_dev, width), "ep", split_axis=0, concat_axis=0, tiled=True
+        partial_rows.reshape(group, per_dev, width),
+        "ep",
+        split_axis=0,
+        concat_axis=0,
+        axis_index_groups=[list(range(g, g + group)) for g in range(0, ep_count, group)],
+        tiled=True,
     )
     shared = jnp.sum(partial_back.astype(f32), axis=0)
 

time: 115 us -> 104 us (0.904)
  waiting for transfers between devices: 37.1 us -> 22.4 us
  starting transfers between devices: 27.8 us -> 39.3 us
  Pallas kernels: 17.6 us -> 12.3 us
  blocking collectives: 20.2 us -> 16.6 us
  other arithmetic: 3.91 us -> 5.22 us
    all_to_all x1, waiting for transfers between devices: 12.5 us -> 4.12 us  [layer(): lax.all_to_all(partial_rows.reshape(group, per_dev, width), 'ep', split_a...]
    ppermute x6 -> x10, waiting for transfers between devices: 16.4 us -> 10.4 us  [the longest x3 6.83 us: layer(): line.append(lax.ppermute(own_mid, 'ep', plane_shift(ep_count, 0, step)))]
    ppermute x6 -> x10, starting transfers between devices: 9.31 us -> 15 us  [the longest x3 7.17 us: layer(): lax.ppermute(w, ('ep', 'tp'), weight_moves(ep_count, tp_count, core))]
    pallas_call x1, Pallas kernels: 5.75 us -> 1.63 us  [mid_kernel(): pl.pallas_call(functools.partial(mid_body, tp=tp), out_shape=(jax.ShapeDt...]
    all_to_all x1, blocking collectives: 20.2 us -> 16.6 us  [layer(): lax.all_to_all(outgoing.reshape(ep_count, capacity, width), 'ep', split_a...]
    all_to_all x1, starting transfers between devices: 3.72 us -> 7.2 us  [layer(): lax.all_to_all(result.reshape(ep_count, capacity, width), 'ep', split_axi...]
    pallas_call x1, Pallas kernels: 1.63 us -> 0.29 us  [tables_kernel(): pl.pallas_call(functools.partial(tables_body, experts=experts, tp_count=t...]
    pallas_call x1, Pallas kernels: 1.67 us -> 0.35 us  [join_kernel(): pl.pallas_call(join_body, out_shape=jax.ShapeDtypeStruct((per * len(parts...]
  transfers between devices with their start and end apart: 26 -> 30, of which waited for: 13 -> 8; matrix products, arithmetic and copies ran while one was open for 5% -> 9% of each run, Pallas kernels for 7% -> 12%
where the time goes in v1:
time: 104 us
  starting transfers between devices  39.3 us (38%)
  waiting for transfers between devices  22.4 us (22%)
  blocking collectives  16.6 us (16%)
  Pallas kernels  12.3 us (12%)
  other arithmetic  5.22 us (5%)
  local copies, waits for them, and re-layouts  4.86 us (5%)
  matrix products  1.72 us (2%)
  between operations  1.28 us (1%)
    all_to_all x1, blocking collectives, layer(): lax.all_to_all(outgoing.reshape(ep_count, capacity, width), 'ep', split_a...  16.6 us
    ppermute x6, starting transfers between devices, hop_gather(): lax.ppermute(array, 'tp', y_shift(tp_count, step))  8 us
    all_to_all x1, starting transfers between devices, layer(): lax.all_to_all(result.reshape(ep_count, capacity, width), 'ep', split_axi...  7.2 us
    ppermute x3, starting transfers between devices, layer(): lax.ppermute(w, ('ep', 'tp'), weight_moves(ep_count, tp_count, core))  7.17 us
    ppermute x6, waiting for transfers between devices, hop_gather(): lax.ppermute(array, 'tp', y_shift(tp_count, step))  7.12 us
    ppermute x3, waiting for transfers between devices, layer(): line.append(lax.ppermute(own_mid, 'ep', plane_shift(ep_count, 0, step)))  6.83 us
    ppermute x3, starting transfers between devices, layer(): line.append(lax.ppermute(own_mid, 'ep', plane_shift(ep_count, 0, step)))  5.57 us
    pallas_call x1, Pallas kernels, shared_kernel(): pl.pallas_call(functools.partial(shared_body, side=side), out_shape=jax.S...  5.54 us
  transfers between devices with their start and end apart: 30, of which 8 were waited for; matrix products, arithmetic and copies ran while one was open for 9% of the time, Pallas kernels for 12%

profile of v1, /device:TPU:0, one launch (start us, length us, event | category | flops | bytes accessed | tf_op | source)
XLA Modules:
  0.0 103.6 jit_solution(14359516697296862581)
XLA Ops:
  0.7 1.8 %collective-permute-start = (bf16[128,256]{1,0:T(8,128)(2,1)}, bf16[128,256]{1,0:T(8,128)(2,1)S(1)}, u32[]{:S(2)}, u32[]{:S(2)}) collective-permute-start(bf16[128,256]{1,0:T(8,128)(2,1)} %refs_0_.1), channel_id=1, source_target_pairs={{0,2},{1,3},{2,4},{3,5},{4,6},{5,7},{6,0},{7,1},{8,10},{9,11},{10,... | collective-permute-start | bytes 196616 | tf_op jit(solution)/shard_map/ppermute | solution.py:35
  2.4 2.9 %collective-permute-start.1 = (bf16[128,256]{1,0:T(8,128)(2,1)}, bf16[128,256]{1,0:T(8,128)(2,1)S(1)}, u32[]{:S(2)}, u32[]{:S(2)}) collective-permute-start(bf16[128,256]{1,0:T(8,128)(2,1)} %refs_0_.1), channel_id=1, source_target_pairs={{0,4},{1,5},{2,6},{3,7},{4,0},{5,1},{6,2},{7,3},{8,12},{9,13},{10,... | collective-permute-start | bytes 196616 | tf_op jit(solution)/shard_map/ppermute | solution.py:35
  5.3 1.3 %collective-permute-start.2 = (bf16[128,256]{1,0:T(8,128)(2,1)}, bf16[128,256]{1,0:T(8,128)(2,1)S(1)}, u32[]{:S(2)}, u32[]{:S(2)}) collective-permute-start(bf16[128,256]{1,0:T(8,128)(2,1)} %refs_0_.1), channel_id=1, source_target_pairs={{0,6},{1,7},{2,0},{3,1},{4,2},{5,3},{6,4},{7,5},{8,14},{9,15},{10,... | collective-permute-start | bytes 196616 | tf_op jit(solution)/shard_map/ppermute | solution.py:35
  6.7 4.1 %collective-permute-start.22 = (bf16[2048,256]{1,0:T(8,128)(2,1)}, bf16[2048,256]{1,0:T(8,128)(2,1)}, u32[]{:S(2)}, u32[]{:S(2)}) collective-permute-start(bf16[2048,256]{1,0:T(8,128)(2,1)} %gate_hbm.1), channel_id=1, source_target_pairs={{0,97},{1,0},{2,99},{3,2},{4,101},{5,4},{6,103},{7,6},{8,105},{9,8... | collective-permute-start | bytes 3145736 | tf_op jit(solution)/shard_map/ppermute | solution.py:518
  10.8 1.1 %fusion.50 = (f32[1,128,512]{2,1,0:T(8,128)S(1)}, f32[1,128,512]{2,1,0:T(8,128)S(1)}) fusion(f32[2,128,512]{2,1,0:T(8,128)} %param.24), kind=kLoop, calls=%fused_computation.86 | loop fusion | bytes 1048576 | tf_op jit(solution)/shard_map/slice | solution.py:108
  11.9 0.7 exp.9
  12.6 0.5 collective-permute-start.5
  13.2 0.8 add_divide_fusion
  14.4 0.5 collective-permute-start.23
  14.9 2.5 %collective-permute-start.24 = (bf16[256,2048]{1,0:T(8,128)(2,1)}, bf16[256,2048]{1,0:T(8,128)(2,1)}, u32[]{:S(2)}, u32[]{:S(2)}) collective-permute-start(bf16[256,2048]{1,0:T(8,128)(2,1)} %down_hbm.1), channel_id=1, source_target_pairs={{0,97},{1,0},{2,99},{3,2},{4,101},{5,4},{6,103},{7,6},{8,105},{9,8... | collective-permute-start | bytes 3145736 | tf_op jit(solution)/shard_map/ppermute | solution.py:518
  18.0 0.4 convolution_convert_fusion
  18.5 0.3 fusion
  18.8 0.3 fusion.1
  19.5 0.8 fusion.30.refs_8_
  20.4 0.7 collective-permute-start.7
  21.1 1.2 %collective-permute-start.8 = (bf16[128,128]{1,0:T(8,128)(2,1)S(1)}, bf16[128,128]{1,0:T(8,128)(2,1)S(1)}, u32[]{:S(2)}, u32[]{:S(2)}) collective-permute-start(bf16[128,128]{1,0:T(8,128)(2,1)S(1)} %fusion.30.refs_8_), channel_id=1, source_target_pairs={{0,4},{1,5},{2,6},{3,7},{4,0},{5,1},{6,2},{7,3},{8,12},{9,13},{10,... | collective-permute-start | bytes 98312 | tf_op jit(solution)/shard_map/ppermute | solution.py:35
  22.4 3.2 %collective-permute-done.7.refs_9_ = bf16[128,128]{1,0:T(8,128)(2,1)S(1)} collective-permute-done((bf16[128,128]{1,0:T(8,128)(2,1)S(1)}, bf16[128,128]{1,0:T(8,128)(2,1)S(1)}, u32[]{:S(2)}, u32[]{:S(2)}) %collective-permute-start.7) | collective-permute-done | bytes 32800 | tf_op jit(solution)/shard_map/ppermute | solution.py:35
  25.6 1.0 collective-permute-done.8.refs_10_
  26.5 2.9 %collective-permute-done.9.refs_11_ = bf16[128,128]{1,0:T(8,128)(2,1)S(1)} collective-permute-done((bf16[128,128]{1,0:T(8,128)(2,1)S(1)}, bf16[128,128]{1,0:T(8,128)(2,1)S(1)}, u32[]{:S(2)}, u32[]{:S(2)}) %collective-permute-start.9) | collective-permute-done | bytes 32800 | tf_op jit(solution)/shard_map/ppermute | solution.py:35
  29.5 0.5 collective-permute-start.12
  30.0 0.7 collective-permute-done.11.refs_13_
  30.9 2.2 %copy-done.1 = bf16[1024,2048]{1,0:T(8,128)(2,1)S(1)} copy-done((bf16[1024,2048]{1,0:T(8,128)(2,1)S(1)}, bf16[1024,2048]{1,0:T(8,128)(2,1)}, u32[]{:S(2)}) %copy-start.1) | copy-done | bytes 4194328
  33.0 0.3 pull_weight.1.refs_16_
  33.4 0.3 slot_tables.1
  33.7 1.6 %out_proj_norm.1 = (bf16[16,2048]{1,0:T(8,128)(2,1)S(1)}, f32[16,2048]{1,0:T(8,128)S(1)}, bf16[128,2048]{1,0:T(8,128)(2,1)S(1)}) custom-call(s32[1]{0:T(128)} %bitcast.place, bf16[128,256]{1,0:T(8,128)(2,1)S(1)} %copy-done.3, bf16[128,256]{1,0:T(8,128)(2,1)S(1)} %collective-permute-done.refs_1_, bf16[128,256]{1,0:T(8,128)(2,1)S(1)} %collective-permute-done.1.refs_2_, ...), custom_call_target="tpu_custom_call" | custom-call | tf_op jit(solution)/shard_map/out_proj_norm/pallas_call | solution.py:380
  35.3 16.6 %all_to_all.15 = bf16[16,8,2048]{2,1,0:T(8,128)(2,1)} all-to-all(bf16[16,8,2048]{2,1,0:T(8,128)(2,1)S(1)} %bitcast.95), channel_id=1, replica_groups=mesh['ep'=16,'tp'=8] {'ep'}, dimensions={0} | all-to-all | bytes 1048576 | tf_op jit(solution)/shard_map/all_to_all | solution.py:542
  51.9 4.2 %expert_mlp.1 = bf16[128,2048]{1,0:T(8,128)(2,1)} custom-call(bf16[128,2048]{1,0:T(8,128)(2,1)} %bitcast.114, bf16[8,256,512]{2,1,0:T(8,128)(2,1)} %bitcast.115, bf16[8,256,512]{2,1,0:T(8,128)(2,1)} %bitcast.116, bf16[512,2048]{1,0:T(8,128)(2,1)} %bitcast.117), custom_call_target="tpu_custom_call" | custom-call | tf_op jit(solution)/shard_map/expert_mlp/pallas_call | solution.py:189
  56.1 7.2 %all-to-all-start.1 = ((bf16[16,8,2048]{2,1,0:T(8,128)(2,1)}), bf16[16,8,2048]{2,1,0:T(8,128)(2,1)S(1)}, u32[]{:S(2)}, u32[]{:S(2)}) async-start(bf16[16,8,2048]{2,1,0:T(8,128)(2,1)} %bitcast.113), calls=%async_computation.1 | async-start | bytes 1048576 | tf_op jit(solution)/shard_map/all_to_all | solution.py:547
  63.4 0.5 collective-permute-start.26
  64.0 1.9 %collective-permute-start.18 = (bf16[16,2048]{1,0:T(8,128)(2,1)S(1)}, bf16[16,2048]{1,0:T(8,128)(2,1)S(1)}, u32[]{:S(2)}, u32[]{:S(2)}) collective-permute-start(bf16[16,2048]{1,0:T(8,128)(2,1)S(1)} %get-tuple-element.11.refs_0_), channel_id=1, source_target_pairs={{0,8},{8,16},{16,24},{24,0},{32,40},{40,48},{48,56},{56,32},{64,72... | collective-permute-start | bytes 196616 | tf_op jit(solution)/shard_map/ppermute | solution.py:539
  65.9 2.8 %collective-permute-start.19 = (bf16[16,2048]{1,0:T(8,128)(2,1)S(1)}, bf16[16,2048]{1,0:T(8,128)(2,1)S(1)}, u32[]{:S(2)}, u32[]{:S(2)}) collective-permute-start(bf16[16,2048]{1,0:T(8,128)(2,1)S(1)} %get-tuple-element.11.refs_0_), channel_id=1, source_target_pairs={{0,16},{8,24},{16,0},{24,8},{32,48},{40,56},{48,32},{56,40},{64,80... | collective-permute-start | bytes 196616 | tf_op jit(solution)/shard_map/ppermute | solution.py:539
  68.7 4.4 %collective-permute-done.18.refs_1_ = bf16[16,2048]{1,0:T(8,128)(2,1)S(1)} collective-permute-done((bf16[16,2048]{1,0:T(8,128)(2,1)S(1)}, bf16[16,2048]{1,0:T(8,128)(2,1)S(1)}, u32[]{:S(2)}, u32[]{:S(2)}) %collective-permute-start.18) | collective-permute-done | bytes 65568 | tf_op jit(solution)/shard_map/ppermute | solution.py:539
  73.1 0.9 collective-permute-start.20
  74.0 0.7 pad_add_fusion.place
  74.9 2.4 %collective-permute-done.20.refs_3_ = bf16[16,2048]{1,0:T(8,128)(2,1)S(1)} collective-permute-done((bf16[16,2048]{1,0:T(8,128)(2,1)S(1)}, bf16[16,2048]{1,0:T(8,128)(2,1)S(1)}, u32[]{:S(2)}, u32[]{:S(2)}) %collective-permute-start.20) | collective-permute-done | bytes 65568 | tf_op jit(solution)/shard_map/ppermute | solution.py:539
  77.3 0.3 join_rows.1.line_hbm
  77.7 1.5 %collective-permute-start.21 = (bf16[64,2048]{1,0:T(8,128)(2,1)S(1)}, bf16[64,2048]{1,0:T(8,128)(2,1)}, u32[]{:S(2)}, u32[]{:S(2)}) collective-permute-start(bf16[64,2048]{1,0:T(8,128)(2,1)S(1)} %join_rows.1.line_hbm), channel_id=1, source_target_pairs={{0,32},{8,40},{16,48},{24,56},{32,0},{40,8},{48,16},{56,24},{64,96... | collective-permute-start | bytes 786440 | tf_op jit(solution)/shard_map/ppermute | solution.py:541
  79.2 0.3 fusion.10
  79.7 0.8 pad_maximum_fusion
  80.7 3.6 %collective-permute-done.21.pair_hbm = bf16[64,2048]{1,0:T(8,128)(2,1)} collective-permute-done((bf16[64,2048]{1,0:T(8,128)(2,1)S(1)}, bf16[64,2048]{1,0:T(8,128)(2,1)}, u32[]{:S(2)}, u32[]{:S(2)}) %collective-permute-start.21) | collective-permute-done | bytes 262176 | tf_op jit(solution)/shard_map/ppermute | solution.py:541
  84.3 5.5 %shared_mlp.1 = bf16[128,2048]{1,0:T(8,128)(2,1)} custom-call(s32[2]{0:T(128)} %pad_add_fusion.place, bf16[64,2048]{1,0:T(8,128)(2,1)} %copy-done.2, bf16[64,2048]{1,0:T(8,128)(2,1)} %collective-permute-done.21.pair_hbm, bf16[2048,256]{1,0:T(8,128)(2,1)} %gate_hbm.1, bf16[2048,256]{1,0:T(8,128)(2,1)} %up_hbm.1, bf16[256,2048]{1,0:T(8,128)(2,1)} %down_hbm.1, ...), custom_call_target="tpu_custom_call" | custom-call | tf_op jit(solution)/shard_map/shared_mlp/pallas_call | solution.py:304
  89.8 4.3 %all-to-all-start.2 = ((bf16[8,16,2048]{2,1,0:T(8,128)(2,1)}), bf16[8,16,2048]{2,1,0:T(8,128)(2,1)S(1)}, u32[]{:S(2)}, u32[]{:S(2)}) async-start(bf16[8,16,2048]{2,1,0:T(8,128)(2,1)} %bitcast.119), calls=%async_computation.2 | async-start | bytes 1048576 | tf_op jit(solution)/shard_map/all_to_all | solution.py:554
  94.1 1.0 fusion.49
  95.2 0.8 collective-permute-start.15
  95.9 0.8 collective-permute-start.16
  96.7 2.0 %collective-permute-start.17 = (bf16[16,2048]{1,0:T(8,128)(2,1)S(1)}, bf16[16,2048]{1,0:T(8,128)(2,1)S(1)}, u32[]{:S(2)}, u32[]{:S(2)}) collective-permute-start(bf16[16,2048]{1,0:T(8,128)(2,1)S(1)} %get-tuple-element.21), channel_id=1, source_target_pairs={{0,6},{1,7},{2,0},{3,1},{4,2},{5,3},{6,4},{7,5},{8,14},{9,15},{10,... | collective-permute-start | bytes 196616 | tf_op jit(solution)/shard_map/ppermute | solution.py:576
  98.7 4.1 %all-to-all-done.2 = bf16[8,16,2048]{2,1,0:T(8,128)(2,1)S(1)} async-done(((bf16[8,16,2048]{2,1,0:T(8,128)(2,1)}), bf16[8,16,2048]{2,1,0:T(8,128)(2,1)S(1)}, u32[]{:S(2)}, u32[]{:S(2)}) %all-to-all-start.2) | async-done | bytes 524320 | tf_op jit(solution)/shard_map/all_to_all | solution.py:554
  102.9 0.7 fusion.22
  (81 shorter events, 2.3 us)
Async XLA Ops:
  0.6 17.3 %copy-start = (bf16[2048,128]{1,0:T(8,128)(2,1)S(1)}, bf16[2048,128]{1,0:T(8,128)(2,1)}, u32[]{:S(2)}) copy-start(bf16[2048,128]{1,0:T(8,128)(2,1)} %param.23) | copy-start | bytes 1572868
  0.6 16.8 %copy-start.3 = (bf16[128,256]{1,0:T(8,128)(2,1)S(1)}, bf16[128,256]{1,0:T(8,128)(2,1)}, u32[]{:S(2)}) copy-start(bf16[128,256]{1,0:T(8,128)(2,1)} %refs_0_.1) | copy-start | bytes 196612
  0.7 13.7 %copy-start.7 = (bf16[2048,256]{1,0:T(8,128)(2,1)S(1)}, bf16[2048,256]{1,0:T(8,128)(2,1)}, u32[]{:S(2)}) copy-start(bf16[2048,256]{1,0:T(8,128)(2,1)} %up_hbm.1) | copy-start | bytes 3145732
  0.7 11.9 %collective-permute-start = (bf16[128,256]{1,0:T(8,128)(2,1)}, bf16[128,256]{1,0:T(8,128)(2,1)S(1)}, u32[]{:S(2)}, u32[]{:S(2)}) collective-permute-start(bf16[128,256]{1,0:T(8,128)(2,1)} %refs_0_.1), channel_id=1, source_target_pairs={{0,2},{1,3},{2,4},{3,5},{4,6},{5,7},{6,0},{7,1},{8,10},{9,11},{10,... | collective-permute-start | bytes 196616 | tf_op jit(solution)/shard_map/ppermute | solution.py:35
  2.4 10.2 %collective-permute-start.1 = (bf16[128,256]{1,0:T(8,128)(2,1)}, bf16[128,256]{1,0:T(8,128)(2,1)S(1)}, u32[]{:S(2)}, u32[]{:S(2)}) collective-permute-start(bf16[128,256]{1,0:T(8,128)(2,1)} %refs_0_.1), channel_id=1, source_target_pairs={{0,4},{1,5},{2,6},{3,7},{4,0},{5,1},{6,2},{7,3},{8,12},{9,13},{10,... | collective-permute-start | bytes 196616 | tf_op jit(solution)/shard_map/ppermute | solution.py:35
  5.3 7.8 %collective-permute-start.2 = (bf16[128,256]{1,0:T(8,128)(2,1)}, bf16[128,256]{1,0:T(8,128)(2,1)S(1)}, u32[]{:S(2)}, u32[]{:S(2)}) collective-permute-start(bf16[128,256]{1,0:T(8,128)(2,1)} %refs_0_.1), channel_id=1, source_target_pairs={{0,6},{1,7},{2,0},{3,1},{4,2},{5,3},{6,4},{7,5},{8,14},{9,15},{10,... | collective-permute-start | bytes 196616 | tf_op jit(solution)/shard_map/ppermute | solution.py:35
  6.7 7.7 %collective-permute-start.3 = (bf16[128,256]{1,0:T(8,128)(2,1)}, bf16[128,256]{1,0:T(8,128)(2,1)S(1)}, u32[]{:S(2)}, u32[]{:S(2)}) collective-permute-start(bf16[128,256]{1,0:T(8,128)(2,1)} %refs_0_.1), channel_id=1, source_target_pairs={{0,1},{1,0},{2,3},{3,2},{4,5},{5,4},{6,7},{7,6},{8,9},{9,8},{10,11... | collective-permute-start | bytes 196616 | tf_op jit(solution)/shard_map/ppermute | solution.py:37
  6.7 56.6 %collective-permute-start.22 = (bf16[2048,256]{1,0:T(8,128)(2,1)}, bf16[2048,256]{1,0:T(8,128)(2,1)}, u32[]{:S(2)}, u32[]{:S(2)}) collective-permute-start(bf16[2048,256]{1,0:T(8,128)(2,1)} %gate_hbm.1), channel_id=1, source_target_pairs={{0,97},{1,0},{2,99},{3,2},{4,101},{5,4},{6,103},{7,6},{8,105},{9,8... | collective-permute-start | bytes 3145736 | tf_op jit(solution)/shard_map/ppermute | solution.py:518
  11.9 6.1 %copy-start.12 = (f32[2048]{0:T(1024)S(1)}, f32[2048]{0:T(1024)}, u32[]{:S(2)}) copy-start(f32[2048]{0:T(1024)} %param.22) | copy-start | bytes 24580
  12.6 2.3 %collective-permute-start.4 = (bf16[128,256]{1,0:T(8,128)(2,1)S(1)}, bf16[128,256]{1,0:T(8,128)(2,1)S(1)}, u32[]{:S(2)}, u32[]{:S(2)}) collective-permute-start(bf16[128,256]{1,0:T(8,128)(2,1)S(1)} %collective-permute-done.refs_1_), channel_id=1, source_target_pairs={{0,1},{1,0},{2,3},{3,2},{4,5},{5,4},{6,7},{7,6},{8,9},{9,8},{10,11... | collective-permute-start | bytes 196616 | tf_op jit(solution)/shard_map/ppermute | solution.py:37
  12.6 4.8 %collective-permute-start.5 = (bf16[128,256]{1,0:T(8,128)(2,1)S(1)}, bf16[128,256]{1,0:T(8,128)(2,1)S(1)}, u32[]{:S(2)}, u32[]{:S(2)}) collective-permute-start(bf16[128,256]{1,0:T(8,128)(2,1)S(1)} %collective-permute-done.1.refs_2_), channel_id=1, source_target_pairs={{0,1},{1,0},{2,3},{3,2},{4,5},{5,4},{6,7},{7,6},{8,9},{9,8},{10,11... | collective-permute-start | bytes 196616 | tf_op jit(solution)/shard_map/ppermute | solution.py:37
  13.1 4.3 %collective-permute-start.6 = (bf16[128,256]{1,0:T(8,128)(2,1)S(1)}, bf16[128,256]{1,0:T(8,128)(2,1)S(1)}, u32[]{:S(2)}, u32[]{:S(2)}) collective-permute-start(bf16[128,256]{1,0:T(8,128)(2,1)S(1)} %collective-permute-done.2.refs_3_), channel_id=1, source_target_pairs={{0,1},{1,0},{2,3},{3,2},{4,5},{5,4},{6,7},{7,6},{8,9},{9,8},{10,11... | collective-permute-start | bytes 196616 | tf_op jit(solution)/shard_map/ppermute | solution.py:37
  14.4 49.0 %collective-permute-start.23 = (bf16[2048,256]{1,0:T(8,128)(2,1)S(1)}, bf16[2048,256]{1,0:T(8,128)(2,1)}, u32[]{:S(2)}, u32[]{:S(2)}) collective-permute-start(bf16[2048,256]{1,0:T(8,128)(2,1)S(1)} %copy-done.7), channel_id=1, source_target_pairs={{0,1},{1,96},{2,3},{3,98},{4,5},{5,100},{6,7},{7,102},{8,9},{9,104... | collective-permute-start | bytes 3145736 | tf_op jit(solution)/shard_map/ppermute | solution.py:518
  14.9 49.0 %collective-permute-start.24 = (bf16[256,2048]{1,0:T(8,128)(2,1)}, bf16[256,2048]{1,0:T(8,128)(2,1)}, u32[]{:S(2)}, u32[]{:S(2)}) collective-permute-start(bf16[256,2048]{1,0:T(8,128)(2,1)} %down_hbm.1), channel_id=1, source_target_pairs={{0,97},{1,0},{2,99},{3,2},{4,101},{5,4},{6,103},{7,6},{8,105},{9,8... | collective-permute-start | bytes 3145736 | tf_op jit(solution)/shard_map/ppermute | solution.py:518
  17.4 1.0 %copy-start.8 = (f32[2,8,64,16]{2,3,1,0:T(8,128)S(1)}, f32[2,8,64,16]{2,3,1,0:T(8,128)}, u32[]{:S(2)}) copy-start(f32[2,8,64,16]{2,3,1,0:T(8,128)} %param.28) | copy-start | bytes 196612
  17.7 1.4 %copy-start.9 = (f32[2,8,16,64]{3,2,1,0:T(8,128)S(1)}, f32[2,8,16,64]{3,2,1,0:T(8,128)}, u32[]{:S(2)}) copy-start(f32[2,8,16,64]{3,2,1,0:T(8,128)} %param.29) | copy-start | bytes 196612
  18.4 0.7 copy-start.10
  19.5 13.8 %copy-start.5 = (s32[128,4]{0,1:T(4,128)S(1)}, s32[128,4]{0,1:T(4,128)}, u32[]{:S(2)}) copy-start(s32[128,4]{0,1:T(4,128)} %param.34) | copy-start | bytes 6148
  19.5 13.8 %copy-start.6 = (f32[128,4]{0,1:T(4,128)S(1)}, f32[128,4]{0,1:T(4,128)}, u32[]{:S(2)}) copy-start(f32[128,4]{0,1:T(4,128)} %param.35) | copy-start | bytes 6148
  19.5 14.1 %copy-start.4 = (f32[2048]{0:T(1024)S(1)}, f32[2048]{0:T(1024)}, u32[]{:S(2)}) copy-start(f32[2048]{0:T(1024)} %param.32) | copy-start | bytes 24580
  20.4 5.2 %collective-permute-start.7 = (bf16[128,128]{1,0:T(8,128)(2,1)S(1)}, bf16[128,128]{1,0:T(8,128)(2,1)S(1)}, u32[]{:S(2)}, u32[]{:S(2)}) collective-permute-start(bf16[128,128]{1,0:T(8,128)(2,1)S(1)} %fusion.30.refs_8_), channel_id=1, source_target_pairs={{0,2},{1,3},{2,4},{3,5},{4,6},{5,7},{6,0},{7,1},{8,10},{9,11},{10,... | collective-permute-start | bytes 98312 | tf_op jit(solution)/shard_map/ppermute | solution.py:35
  21.1 5.4 %collective-permute-start.8 = (bf16[128,128]{1,0:T(8,128)(2,1)S(1)}, bf16[128,128]{1,0:T(8,128)(2,1)S(1)}, u32[]{:S(2)}, u32[]{:S(2)}) collective-permute-start(bf16[128,128]{1,0:T(8,128)(2,1)S(1)} %fusion.30.refs_8_), channel_id=1, source_target_pairs={{0,4},{1,5},{2,6},{3,7},{4,0},{5,1},{6,2},{7,3},{8,12},{9,13},{10,... | collective-permute-start | bytes 98312 | tf_op jit(solution)/shard_map/ppermute | solution.py:35
  25.6 3.9 %collective-permute-start.9 = (bf16[128,128]{1,0:T(8,128)(2,1)S(1)}, bf16[128,128]{1,0:T(8,128)(2,1)S(1)}, u32[]{:S(2)}, u32[]{:S(2)}) collective-permute-start(bf16[128,128]{1,0:T(8,128)(2,1)S(1)} %fusion.30.refs_8_), channel_id=1, source_target_pairs={{0,6},{1,7},{2,0},{3,1},{4,2},{5,3},{6,4},{7,5},{8,14},{9,15},{10,... | collective-permute-start | bytes 98312 | tf_op jit(solution)/shard_map/ppermute | solution.py:35
  26.5 3.0 %collective-permute-start.10 = (bf16[128,128]{1,0:T(8,128)(2,1)S(1)}, bf16[128,128]{1,0:T(8,128)(2,1)S(1)}, u32[]{:S(2)}, u32[]{:S(2)}) collective-permute-start(bf16[128,128]{1,0:T(8,128)(2,1)S(1)} %fusion.30.refs_8_), channel_id=1, source_target_pairs={{0,1},{1,0},{2,3},{3,2},{4,5},{5,4},{6,7},{7,6},{8,9},{9,8},{10,11... | collective-permute-start | bytes 98312 | tf_op jit(solution)/shard_map/ppermute | solution.py:37
  29.5 1.2 %collective-permute-start.11 = (bf16[128,128]{1,0:T(8,128)(2,1)S(1)}, bf16[128,128]{1,0:T(8,128)(2,1)S(1)}, u32[]{:S(2)}, u32[]{:S(2)}) collective-permute-start(bf16[128,128]{1,0:T(8,128)(2,1)S(1)} %collective-permute-done.7.refs_9_), channel_id=1, source_target_pairs={{0,1},{1,0},{2,3},{3,2},{4,5},{5,4},{6,7},{7,6},{8,9},{9,8},{10,11... | collective-permute-start | bytes 98312 | tf_op jit(solution)/shard_map/ppermute | solution.py:37
  29.5 4.2 %collective-permute-start.12 = (bf16[128,128]{1,0:T(8,128)(2,1)S(1)}, bf16[128,128]{1,0:T(8,128)(2,1)S(1)}, u32[]{:S(2)}, u32[]{:S(2)}) collective-permute-start(bf16[128,128]{1,0:T(8,128)(2,1)S(1)} %collective-permute-done.8.refs_10_), channel_id=1, source_target_pairs={{0,1},{1,0},{2,3},{3,2},{4,5},{5,4},{6,7},{7,6},{8,9},{9,8},{10,11... | collective-permute-start | bytes 98312 | tf_op jit(solution)/shard_map/ppermute | solution.py:37
  30.7 3.0 %collective-permute-start.13 = (bf16[128,128]{1,0:T(8,128)(2,1)S(1)}, bf16[128,128]{1,0:T(8,128)(2,1)S(1)}, u32[]{:S(2)}, u32[]{:S(2)}) collective-permute-start(bf16[128,128]{1,0:T(8,128)(2,1)S(1)} %collective-permute-done.9.refs_11_), channel_id=1, source_target_pairs={{0,1},{1,0},{2,3},{3,2},{4,5},{5,4},{6,7},{7,6},{8,9},{9,8},{10,11... | collective-permute-start | bytes 98312 | tf_op jit(solution)/shard_map/ppermute | solution.py:37
  30.8 2.2 %copy-start.1 = (bf16[1024,2048]{1,0:T(8,128)(2,1)S(1)}, bf16[1024,2048]{1,0:T(8,128)(2,1)}, u32[]{:S(2)}) copy-start(bf16[1024,2048]{1,0:T(8,128)(2,1)} %weight_hbm.1) | copy-start | bytes 12582916
  51.9 14.0 %copy-start.11 = (bf16[2048]{0:T(1024)(128)(2,1)S(1)}, bf16[2048]{0:T(1024)(128)(2,1)}, u32[]{:S(2)}) copy-start(bf16[2048]{0:T(1024)(128)(2,1)} %param.33) | copy-start | bytes 12292
  56.1 23.2 %all-to-all-start.1 = ((bf16[16,8,2048]{2,1,0:T(8,128)(2,1)}), bf16[16,8,2048]{2,1,0:T(8,128)(2,1)S(1)}, u32[]{:S(2)}, u32[]{:S(2)}) async-start(bf16[16,8,2048]{2,1,0:T(8,128)(2,1)} %bitcast.113), calls=%async_computation.1 | async-start | bytes 1048576 | tf_op jit(solution)/shard_map/all_to_all | solution.py:547
  63.3 21.0 %collective-permute-start.25 = (bf16[2048,256]{1,0:T(8,128)(2,1)}, bf16[2048,256]{1,0:T(8,128)(2,1)}, u32[]{:S(2)}, u32[]{:S(2)}) collective-permute-start(bf16[2048,256]{1,0:T(8,128)(2,1)} %collective-permute-done.22.gate_far), channel_id=1, source_target_pairs={{0,1},{1,0},{2,3},{3,2},{4,5},{5,4},{6,7},{7,6},{8,9},{9,8},{10,11... | collective-permute-start | bytes 3145736 | tf_op jit(solution)/shard_map/ppermute | solution.py:521
  63.4 20.9 %collective-permute-start.26 = (bf16[2048,256]{1,0:T(8,128)(2,1)}, bf16[2048,256]{1,0:T(8,128)(2,1)}, u32[]{:S(2)}, u32[]{:S(2)}) collective-permute-start(bf16[2048,256]{1,0:T(8,128)(2,1)} %collective-permute-done.23.up_far), channel_id=1, source_target_pairs={{0,1},{1,0},{2,3},{3,2},{4,5},{5,4},{6,7},{7,6},{8,9},{9,8},{10,11... | collective-permute-start | bytes 3145736 | tf_op jit(solution)/shard_map/ppermute | solution.py:521
  63.9 20.4 %collective-permute-start.27 = (bf16[256,2048]{1,0:T(8,128)(2,1)}, bf16[256,2048]{1,0:T(8,128)(2,1)}, u32[]{:S(2)}, u32[]{:S(2)}) collective-permute-start(bf16[256,2048]{1,0:T(8,128)(2,1)} %collective-permute-done.24.down_far), channel_id=1, source_target_pairs={{0,1},{1,0},{2,3},{3,2},{4,5},{5,4},{6,7},{7,6},{8,9},{9,8},{10,11... | collective-permute-start | bytes 3145736 | tf_op jit(solution)/shard_map/ppermute | solution.py:521
  64.0 9.1 %collective-permute-start.18 = (bf16[16,2048]{1,0:T(8,128)(2,1)S(1)}, bf16[16,2048]{1,0:T(8,128)(2,1)S(1)}, u32[]{:S(2)}, u32[]{:S(2)}) collective-permute-start(bf16[16,2048]{1,0:T(8,128)(2,1)S(1)} %get-tuple-element.11.refs_0_), channel_id=1, source_target_pairs={{0,8},{8,16},{16,24},{24,0},{32,40},{40,48},{48,56},{56,32},{64,72... | collective-permute-start | bytes 196616 | tf_op jit(solution)/shard_map/ppermute | solution.py:539
  65.9 9.0 %collective-permute-start.19 = (bf16[16,2048]{1,0:T(8,128)(2,1)S(1)}, bf16[16,2048]{1,0:T(8,128)(2,1)S(1)}, u32[]{:S(2)}, u32[]{:S(2)}) collective-permute-start(bf16[16,2048]{1,0:T(8,128)(2,1)S(1)} %get-tuple-element.11.refs_0_), channel_id=1, source_target_pairs={{0,16},{8,24},{16,0},{24,8},{32,48},{40,56},{48,32},{56,40},{64,80... | collective-permute-start | bytes 196616 | tf_op jit(solution)/shard_map/ppermute | solution.py:539
  73.1 4.3 %collective-permute-start.20 = (bf16[16,2048]{1,0:T(8,128)(2,1)S(1)}, bf16[16,2048]{1,0:T(8,128)(2,1)S(1)}, u32[]{:S(2)}, u32[]{:S(2)}) collective-permute-start(bf16[16,2048]{1,0:T(8,128)(2,1)S(1)} %get-tuple-element.11.refs_0_), channel_id=1, source_target_pairs={{0,24},{8,0},{16,8},{24,16},{32,56},{40,32},{48,40},{56,48},{64,88... | collective-permute-start | bytes 196616 | tf_op jit(solution)/shard_map/ppermute | solution.py:539
  77.7 6.6 %copy-start.2 = (bf16[64,2048]{1,0:T(8,128)(2,1)}, bf16[64,2048]{1,0:T(8,128)(2,1)S(1)}, u32[]{:S(2)}) copy-start(bf16[64,2048]{1,0:T(8,128)(2,1)S(1)} %join_rows.1.line_hbm) | copy-start | bytes 786436
  77.7 6.6 %collective-permute-start.21 = (bf16[64,2048]{1,0:T(8,128)(2,1)S(1)}, bf16[64,2048]{1,0:T(8,128)(2,1)}, u32[]{:S(2)}, u32[]{:S(2)}) collective-permute-start(bf16[64,2048]{1,0:T(8,128)(2,1)S(1)} %join_rows.1.line_hbm), channel_id=1, source_target_pairs={{0,32},{8,40},{16,48},{24,56},{32,0},{40,8},{48,16},{56,24},{64,96... | collective-permute-start | bytes 786440 | tf_op jit(solution)/shard_map/ppermute | solution.py:541
  79.6 14.5 %collective-permute-start.14 = (bf16[64,2048]{1,0:T(8,128)(2,1)S(1)}, bf16[64,2048]{1,0:T(8,128)(2,1)}, u32[]{:S(2)}, u32[]{:S(2)}) collective-permute-start(bf16[64,2048]{1,0:T(8,128)(2,1)S(1)} %slice.94), channel_id=1, source_target_pairs={{0,1},{1,0},{2,3},{3,2},{4,5},{5,4},{6,7},{7,6},{8,9},{9,8},{10,11... | collective-permute-start | bytes 786440 | tf_op jit(solution)/shard_map/ppermute | solution.py:571
  89.8 13.0 %all-to-all-start.2 = ((bf16[8,16,2048]{2,1,0:T(8,128)(2,1)}), bf16[8,16,2048]{2,1,0:T(8,128)(2,1)S(1)}, u32[]{:S(2)}, u32[]{:S(2)}) async-start(bf16[8,16,2048]{2,1,0:T(8,128)(2,1)} %bitcast.119), calls=%async_computation.2 | async-start | bytes 1048576 | tf_op jit(solution)/shard_map/all_to_all | solution.py:554
  95.2 7.7 %collective-permute-start.15 = (bf16[16,2048]{1,0:T(8,128)(2,1)S(1)}, bf16[16,2048]{1,0:T(8,128)(2,1)S(1)}, u32[]{:S(2)}, u32[]{:S(2)}) collective-permute-start(bf16[16,2048]{1,0:T(8,128)(2,1)S(1)} %get-tuple-element.20), channel_id=1, source_target_pairs={{0,2},{1,3},{2,4},{3,5},{4,6},{5,7},{6,0},{7,1},{8,10},{9,11},{10,... | collective-permute-start | bytes 196616 | tf_op jit(solution)/shard_map/ppermute | solution.py:576
  95.9 7.0 %collective-permute-start.16 = (bf16[16,2048]{1,0:T(8,128)(2,1)S(1)}, bf16[16,2048]{1,0:T(8,128)(2,1)S(1)}, u32[]{:S(2)}, u32[]{:S(2)}) collective-permute-start(bf16[16,2048]{1,0:T(8,128)(2,1)S(1)} %get-tuple-element.22), channel_id=1, source_target_pairs={{0,4},{1,5},{2,6},{3,7},{4,0},{5,1},{6,2},{7,3},{8,12},{9,13},{10,... | collective-permute-start | bytes 196616 | tf_op jit(solution)/shard_map/ppermute | solution.py:576
  96.7 6.2 %collective-permute-start.17 = (bf16[16,2048]{1,0:T(8,128)(2,1)S(1)}, bf16[16,2048]{1,0:T(8,128)(2,1)S(1)}, u32[]{:S(2)}, u32[]{:S(2)}) collective-permute-start(bf16[16,2048]{1,0:T(8,128)(2,1)S(1)} %get-tuple-element.21), channel_id=1, source_target_pairs={{0,6},{1,7},{2,0},{3,1},{4,2},{5,3},{6,4},{7,5},{8,14},{9,15},{10,... | collective-permute-start | bytes 196616 | tf_op jit(solution)/shard_map/ppermute | solution.py:576

commit v2 on v1

--- a/solution.py
+++ b/solution.py
@@ -211,6 +211,7 @@
 
 
 def shared_body(
+    here,
     place,
     line_hbm,
     pair_hbm,
@@ -233,8 +234,8 @@
     *,
     side,
 ):
-    here, core = place[0], lax.rem(place[1], cores)
-    z, x = lax.rem(lax.div(here, side), 2), lax.rem(here, side)
+    core = lax.rem(place[0], cores)
+    z, x = lax.rem(lax.div(here[0], side), 2), lax.rem(here[0], side)
     order = [
         lax.rem(z + i, 2) * side + lax.rem(x + side - j, side) for i in range(2) for j in range(side)
     ]
@@ -298,13 +299,13 @@
         store.wait()
 
 
-def shared_kernel(place, line, pair, own, far, swap, side):
+def shared_kernel(here, place, line, pair, own, far, swap, side):
     count, width = line.shape
     inner = own[0].shape[1]
     return pl.pallas_call(
         functools.partial(shared_body, side=side),
         out_shape=jax.ShapeDtypeStruct((count * 2, width), bf16),
-        in_specs=[in_smem()] + [in_hbm()] * 11,
+        in_specs=[in_smem()] * 2 + [in_hbm()] * 11,
         out_specs=in_hbm(),
         scratch_shapes=[
             pltpu.VMEM((2, width, inner), bf16),
@@ -316,7 +317,7 @@
         ],
         compiler_params=pltpu.CompilerParams(vmem_limit_bytes=60 * 1024 * 1024),
         name="shared_mlp",
-    )(place, line, pair, *own, *far, *swap)
+    )(here, place, line, pair, *own, *far, *swap)
 
 
 def pull_body(weight_hbm, out, sem):
@@ -514,10 +515,9 @@
 
     resid_mine, resid_other = hop_gather(residual, tp_count)
     own = (shared_gate, shared_up, shared_down)
-    far = [
-        lax.ppermute(w, ("ep", "tp"), weight_moves(ep_count, tp_count, core))
-        for w, core in zip(own, (0, 1, 0))
-    ]
+    far = []
+    for w, core in zip(own, (0, 1, 0)):
+        far.append(lax.ppermute(w, ("ep", "tp"), weight_moves(ep_count, tp_count, core)))
     swap = [lax.ppermute(w, "tp", core_swap(tp_count)) for w in far]
     full_resid = natural_blocks(jnp.stack(resid_mine), jnp.stack(resid_other), tp_count, place).astype(f32)
     normed = layer_norm(full_resid, in_gain).astype(bf16)
@@ -549,8 +549,9 @@
     ).reshape(slots, width)
 
     group = 2 * side
-    where = jnp.stack([lax.axis_index("ep"), place]).astype(jnp.int32)
-    partial_rows = shared_kernel(where, line, pair, own, far, swap, side)
+    partial_rows = shared_kernel(
+        lax.axis_index("ep").reshape(1), place.reshape(1), line, pair, own, far, swap, side
+    )
     partial_back = lax.all_to_all(
         partial_rows.reshape(group, per_dev, width),
         "ep",
@@ -561,15 +562,16 @@
     )
     shared = jnp.sum(partial_back.astype(f32), axis=0)
 
-    both = lax.dot_general(
-        share,
-        jnp.concatenate([returned, returned], axis=0),
-        (((0,), (0,)), ((), ())),
-        preferred_element_type=f32,
-    )
     half = per_dev * chips
-    theirs = lax.ppermute(both[half:].astype(bf16), "tp", core_swap(tp_count))
-    pair = both[:half] + theirs.astype(f32)
+    doubled = jnp.concatenate([returned, returned], axis=0)
+    send, keep = (
+        lax.dot_general(
+            part, doubled, (((0,), (0,)), ((), ())), preferred_element_type=f32
+        ).astype(bf16)
+        for part in (share[:, half:], share[:, :half])
+    )
+    theirs = lax.ppermute(send, "tp", core_swap(tp_count))
+    pair = keep.astype(f32) + theirs.astype(f32)
     routed = pair[:per_dev]
     pair = pair.astype(bf16)
     for step in range(1, chips):

time: 104 us -> 104 us (level)
  other arithmetic: 5.22 us -> 2.77 us
  matrix products: 1.72 us -> 3.76 us
    dot_general x1 -> x2, matrix products: 0.33 us -> 2.37 us  [layer(): lax.dot_general(part, doubled, (((0,), (0,)), ((), ())), preferred_elemen...]
    unnamed x34 -> x36, local copies, waits for them, and re-layouts: 2.36 us -> 3.32 us
  transfers between devices with their start and end apart: 30 -> 30, of which waited for: 8 -> 8; matrix products, arithmetic and copies ran while one was open for 9% -> 8% of each run, Pallas kernels for 12% -> 11%
where the time goes in v2:
time: 104 us
  starting transfers between devices  39.2 us (38%)
  waiting for transfers between devices  22.2 us (21%)
  blocking collectives  17.3 us (17%)
  Pallas kernels  11.6 us (11%)
  local copies, waits for them, and re-layouts  5.79 us (6%)
  matrix products  3.76 us (4%)
  other arithmetic  2.77 us (3%)
  between operations  1.27 us (1%)
    all_to_all x1, blocking collectives, layer(): lax.all_to_all(outgoing.reshape(ep_count, capacity, width), 'ep', split_a...  17.3 us
    ppermute x6, starting transfers between devices, hop_gather(): lax.ppermute(array, 'tp', y_shift(tp_count, step))  8 us
    ppermute x3, waiting for transfers between devices, layer(): line.append(lax.ppermute(own_mid, 'ep', plane_shift(ep_count, 0, step)))  7.57 us
    all_to_all x1, starting transfers between devices, layer(): lax.all_to_all(result.reshape(ep_count, capacity, width), 'ep', split_axi...  7.2 us
    ppermute x3, starting transfers between devices, layer(): lax.ppermute(w, ('ep', 'tp'), weight_moves(ep_count, tp_count, core))  7.17 us
    ppermute x6, waiting for transfers between devices, hop_gather(): lax.ppermute(array, 'tp', y_shift(tp_count, step))  7.12 us
    ppermute x3, starting transfers between devices, layer(): line.append(lax.ppermute(own_mid, 'ep', plane_shift(ep_count, 0, step)))  5.49 us
    pallas_call x1, Pallas kernels, shared_kernel(): pl.pallas_call(functools.partial(shared_body, side=side), out_shape=jax.S...  4.88 us
  transfers between devices with their start and end apart: 30, of which 8 were waited for; matrix products, arithmetic and copies ran while one was open for 8% of the time, Pallas kernels for 11%

profile of v2, /device:TPU:0, one launch (start us, length us, event | category | flops | bytes accessed | tf_op | source)
XLA Modules:
  0.0 103.9 jit_solution(10377774882879968107)
XLA Ops:
  0.7 1.8 %collective-permute-start = (bf16[128,256]{1,0:T(8,128)(2,1)}, bf16[128,256]{1,0:T(8,128)(2,1)S(1)}, u32[]{:S(2)}, u32[]{:S(2)}) collective-permute-start(bf16[128,256]{1,0:T(8,128)(2,1)} %refs_0_.1), channel_id=1, source_target_pairs={{0,2},{1,3},{2,4},{3,5},{4,6},{5,7},{6,0},{7,1},{8,10},{9,11},{10,... | collective-permute-start | bytes 196616 | tf_op jit(solution)/shard_map/ppermute | solution.py:35
  2.4 2.9 %collective-permute-start.1 = (bf16[128,256]{1,0:T(8,128)(2,1)}, bf16[128,256]{1,0:T(8,128)(2,1)S(1)}, u32[]{:S(2)}, u32[]{:S(2)}) collective-permute-start(bf16[128,256]{1,0:T(8,128)(2,1)} %refs_0_.1), channel_id=1, source_target_pairs={{0,4},{1,5},{2,6},{3,7},{4,0},{5,1},{6,2},{7,3},{8,12},{9,13},{10,... | collective-permute-start | bytes 196616 | tf_op jit(solution)/shard_map/ppermute | solution.py:35
  5.3 1.3 %collective-permute-start.2 = (bf16[128,256]{1,0:T(8,128)(2,1)}, bf16[128,256]{1,0:T(8,128)(2,1)S(1)}, u32[]{:S(2)}, u32[]{:S(2)}) collective-permute-start(bf16[128,256]{1,0:T(8,128)(2,1)} %refs_0_.1), channel_id=1, source_target_pairs={{0,6},{1,7},{2,0},{3,1},{4,2},{5,3},{6,4},{7,5},{8,14},{9,15},{10,... | collective-permute-start | bytes 196616 | tf_op jit(solution)/shard_map/ppermute | solution.py:35
  6.7 4.1 %collective-permute-start.22 = (bf16[2048,256]{1,0:T(8,128)(2,1)}, bf16[2048,256]{1,0:T(8,128)(2,1)}, u32[]{:S(2)}, u32[]{:S(2)}) collective-permute-start(bf16[2048,256]{1,0:T(8,128)(2,1)} %gate_hbm.1), channel_id=1, source_target_pairs={{0,97},{1,0},{2,99},{3,2},{4,101},{5,4},{6,103},{7,6},{8,105},{9,8... | collective-permute-start | bytes 3145736 | tf_op jit(solution)/shard_map/ppermute | solution.py:520
  10.8 1.1 %fusion.51 = (f32[1,128,512]{2,1,0:T(8,128)S(1)}, f32[1,128,512]{2,1,0:T(8,128)S(1)}) fusion(f32[2,128,512]{2,1,0:T(8,128)} %param.24), kind=kLoop, calls=%fused_computation.86 | loop fusion | bytes 1048576 | tf_op jit(solution)/shard_map/slice | solution.py:108
  11.9 0.7 exp.9
  12.6 0.5 collective-permute-start.5
  13.2 0.8 add_divide_fusion
  14.4 0.5 collective-permute-start.23
  14.9 2.5 %collective-permute-start.24 = (bf16[256,2048]{1,0:T(8,128)(2,1)}, bf16[256,2048]{1,0:T(8,128)(2,1)}, u32[]{:S(2)}, u32[]{:S(2)}) collective-permute-start(bf16[256,2048]{1,0:T(8,128)(2,1)} %down_hbm.1), channel_id=1, source_target_pairs={{0,97},{1,0},{2,99},{3,2},{4,101},{5,4},{6,103},{7,6},{8,105},{9,8... | collective-permute-start | bytes 3145736 | tf_op jit(solution)/shard_map/ppermute | solution.py:520
  17.7 0.2 convert_reduce_fusion
  18.0 0.4 convolution_convert_fusion.2
  18.5 0.3 fusion.1
  18.8 0.3 fusion.2
  19.6 0.7 collective-permute-start.7
  20.3 1.2 %collective-permute-start.8 = (bf16[128,128]{1,0:T(8,128)(2,1)S(1)}, bf16[128,128]{1,0:T(8,128)(2,1)S(1)}, u32[]{:S(2)}, u32[]{:S(2)}) collective-permute-start(bf16[128,128]{1,0:T(8,128)(2,1)S(1)} %fusion.27.refs_8_), channel_id=1, source_target_pairs={{0,4},{1,5},{2,6},{3,7},{4,0},{5,1},{6,2},{7,3},{8,12},{9,13},{10,... | collective-permute-start | bytes 98312 | tf_op jit(solution)/shard_map/ppermute | solution.py:35
  21.6 3.2 %collective-permute-done.7.refs_9_ = bf16[128,128]{1,0:T(8,128)(2,1)S(1)} collective-permute-done((bf16[128,128]{1,0:T(8,128)(2,1)S(1)}, bf16[128,128]{1,0:T(8,128)(2,1)S(1)}, u32[]{:S(2)}, u32[]{:S(2)}) %collective-permute-start.7) | collective-permute-done | bytes 32800 | tf_op jit(solution)/shard_map/ppermute | solution.py:35
  24.8 1.0 collective-permute-done.8.refs_10_
  25.8 2.9 %collective-permute-done.9.refs_11_ = bf16[128,128]{1,0:T(8,128)(2,1)S(1)} collective-permute-done((bf16[128,128]{1,0:T(8,128)(2,1)S(1)}, bf16[128,128]{1,0:T(8,128)(2,1)S(1)}, u32[]{:S(2)}, u32[]{:S(2)}) %collective-permute-start.9) | collective-permute-done | bytes 32800 | tf_op jit(solution)/shard_map/ppermute | solution.py:35
  28.7 0.5 collective-permute-start.12
  29.2 0.7 collective-permute-done.11.refs_13_
  30.1 2.2 %copy-done.1 = bf16[1024,2048]{1,0:T(8,128)(2,1)S(1)} copy-done((bf16[1024,2048]{1,0:T(8,128)(2,1)S(1)}, bf16[1024,2048]{1,0:T(8,128)(2,1)}, u32[]{:S(2)}) %copy-start.1) | copy-done | bytes 4194328
  32.3 0.3 pull_weight.1.refs_16_
  32.6 0.3 slot_tables.1
  32.9 1.6 %out_proj_norm.1 = (bf16[16,2048]{1,0:T(8,128)(2,1)S(1)}, f32[16,2048]{1,0:T(8,128)S(1)}, bf16[128,2048]{1,0:T(8,128)(2,1)S(1)}) custom-call(s32[1]{0:T(128)} %bitcast.place, bf16[128,256]{1,0:T(8,128)(2,1)S(1)} %copy-done.3, bf16[128,256]{1,0:T(8,128)(2,1)S(1)} %collective-permute-done.refs_1_, bf16[128,256]{1,0:T(8,128)(2,1)S(1)} %collective-permute-done.1.refs_2_, ...), custom_call_target="tpu_custom_call" | custom-call | tf_op jit(solution)/shard_map/out_proj_norm/pallas_call | solution.py:381
  34.5 17.3 %all_to_all.15 = bf16[16,8,2048]{2,1,0:T(8,128)(2,1)} all-to-all(bf16[16,8,2048]{2,1,0:T(8,128)(2,1)S(1)} %bitcast.94), channel_id=1, replica_groups=mesh['ep'=16,'tp'=8] {'ep'}, dimensions={0} | all-to-all | bytes 1048576 | tf_op jit(solution)/shard_map/all_to_all | solution.py:542
  51.9 4.2 %expert_mlp.1 = bf16[128,2048]{1,0:T(8,128)(2,1)} custom-call(bf16[128,2048]{1,0:T(8,128)(2,1)} %bitcast.113, bf16[8,256,512]{2,1,0:T(8,128)(2,1)} %bitcast.114, bf16[8,256,512]{2,1,0:T(8,128)(2,1)} %bitcast.115, bf16[512,2048]{1,0:T(8,128)(2,1)} %bitcast.116), custom_call_target="tpu_custom_call" | custom-call | tf_op jit(solution)/shard_map/expert_mlp/pallas_call | solution.py:189
  56.1 7.2 %all-to-all-start.1 = ((bf16[16,8,2048]{2,1,0:T(8,128)(2,1)}), bf16[16,8,2048]{2,1,0:T(8,128)(2,1)S(1)}, u32[]{:S(2)}, u32[]{:S(2)}) async-start(bf16[16,8,2048]{2,1,0:T(8,128)(2,1)} %bitcast.112), calls=%async_computation.1 | async-start | bytes 1048576 | tf_op jit(solution)/shard_map/all_to_all | solution.py:547
  63.4 0.5 collective-permute-start.26
  64.0 1.9 %collective-permute-start.18 = (bf16[16,2048]{1,0:T(8,128)(2,1)S(1)}, bf16[16,2048]{1,0:T(8,128)(2,1)S(1)}, u32[]{:S(2)}, u32[]{:S(2)}) collective-permute-start(bf16[16,2048]{1,0:T(8,128)(2,1)S(1)} %get-tuple-element.11.refs_0_), channel_id=1, source_target_pairs={{0,8},{8,16},{16,24},{24,0},{32,40},{40,48},{48,56},{56,32},{64,72... | collective-permute-start | bytes 196616 | tf_op jit(solution)/shard_map/ppermute | solution.py:539
  65.9 2.7 %collective-permute-start.19 = (bf16[16,2048]{1,0:T(8,128)(2,1)S(1)}, bf16[16,2048]{1,0:T(8,128)(2,1)S(1)}, u32[]{:S(2)}, u32[]{:S(2)}) collective-permute-start(bf16[16,2048]{1,0:T(8,128)(2,1)S(1)} %get-tuple-element.11.refs_0_), channel_id=1, source_target_pairs={{0,16},{8,24},{16,0},{24,8},{32,48},{40,56},{48,32},{56,40},{64,80... | collective-permute-start | bytes 196616 | tf_op jit(solution)/shard_map/ppermute | solution.py:539
  68.6 4.5 %collective-permute-done.18.refs_1_ = bf16[16,2048]{1,0:T(8,128)(2,1)S(1)} collective-permute-done((bf16[16,2048]{1,0:T(8,128)(2,1)S(1)}, bf16[16,2048]{1,0:T(8,128)(2,1)S(1)}, u32[]{:S(2)}, u32[]{:S(2)}) %collective-permute-start.18) | collective-permute-done | bytes 65568 | tf_op jit(solution)/shard_map/ppermute | solution.py:539
  73.1 0.9 collective-permute-start.20
  74.3 3.1 %collective-permute-done.20.refs_3_ = bf16[16,2048]{1,0:T(8,128)(2,1)S(1)} collective-permute-done((bf16[16,2048]{1,0:T(8,128)(2,1)S(1)}, bf16[16,2048]{1,0:T(8,128)(2,1)S(1)}, u32[]{:S(2)}, u32[]{:S(2)}) %collective-permute-start.20) | collective-permute-done | bytes 65568 | tf_op jit(solution)/shard_map/ppermute | solution.py:539
  77.3 0.3 join_rows.1.line_hbm
  77.7 1.5 %collective-permute-start.21 = (bf16[64,2048]{1,0:T(8,128)(2,1)S(1)}, bf16[64,2048]{1,0:T(8,128)(2,1)}, u32[]{:S(2)}, u32[]{:S(2)}) collective-permute-start(bf16[64,2048]{1,0:T(8,128)(2,1)S(1)} %join_rows.1.line_hbm), channel_id=1, source_target_pairs={{0,32},{8,40},{16,48},{24,56},{32,0},{40,8},{48,16},{56,24},{64,96... | collective-permute-start | bytes 786440 | tf_op jit(solution)/shard_map/ppermute | solution.py:541
  79.2 1.1 %convolution_convert_fusion = bf16[64,2048]{1,0:T(8,128)(2,1)} fusion(bf16[128,2048]{1,0:T(8,128)(2,1)S(1)} %bitcast.118, bf16[256,128]{1,0:T(8,128)(2,1)S(1)} %get-tuple-element.9), kind=kOutput, calls=%fused_computation | convolution fusion | flops 69337088 | bytes 851968 | tf_op jit(solution)/shard_map/dot_general | solution.py:568
  80.3 0.8 pad_maximum_fusion.3
  81.3 2.9 %collective-permute-done.21.pair_hbm = bf16[64,2048]{1,0:T(8,128)(2,1)} collective-permute-done((bf16[64,2048]{1,0:T(8,128)(2,1)S(1)}, bf16[64,2048]{1,0:T(8,128)(2,1)}, u32[]{:S(2)}, u32[]{:S(2)}) %collective-permute-start.21) | collective-permute-done | bytes 262176 | tf_op jit(solution)/shard_map/ppermute | solution.py:541
  84.3 1.0 copy-done.8
  85.2 4.9 %shared_mlp.1 = bf16[128,2048]{1,0:T(8,128)(2,1)} custom-call(s32[1]{0:T(128)} %bitcast.39.here, s32[1]{0:T(128)} %bitcast.place, bf16[64,2048]{1,0:T(8,128)(2,1)} %copy-done.2, bf16[64,2048]{1,0:T(8,128)(2,1)} %collective-permute-done.21.pair_hbm, bf16[2048,256]{1,0:T(8,128)(2,1)} %gate_hbm.1, bf16[2048,256]{1,0:T(8,128)(2,1)} %up_hbm.1, ...), custom_call_target="tpu_custom_call" | custom-call | tf_op jit(solution)/shard_map/shared_mlp/pallas_call | solution.py:305
  90.1 4.3 %all-to-all-start.2 = ((bf16[8,16,2048]{2,1,0:T(8,128)(2,1)}), bf16[8,16,2048]{2,1,0:T(8,128)(2,1)S(1)}, u32[]{:S(2)}, u32[]{:S(2)}) async-start(bf16[8,16,2048]{2,1,0:T(8,128)(2,1)} %bitcast.117), calls=%async_computation.2 | async-start | bytes 1048576 | tf_op jit(solution)/shard_map/all_to_all | solution.py:555
  94.4 1.3 %fusion.53 = (bf16[64,2048]{1,0:T(8,128)(2,1)S(1)}, f32[64,2048]{1,0:T(8,128)S(1)}) fusion(bf16[64,2048]{1,0:T(8,128)(2,1)} %collective-permute-done.14, bf16[128,2048]{1,0:T(8,128)(2,1)S(1)} %bitcast.119, bf16[256,128]{1,0:T(8,128)(2,1)S(1)} %get-tuple-element.9), kind=kOutput, calls=%fused_computation.88 | convolution fusion | flops 69861376 | bytes 1638400 | tf_op jit(solution)/shard_map/dot_general | solution.py:568
  95.7 0.8 collective-permute-start.15
  96.5 0.8 collective-permute-start.16
  97.3 2.0 %collective-permute-start.17 = (bf16[16,2048]{1,0:T(8,128)(2,1)S(1)}, bf16[16,2048]{1,0:T(8,128)(2,1)S(1)}, u32[]{:S(2)}, u32[]{:S(2)}) collective-permute-start(bf16[16,2048]{1,0:T(8,128)(2,1)S(1)} %get-tuple-element.19), channel_id=1, source_target_pairs={{0,6},{1,7},{2,0},{3,1},{4,2},{5,3},{6,4},{7,5},{8,14},{9,15},{10,... | collective-permute-start | bytes 196616 | tf_op jit(solution)/shard_map/ppermute | solution.py:578
  99.2 3.9 %all-to-all-done.2 = bf16[8,16,2048]{2,1,0:T(8,128)(2,1)S(1)} async-done(((bf16[8,16,2048]{2,1,0:T(8,128)(2,1)}), bf16[8,16,2048]{2,1,0:T(8,128)(2,1)S(1)}, u32[]{:S(2)}, u32[]{:S(2)}) %all-to-all-start.2) | async-done | bytes 524320 | tf_op jit(solution)/shard_map/all_to_all | solution.py:555
  103.2 0.7 fusion.19
  (81 shorter events, 2.1 us)
Async XLA Ops:
  0.6 17.3 %copy-start = (bf16[2048,128]{1,0:T(8,128)(2,1)S(1)}, bf16[2048,128]{1,0:T(8,128)(2,1)}, u32[]{:S(2)}) copy-start(bf16[2048,128]{1,0:T(8,128)(2,1)} %param.23) | copy-start | bytes 1572868
  0.6 16.8 %copy-start.3 = (bf16[128,256]{1,0:T(8,128)(2,1)S(1)}, bf16[128,256]{1,0:T(8,128)(2,1)}, u32[]{:S(2)}) copy-start(bf16[128,256]{1,0:T(8,128)(2,1)} %refs_0_.1) | copy-start | bytes 196612
  0.7 13.7 %copy-start.7 = (bf16[2048,256]{1,0:T(8,128)(2,1)S(1)}, bf16[2048,256]{1,0:T(8,128)(2,1)}, u32[]{:S(2)}) copy-start(bf16[2048,256]{1,0:T(8,128)(2,1)} %up_hbm.1) | copy-start | bytes 3145732
  0.7 11.9 %collective-permute-start = (bf16[128,256]{1,0:T(8,128)(2,1)}, bf16[128,256]{1,0:T(8,128)(2,1)S(1)}, u32[]{:S(2)}, u32[]{:S(2)}) collective-permute-start(bf16[128,256]{1,0:T(8,128)(2,1)} %refs_0_.1), channel_id=1, source_target_pairs={{0,2},{1,3},{2,4},{3,5},{4,6},{5,7},{6,0},{7,1},{8,10},{9,11},{10,... | collective-permute-start | bytes 196616 | tf_op jit(solution)/shard_map/ppermute | solution.py:35
  2.4 10.2 %collective-permute-start.1 = (bf16[128,256]{1,0:T(8,128)(2,1)}, bf16[128,256]{1,0:T(8,128)(2,1)S(1)}, u32[]{:S(2)}, u32[]{:S(2)}) collective-permute-start(bf16[128,256]{1,0:T(8,128)(2,1)} %refs_0_.1), channel_id=1, source_target_pairs={{0,4},{1,5},{2,6},{3,7},{4,0},{5,1},{6,2},{7,3},{8,12},{9,13},{10,... | collective-permute-start | bytes 196616 | tf_op jit(solution)/shard_map/ppermute | solution.py:35
  5.3 7.8 %collective-permute-start.2 = (bf16[128,256]{1,0:T(8,128)(2,1)}, bf16[128,256]{1,0:T(8,128)(2,1)S(1)}, u32[]{:S(2)}, u32[]{:S(2)}) collective-permute-start(bf16[128,256]{1,0:T(8,128)(2,1)} %refs_0_.1), channel_id=1, source_target_pairs={{0,6},{1,7},{2,0},{3,1},{4,2},{5,3},{6,4},{7,5},{8,14},{9,15},{10,... | collective-permute-start | bytes 196616 | tf_op jit(solution)/shard_map/ppermute | solution.py:35
  6.7 7.7 %collective-permute-start.3 = (bf16[128,256]{1,0:T(8,128)(2,1)}, bf16[128,256]{1,0:T(8,128)(2,1)S(1)}, u32[]{:S(2)}, u32[]{:S(2)}) collective-permute-start(bf16[128,256]{1,0:T(8,128)(2,1)} %refs_0_.1), channel_id=1, source_target_pairs={{0,1},{1,0},{2,3},{3,2},{4,5},{5,4},{6,7},{7,6},{8,9},{9,8},{10,11... | collective-permute-start | bytes 196616 | tf_op jit(solution)/shard_map/ppermute | solution.py:37
  6.7 56.6 %collective-permute-start.22 = (bf16[2048,256]{1,0:T(8,128)(2,1)}, bf16[2048,256]{1,0:T(8,128)(2,1)}, u32[]{:S(2)}, u32[]{:S(2)}) collective-permute-start(bf16[2048,256]{1,0:T(8,128)(2,1)} %gate_hbm.1), channel_id=1, source_target_pairs={{0,97},{1,0},{2,99},{3,2},{4,101},{5,4},{6,103},{7,6},{8,105},{9,8... | collective-permute-start | bytes 3145736 | tf_op jit(solution)/shard_map/ppermute | solution.py:520
  11.9 6.1 %copy-start.13 = (f32[2048]{0:T(1024)S(1)}, f32[2048]{0:T(1024)}, u32[]{:S(2)}) copy-start(f32[2048]{0:T(1024)} %param.22) | copy-start | bytes 24580
  12.6 2.3 %collective-permute-start.4 = (bf16[128,256]{1,0:T(8,128)(2,1)S(1)}, bf16[128,256]{1,0:T(8,128)(2,1)S(1)}, u32[]{:S(2)}, u32[]{:S(2)}) collective-permute-start(bf16[128,256]{1,0:T(8,128)(2,1)S(1)} %collective-permute-done.refs_1_), channel_id=1, source_target_pairs={{0,1},{1,0},{2,3},{3,2},{4,5},{5,4},{6,7},{7,6},{8,9},{9,8},{10,11... | collective-permute-start | bytes 196616 | tf_op jit(solution)/shard_map/ppermute | solution.py:37
  12.6 4.8 %collective-permute-start.5 = (bf16[128,256]{1,0:T(8,128)(2,1)S(1)}, bf16[128,256]{1,0:T(8,128)(2,1)S(1)}, u32[]{:S(2)}, u32[]{:S(2)}) collective-permute-start(bf16[128,256]{1,0:T(8,128)(2,1)S(1)} %collective-permute-done.1.refs_2_), channel_id=1, source_target_pairs={{0,1},{1,0},{2,3},{3,2},{4,5},{5,4},{6,7},{7,6},{8,9},{9,8},{10,11... | collective-permute-start | bytes 196616 | tf_op jit(solution)/shard_map/ppermute | solution.py:37
  13.1 4.3 %collective-permute-start.6 = (bf16[128,256]{1,0:T(8,128)(2,1)S(1)}, bf16[128,256]{1,0:T(8,128)(2,1)S(1)}, u32[]{:S(2)}, u32[]{:S(2)}) collective-permute-start(bf16[128,256]{1,0:T(8,128)(2,1)S(1)} %collective-permute-done.2.refs_3_), channel_id=1, source_target_pairs={{0,1},{1,0},{2,3},{3,2},{4,5},{5,4},{6,7},{7,6},{8,9},{9,8},{10,11... | collective-permute-start | bytes 196616 | tf_op jit(solution)/shard_map/ppermute | solution.py:37
  14.4 49.0 %collective-permute-start.23 = (bf16[2048,256]{1,0:T(8,128)(2,1)S(1)}, bf16[2048,256]{1,0:T(8,128)(2,1)}, u32[]{:S(2)}, u32[]{:S(2)}) collective-permute-start(bf16[2048,256]{1,0:T(8,128)(2,1)S(1)} %copy-done.7), channel_id=1, source_target_pairs={{0,1},{1,96},{2,3},{3,98},{4,5},{5,100},{6,7},{7,102},{8,9},{9,104... | collective-permute-start | bytes 3145736 | tf_op jit(solution)/shard_map/ppermute | solution.py:520
  14.9 49.0 %collective-permute-start.24 = (bf16[256,2048]{1,0:T(8,128)(2,1)}, bf16[256,2048]{1,0:T(8,128)(2,1)}, u32[]{:S(2)}, u32[]{:S(2)}) collective-permute-start(bf16[256,2048]{1,0:T(8,128)(2,1)} %down_hbm.1), channel_id=1, source_target_pairs={{0,97},{1,0},{2,99},{3,2},{4,101},{5,4},{6,103},{7,6},{8,105},{9,8... | collective-permute-start | bytes 3145736 | tf_op jit(solution)/shard_map/ppermute | solution.py:520
  17.4 1.0 %copy-start.9 = (f32[2,8,64,16]{2,3,1,0:T(8,128)S(1)}, f32[2,8,64,16]{2,3,1,0:T(8,128)}, u32[]{:S(2)}) copy-start(f32[2,8,64,16]{2,3,1,0:T(8,128)} %param.28) | copy-start | bytes 196612
  17.7 1.4 %copy-start.10 = (f32[2,8,16,64]{3,2,1,0:T(8,128)S(1)}, f32[2,8,16,64]{3,2,1,0:T(8,128)}, u32[]{:S(2)}) copy-start(f32[2,8,16,64]{3,2,1,0:T(8,128)} %param.29) | copy-start | bytes 196612
  18.0 1.5 %copy-start.12 = (f32[128]{0:T(128)S(1)}, f32[128]{0:T(128)}, u32[]{:S(2)}) copy-start(f32[128]{0:T(128)} %param.30) | copy-start | bytes 1540
  19.5 13.1 %copy-start.5 = (s32[128,4]{0,1:T(4,128)S(1)}, s32[128,4]{0,1:T(4,128)}, u32[]{:S(2)}) copy-start(s32[128,4]{0,1:T(4,128)} %param.34) | copy-start | bytes 6148
  19.5 13.1 %copy-start.6 = (f32[128,4]{0,1:T(4,128)S(1)}, f32[128,4]{0,1:T(4,128)}, u32[]{:S(2)}) copy-start(f32[128,4]{0,1:T(4,128)} %param.35) | copy-start | bytes 6148
  19.5 13.4 %copy-start.4 = (f32[2048]{0:T(1024)S(1)}, f32[2048]{0:T(1024)}, u32[]{:S(2)}) copy-start(f32[2048]{0:T(1024)} %param.32) | copy-start | bytes 24580
  19.6 5.2 %collective-permute-start.7 = (bf16[128,128]{1,0:T(8,128)(2,1)S(1)}, bf16[128,128]{1,0:T(8,128)(2,1)S(1)}, u32[]{:S(2)}, u32[]{:S(2)}) collective-permute-start(bf16[128,128]{1,0:T(8,128)(2,1)S(1)} %fusion.27.refs_8_), channel_id=1, source_target_pairs={{0,2},{1,3},{2,4},{3,5},{4,6},{5,7},{6,0},{7,1},{8,10},{9,11},{10,... | collective-permute-start | bytes 98312 | tf_op jit(solution)/shard_map/ppermute | solution.py:35
  20.3 5.4 %collective-permute-start.8 = (bf16[128,128]{1,0:T(8,128)(2,1)S(1)}, bf16[128,128]{1,0:T(8,128)(2,1)S(1)}, u32[]{:S(2)}, u32[]{:S(2)}) collective-permute-start(bf16[128,128]{1,0:T(8,128)(2,1)S(1)} %fusion.27.refs_8_), channel_id=1, source_target_pairs={{0,4},{1,5},{2,6},{3,7},{4,0},{5,1},{6,2},{7,3},{8,12},{9,13},{10,... | collective-permute-start | bytes 98312 | tf_op jit(solution)/shard_map/ppermute | solution.py:35
  24.8 3.9 %collective-permute-start.9 = (bf16[128,128]{1,0:T(8,128)(2,1)S(1)}, bf16[128,128]{1,0:T(8,128)(2,1)S(1)}, u32[]{:S(2)}, u32[]{:S(2)}) collective-permute-start(bf16[128,128]{1,0:T(8,128)(2,1)S(1)} %fusion.27.refs_8_), channel_id=1, source_target_pairs={{0,6},{1,7},{2,0},{3,1},{4,2},{5,3},{6,4},{7,5},{8,14},{9,15},{10,... | collective-permute-start | bytes 98312 | tf_op jit(solution)/shard_map/ppermute | solution.py:35
  25.8 3.0 %collective-permute-start.10 = (bf16[128,128]{1,0:T(8,128)(2,1)S(1)}, bf16[128,128]{1,0:T(8,128)(2,1)S(1)}, u32[]{:S(2)}, u32[]{:S(2)}) collective-permute-start(bf16[128,128]{1,0:T(8,128)(2,1)S(1)} %fusion.27.refs_8_), channel_id=1, source_target_pairs={{0,1},{1,0},{2,3},{3,2},{4,5},{5,4},{6,7},{7,6},{8,9},{9,8},{10,11... | collective-permute-start | bytes 98312 | tf_op jit(solution)/shard_map/ppermute | solution.py:37
  28.7 1.2 %collective-permute-start.11 = (bf16[128,128]{1,0:T(8,128)(2,1)S(1)}, bf16[128,128]{1,0:T(8,128)(2,1)S(1)}, u32[]{:S(2)}, u32[]{:S(2)}) collective-permute-start(bf16[128,128]{1,0:T(8,128)(2,1)S(1)} %collective-permute-done.7.refs_9_), channel_id=1, source_target_pairs={{0,1},{1,0},{2,3},{3,2},{4,5},{5,4},{6,7},{7,6},{8,9},{9,8},{10,11... | collective-permute-start | bytes 98312 | tf_op jit(solution)/shard_map/ppermute | solution.py:37
  28.7 4.2 %collective-permute-start.12 = (bf16[128,128]{1,0:T(8,128)(2,1)S(1)}, bf16[128,128]{1,0:T(8,128)(2,1)S(1)}, u32[]{:S(2)}, u32[]{:S(2)}) collective-permute-start(bf16[128,128]{1,0:T(8,128)(2,1)S(1)} %collective-permute-done.8.refs_10_), channel_id=1, source_target_pairs={{0,1},{1,0},{2,3},{3,2},{4,5},{5,4},{6,7},{7,6},{8,9},{9,8},{10,11... | collective-permute-start | bytes 98312 | tf_op jit(solution)/shard_map/ppermute | solution.py:37
  29.9 3.0 %collective-permute-start.13 = (bf16[128,128]{1,0:T(8,128)(2,1)S(1)}, bf16[128,128]{1,0:T(8,128)(2,1)S(1)}, u32[]{:S(2)}, u32[]{:S(2)}) collective-permute-start(bf16[128,128]{1,0:T(8,128)(2,1)S(1)} %collective-permute-done.9.refs_11_), channel_id=1, source_target_pairs={{0,1},{1,0},{2,3},{3,2},{4,5},{5,4},{6,7},{7,6},{8,9},{9,8},{10,11... | collective-permute-start | bytes 98312 | tf_op jit(solution)/shard_map/ppermute | solution.py:37
  30.1 2.2 %copy-start.1 = (bf16[1024,2048]{1,0:T(8,128)(2,1)S(1)}, bf16[1024,2048]{1,0:T(8,128)(2,1)}, u32[]{:S(2)}) copy-start(bf16[1024,2048]{1,0:T(8,128)(2,1)} %weight_hbm.1) | copy-start | bytes 12582916
  51.9 22.1 %copy-start.11 = (bf16[2048]{0:T(1024)(128)(2,1)S(1)}, bf16[2048]{0:T(1024)(128)(2,1)}, u32[]{:S(2)}) copy-start(bf16[2048]{0:T(1024)(128)(2,1)} %param.33) | copy-start | bytes 12292
  56.1 23.2 %all-to-all-start.1 = ((bf16[16,8,2048]{2,1,0:T(8,128)(2,1)}), bf16[16,8,2048]{2,1,0:T(8,128)(2,1)S(1)}, u32[]{:S(2)}, u32[]{:S(2)}) async-start(bf16[16,8,2048]{2,1,0:T(8,128)(2,1)} %bitcast.112), calls=%async_computation.1 | async-start | bytes 1048576 | tf_op jit(solution)/shard_map/all_to_all | solution.py:547
  63.3 21.0 %collective-permute-start.25 = (bf16[2048,256]{1,0:T(8,128)(2,1)}, bf16[2048,256]{1,0:T(8,128)(2,1)}, u32[]{:S(2)}, u32[]{:S(2)}) collective-permute-start(bf16[2048,256]{1,0:T(8,128)(2,1)} %collective-permute-done.22.gate_far), channel_id=1, source_target_pairs={{0,1},{1,0},{2,3},{3,2},{4,5},{5,4},{6,7},{7,6},{8,9},{9,8},{10,11... | collective-permute-start | bytes 3145736 | tf_op jit(solution)/shard_map/ppermute | solution.py:521
  63.4 20.9 %collective-permute-start.26 = (bf16[2048,256]{1,0:T(8,128)(2,1)}, bf16[2048,256]{1,0:T(8,128)(2,1)S(1)}, u32[]{:S(2)}, u32[]{:S(2)}) collective-permute-start(bf16[2048,256]{1,0:T(8,128)(2,1)} %collective-permute-done.23.up_far), channel_id=1, source_target_pairs={{0,1},{1,0},{2,3},{3,2},{4,5},{5,4},{6,7},{7,6},{8,9},{9,8},{10,11... | collective-permute-start | bytes 3145736 | tf_op jit(solution)/shard_map/ppermute | solution.py:521
  63.9 20.4 %collective-permute-start.27 = (bf16[256,2048]{1,0:T(8,128)(2,1)}, bf16[256,2048]{1,0:T(8,128)(2,1)}, u32[]{:S(2)}, u32[]{:S(2)}) collective-permute-start(bf16[256,2048]{1,0:T(8,128)(2,1)} %collective-permute-done.24.down_far), channel_id=1, source_target_pairs={{0,1},{1,0},{2,3},{3,2},{4,5},{5,4},{6,7},{7,6},{8,9},{9,8},{10,11... | collective-permute-start | bytes 3145736 | tf_op jit(solution)/shard_map/ppermute | solution.py:521
  64.0 9.1 %collective-permute-start.18 = (bf16[16,2048]{1,0:T(8,128)(2,1)S(1)}, bf16[16,2048]{1,0:T(8,128)(2,1)S(1)}, u32[]{:S(2)}, u32[]{:S(2)}) collective-permute-start(bf16[16,2048]{1,0:T(8,128)(2,1)S(1)} %get-tuple-element.11.refs_0_), channel_id=1, source_target_pairs={{0,8},{8,16},{16,24},{24,0},{32,40},{40,48},{48,56},{56,32},{64,72... | collective-permute-start | bytes 196616 | tf_op jit(solution)/shard_map/ppermute | solution.py:539
  65.9 8.4 %collective-permute-start.19 = (bf16[16,2048]{1,0:T(8,128)(2,1)S(1)}, bf16[16,2048]{1,0:T(8,128)(2,1)S(1)}, u32[]{:S(2)}, u32[]{:S(2)}) collective-permute-start(bf16[16,2048]{1,0:T(8,128)(2,1)S(1)} %get-tuple-element.11.refs_0_), channel_id=1, source_target_pairs={{0,16},{8,24},{16,0},{24,8},{32,48},{40,56},{48,32},{56,40},{64,80... | collective-permute-start | bytes 196616 | tf_op jit(solution)/shard_map/ppermute | solution.py:539
  73.1 4.3 %collective-permute-start.20 = (bf16[16,2048]{1,0:T(8,128)(2,1)S(1)}, bf16[16,2048]{1,0:T(8,128)(2,1)S(1)}, u32[]{:S(2)}, u32[]{:S(2)}) collective-permute-start(bf16[16,2048]{1,0:T(8,128)(2,1)S(1)} %get-tuple-element.11.refs_0_), channel_id=1, source_target_pairs={{0,24},{8,0},{16,8},{24,16},{32,56},{40,32},{48,40},{56,48},{64,88... | collective-permute-start | bytes 196616 | tf_op jit(solution)/shard_map/ppermute | solution.py:539
  77.7 6.6 %copy-start.2 = (bf16[64,2048]{1,0:T(8,128)(2,1)}, bf16[64,2048]{1,0:T(8,128)(2,1)S(1)}, u32[]{:S(2)}) copy-start(bf16[64,2048]{1,0:T(8,128)(2,1)S(1)} %join_rows.1.line_hbm) | copy-start | bytes 786436
  77.7 6.6 %collective-permute-start.21 = (bf16[64,2048]{1,0:T(8,128)(2,1)S(1)}, bf16[64,2048]{1,0:T(8,128)(2,1)}, u32[]{:S(2)}, u32[]{:S(2)}) collective-permute-start(bf16[64,2048]{1,0:T(8,128)(2,1)S(1)} %join_rows.1.line_hbm), channel_id=1, source_target_pairs={{0,32},{8,40},{16,48},{24,56},{32,0},{40,8},{48,16},{56,24},{64,96... | collective-permute-start | bytes 786440 | tf_op jit(solution)/shard_map/ppermute | solution.py:541
  80.3 14.1 %collective-permute-start.14 = (bf16[64,2048]{1,0:T(8,128)(2,1)}, bf16[64,2048]{1,0:T(8,128)(2,1)}, u32[]{:S(2)}, u32[]{:S(2)}) collective-permute-start(bf16[64,2048]{1,0:T(8,128)(2,1)} %convolution_convert_fusion), channel_id=1, source_target_pairs={{0,1},{1,0},{2,3},{3,2},{4,5},{5,4},{6,7},{7,6},{8,9},{9,8},{10,11... | collective-permute-start | bytes 786440 | tf_op jit(solution)/shard_map/ppermute | solution.py:573
  84.3 1.0 copy-start.8
  90.1 13.0 %all-to-all-start.2 = ((bf16[8,16,2048]{2,1,0:T(8,128)(2,1)}), bf16[8,16,2048]{2,1,0:T(8,128)(2,1)S(1)}, u32[]{:S(2)}, u32[]{:S(2)}) async-start(bf16[8,16,2048]{2,1,0:T(8,128)(2,1)} %bitcast.117), calls=%async_computation.2 | async-start | bytes 1048576 | tf_op jit(solution)/shard_map/all_to_all | solution.py:555
  95.7 7.5 %collective-permute-start.15 = (bf16[16,2048]{1,0:T(8,128)(2,1)S(1)}, bf16[16,2048]{1,0:T(8,128)(2,1)S(1)}, u32[]{:S(2)}, u32[]{:S(2)}) collective-permute-start(bf16[16,2048]{1,0:T(8,128)(2,1)S(1)} %get-tuple-element.18), channel_id=1, source_target_pairs={{0,2},{1,3},{2,4},{3,5},{4,6},{5,7},{6,0},{7,1},{8,10},{9,11},{10,... | collective-permute-start | bytes 196616 | tf_op jit(solution)/shard_map/ppermute | solution.py:578
  96.5 6.7 %collective-permute-start.16 = (bf16[16,2048]{1,0:T(8,128)(2,1)S(1)}, bf16[16,2048]{1,0:T(8,128)(2,1)S(1)}, u32[]{:S(2)}, u32[]{:S(2)}) collective-permute-start(bf16[16,2048]{1,0:T(8,128)(2,1)S(1)} %get-tuple-element.20), channel_id=1, source_target_pairs={{0,4},{1,5},{2,6},{3,7},{4,0},{5,1},{6,2},{7,3},{8,12},{9,13},{10,... | collective-permute-start | bytes 196616 | tf_op jit(solution)/shard_map/ppermute | solution.py:578
  97.3 5.9 %collective-permute-start.17 = (bf16[16,2048]{1,0:T(8,128)(2,1)S(1)}, bf16[16,2048]{1,0:T(8,128)(2,1)S(1)}, u32[]{:S(2)}, u32[]{:S(2)}) collective-permute-start(bf16[16,2048]{1,0:T(8,128)(2,1)S(1)} %get-tuple-element.19), channel_id=1, source_target_pairs={{0,6},{1,7},{2,0},{3,1},{4,2},{5,3},{6,4},{7,5},{8,14},{9,15},{10,... | collective-permute-start | bytes 196616 | tf_op jit(solution)/shard_map/ppermute | solution.py:578

commit v3 on v2

--- a/solution.py
+++ b/solution.py
@@ -575,9 +575,10 @@
     routed = pair[:per_dev]
     pair = pair.astype(bf16)
     for step in range(1, chips):
-        routed = routed + lax.ppermute(
+        piece = lax.ppermute(
             pair[step * per_dev : (step + 1) * per_dev], "tp", y_shift(tp_count, step)
-        ).astype(f32)
+        )
+        routed = routed + piece.astype(f32)
     gate_value = jax.nn.sigmoid(jnp.dot(own_mid, gate_vector, preferred_element_type=f32))
     layer_out = (own_after + routed + gate_value[:, None] * shared).astype(bf16)
     return (layer_out, new_state)

time: 104 us -> 104 us (level)
  no operation moved by 1% of the time
where the time goes in v3:
time: 104 us
  starting transfers between devices  39.2 us (38%)
  waiting for transfers between devices  22.2 us (21%)
  blocking collectives  17.3 us (17%)
  Pallas kernels  11.6 us (11%)
  local copies, waits for them, and re-layouts  5.79 us (6%)
  matrix products  3.76 us (4%)
  other arithmetic  2.77 us (3%)
  between operations  1.27 us (1%)
    all_to_all x1, blocking collectives, layer(): lax.all_to_all(outgoing.reshape(ep_count, capacity, width), 'ep', split_a...  17.3 us
    ppermute x6, starting transfers between devices, hop_gather(): lax.ppermute(array, 'tp', y_shift(tp_count, step))  8 us
    ppermute x3, waiting for transfers between devices, layer(): line.append(lax.ppermute(own_mid, 'ep', plane_shift(ep_count, 0, step)))  7.57 us
    all_to_all x1, starting transfers between devices, layer(): lax.all_to_all(result.reshape(ep_count, capacity, width), 'ep', split_axi...  7.2 us
    ppermute x3, starting transfers between devices, layer(): lax.ppermute(w, ('ep', 'tp'), weight_moves(ep_count, tp_count, core))  7.17 us
    ppermute x6, waiting for transfers between devices, hop_gather(): lax.ppermute(array, 'tp', y_shift(tp_count, step))  7.12 us
    ppermute x3, starting transfers between devices, layer(): line.append(lax.ppermute(own_mid, 'ep', plane_shift(ep_count, 0, step)))  5.49 us
    pallas_call x1, Pallas kernels, shared_kernel(): pl.pallas_call(functools.partial(shared_body, side=side), out_shape=jax.S...  4.88 us
  transfers between devices with their start and end apart: 30, of which 8 were waited for; matrix products, arithmetic and copies ran while one was open for 8% of the time, Pallas kernels for 11%

profile of v3, /device:TPU:0, one launch (start us, length us, event | category | flops | bytes accessed | tf_op | source)
XLA Modules:
  0.0 103.9 jit_solution(10377774882879968107)
XLA Ops:
  0.7 1.8 %collective-permute-start = (bf16[128,256]{1,0:T(8,128)(2,1)}, bf16[128,256]{1,0:T(8,128)(2,1)S(1)}, u32[]{:S(2)}, u32[]{:S(2)}) collective-permute-start(bf16[128,256]{1,0:T(8,128)(2,1)} %refs_0_.1), channel_id=1, source_target_pairs={{0,2},{1,3},{2,4},{3,5},{4,6},{5,7},{6,0},{7,1},{8,10},{9,11},{10,... | collective-permute-start | bytes 196616 | tf_op jit(solution)/shard_map/ppermute | solution.py:35
  2.4 2.9 %collective-permute-start.1 = (bf16[128,256]{1,0:T(8,128)(2,1)}, bf16[128,256]{1,0:T(8,128)(2,1)S(1)}, u32[]{:S(2)}, u32[]{:S(2)}) collective-permute-start(bf16[128,256]{1,0:T(8,128)(2,1)} %refs_0_.1), channel_id=1, source_target_pairs={{0,4},{1,5},{2,6},{3,7},{4,0},{5,1},{6,2},{7,3},{8,12},{9,13},{10,... | collective-permute-start | bytes 196616 | tf_op jit(solution)/shard_map/ppermute | solution.py:35
  5.3 1.3 %collective-permute-start.2 = (bf16[128,256]{1,0:T(8,128)(2,1)}, bf16[128,256]{1,0:T(8,128)(2,1)S(1)}, u32[]{:S(2)}, u32[]{:S(2)}) collective-permute-start(bf16[128,256]{1,0:T(8,128)(2,1)} %refs_0_.1), channel_id=1, source_target_pairs={{0,6},{1,7},{2,0},{3,1},{4,2},{5,3},{6,4},{7,5},{8,14},{9,15},{10,... | collective-permute-start | bytes 196616 | tf_op jit(solution)/shard_map/ppermute | solution.py:35
  6.7 4.1 %collective-permute-start.22 = (bf16[2048,256]{1,0:T(8,128)(2,1)}, bf16[2048,256]{1,0:T(8,128)(2,1)}, u32[]{:S(2)}, u32[]{:S(2)}) collective-permute-start(bf16[2048,256]{1,0:T(8,128)(2,1)} %gate_hbm.1), channel_id=1, source_target_pairs={{0,97},{1,0},{2,99},{3,2},{4,101},{5,4},{6,103},{7,6},{8,105},{9,8... | collective-permute-start | bytes 3145736 | tf_op jit(solution)/shard_map/ppermute | solution.py:520
  10.8 1.1 %fusion.51 = (f32[1,128,512]{2,1,0:T(8,128)S(1)}, f32[1,128,512]{2,1,0:T(8,128)S(1)}) fusion(f32[2,128,512]{2,1,0:T(8,128)} %param.24), kind=kLoop, calls=%fused_computation.86 | loop fusion | bytes 1048576 | tf_op jit(solution)/shard_map/slice | solution.py:108
  11.9 0.7 exp.9
  12.6 0.5 collective-permute-start.5
  13.2 0.8 add_divide_fusion
  14.4 0.5 collective-permute-start.23
  14.9 2.5 %collective-permute-start.24 = (bf16[256,2048]{1,0:T(8,128)(2,1)}, bf16[256,2048]{1,0:T(8,128)(2,1)}, u32[]{:S(2)}, u32[]{:S(2)}) collective-permute-start(bf16[256,2048]{1,0:T(8,128)(2,1)} %down_hbm.1), channel_id=1, source_target_pairs={{0,97},{1,0},{2,99},{3,2},{4,101},{5,4},{6,103},{7,6},{8,105},{9,8... | collective-permute-start | bytes 3145736 | tf_op jit(solution)/shard_map/ppermute | solution.py:520
  17.7 0.2 convert_reduce_fusion
  18.0 0.4 convolution_convert_fusion.2
  18.5 0.3 fusion.1
  18.8 0.3 fusion.2
  19.6 0.7 collective-permute-start.7
  20.3 1.2 %collective-permute-start.8 = (bf16[128,128]{1,0:T(8,128)(2,1)S(1)}, bf16[128,128]{1,0:T(8,128)(2,1)S(1)}, u32[]{:S(2)}, u32[]{:S(2)}) collective-permute-start(bf16[128,128]{1,0:T(8,128)(2,1)S(1)} %fusion.27.refs_8_), channel_id=1, source_target_pairs={{0,4},{1,5},{2,6},{3,7},{4,0},{5,1},{6,2},{7,3},{8,12},{9,13},{10,... | collective-permute-start | bytes 98312 | tf_op jit(solution)/shard_map/ppermute | solution.py:35
  21.6 3.2 %collective-permute-done.7.refs_9_ = bf16[128,128]{1,0:T(8,128)(2,1)S(1)} collective-permute-done((bf16[128,128]{1,0:T(8,128)(2,1)S(1)}, bf16[128,128]{1,0:T(8,128)(2,1)S(1)}, u32[]{:S(2)}, u32[]{:S(2)}) %collective-permute-start.7) | collective-permute-done | bytes 32800 | tf_op jit(solution)/shard_map/ppermute | solution.py:35
  24.8 1.0 collective-permute-done.8.refs_10_
  25.8 2.9 %collective-permute-done.9.refs_11_ = bf16[128,128]{1,0:T(8,128)(2,1)S(1)} collective-permute-done((bf16[128,128]{1,0:T(8,128)(2,1)S(1)}, bf16[128,128]{1,0:T(8,128)(2,1)S(1)}, u32[]{:S(2)}, u32[]{:S(2)}) %collective-permute-start.9) | collective-permute-done | bytes 32800 | tf_op jit(solution)/shard_map/ppermute | solution.py:35
  28.7 0.5 collective-permute-start.12
  29.2 0.7 collective-permute-done.11.refs_13_
  30.1 2.2 %copy-done.1 = bf16[1024,2048]{1,0:T(8,128)(2,1)S(1)} copy-done((bf16[1024,2048]{1,0:T(8,128)(2,1)S(1)}, bf16[1024,2048]{1,0:T(8,128)(2,1)}, u32[]{:S(2)}) %copy-start.1) | copy-done | bytes 4194328
  32.3 0.3 pull_weight.1.refs_16_
  32.6 0.3 slot_tables.1
  32.9 1.6 %out_proj_norm.1 = (bf16[16,2048]{1,0:T(8,128)(2,1)S(1)}, f32[16,2048]{1,0:T(8,128)S(1)}, bf16[128,2048]{1,0:T(8,128)(2,1)S(1)}) custom-call(s32[1]{0:T(128)} %bitcast.place, bf16[128,256]{1,0:T(8,128)(2,1)S(1)} %copy-done.3, bf16[128,256]{1,0:T(8,128)(2,1)S(1)} %collective-permute-done.refs_1_, bf16[128,256]{1,0:T(8,128)(2,1)S(1)} %collective-permute-done.1.refs_2_, ...), custom_call_target="tpu_custom_call" | custom-call | tf_op jit(solution)/shard_map/out_proj_norm/pallas_call | solution.py:381
  34.5 17.3 %all_to_all.15 = bf16[16,8,2048]{2,1,0:T(8,128)(2,1)} all-to-all(bf16[16,8,2048]{2,1,0:T(8,128)(2,1)S(1)} %bitcast.94), channel_id=1, replica_groups=mesh['ep'=16,'tp'=8] {'ep'}, dimensions={0} | all-to-all | bytes 1048576 | tf_op jit(solution)/shard_map/all_to_all | solution.py:542
  51.9 4.2 %expert_mlp.1 = bf16[128,2048]{1,0:T(8,128)(2,1)} custom-call(bf16[128,2048]{1,0:T(8,128)(2,1)} %bitcast.113, bf16[8,256,512]{2,1,0:T(8,128)(2,1)} %bitcast.114, bf16[8,256,512]{2,1,0:T(8,128)(2,1)} %bitcast.115, bf16[512,2048]{1,0:T(8,128)(2,1)} %bitcast.116), custom_call_target="tpu_custom_call" | custom-call | tf_op jit(solution)/shard_map/expert_mlp/pallas_call | solution.py:189
  56.1 7.2 %all-to-all-start.1 = ((bf16[16,8,2048]{2,1,0:T(8,128)(2,1)}), bf16[16,8,2048]{2,1,0:T(8,128)(2,1)S(1)}, u32[]{:S(2)}, u32[]{:S(2)}) async-start(bf16[16,8,2048]{2,1,0:T(8,128)(2,1)} %bitcast.112), calls=%async_computation.1 | async-start | bytes 1048576 | tf_op jit(solution)/shard_map/all_to_all | solution.py:547
  63.4 0.5 collective-permute-start.26
  64.0 1.9 %collective-permute-start.18 = (bf16[16,2048]{1,0:T(8,128)(2,1)S(1)}, bf16[16,2048]{1,0:T(8,128)(2,1)S(1)}, u32[]{:S(2)}, u32[]{:S(2)}) collective-permute-start(bf16[16,2048]{1,0:T(8,128)(2,1)S(1)} %get-tuple-element.11.refs_0_), channel_id=1, source_target_pairs={{0,8},{8,16},{16,24},{24,0},{32,40},{40,48},{48,56},{56,32},{64,72... | collective-permute-start | bytes 196616 | tf_op jit(solution)/shard_map/ppermute | solution.py:539
  65.9 2.7 %collective-permute-start.19 = (bf16[16,2048]{1,0:T(8,128)(2,1)S(1)}, bf16[16,2048]{1,0:T(8,128)(2,1)S(1)}, u32[]{:S(2)}, u32[]{:S(2)}) collective-permute-start(bf16[16,2048]{1,0:T(8,128)(2,1)S(1)} %get-tuple-element.11.refs_0_), channel_id=1, source_target_pairs={{0,16},{8,24},{16,0},{24,8},{32,48},{40,56},{48,32},{56,40},{64,80... | collective-permute-start | bytes 196616 | tf_op jit(solution)/shard_map/ppermute | solution.py:539
  68.6 4.5 %collective-permute-done.18.refs_1_ = bf16[16,2048]{1,0:T(8,128)(2,1)S(1)} collective-permute-done((bf16[16,2048]{1,0:T(8,128)(2,1)S(1)}, bf16[16,2048]{1,0:T(8,128)(2,1)S(1)}, u32[]{:S(2)}, u32[]{:S(2)}) %collective-permute-start.18) | collective-permute-done | bytes 65568 | tf_op jit(solution)/shard_map/ppermute | solution.py:539
  73.1 0.9 collective-permute-start.20
  74.3 3.1 %collective-permute-done.20.refs_3_ = bf16[16,2048]{1,0:T(8,128)(2,1)S(1)} collective-permute-done((bf16[16,2048]{1,0:T(8,128)(2,1)S(1)}, bf16[16,2048]{1,0:T(8,128)(2,1)S(1)}, u32[]{:S(2)}, u32[]{:S(2)}) %collective-permute-start.20) | collective-permute-done | bytes 65568 | tf_op jit(solution)/shard_map/ppermute | solution.py:539
  77.3 0.3 join_rows.1.line_hbm
  77.7 1.5 %collective-permute-start.21 = (bf16[64,2048]{1,0:T(8,128)(2,1)S(1)}, bf16[64,2048]{1,0:T(8,128)(2,1)}, u32[]{:S(2)}, u32[]{:S(2)}) collective-permute-start(bf16[64,2048]{1,0:T(8,128)(2,1)S(1)} %join_rows.1.line_hbm), channel_id=1, source_target_pairs={{0,32},{8,40},{16,48},{24,56},{32,0},{40,8},{48,16},{56,24},{64,96... | collective-permute-start | bytes 786440 | tf_op jit(solution)/shard_map/ppermute | solution.py:541
  79.2 1.1 %convolution_convert_fusion = bf16[64,2048]{1,0:T(8,128)(2,1)} fusion(bf16[128,2048]{1,0:T(8,128)(2,1)S(1)} %bitcast.118, bf16[256,128]{1,0:T(8,128)(2,1)S(1)} %get-tuple-element.9), kind=kOutput, calls=%fused_computation | convolution fusion | flops 69337088 | bytes 851968 | tf_op jit(solution)/shard_map/dot_general | solution.py:568
  80.3 0.8 pad_maximum_fusion.3
  81.3 2.9 %collective-permute-done.21.pair_hbm = bf16[64,2048]{1,0:T(8,128)(2,1)} collective-permute-done((bf16[64,2048]{1,0:T(8,128)(2,1)S(1)}, bf16[64,2048]{1,0:T(8,128)(2,1)}, u32[]{:S(2)}, u32[]{:S(2)}) %collective-permute-start.21) | collective-permute-done | bytes 262176 | tf_op jit(solution)/shard_map/ppermute | solution.py:541
  84.3 1.0 copy-done.8
  85.2 4.9 %shared_mlp.1 = bf16[128,2048]{1,0:T(8,128)(2,1)} custom-call(s32[1]{0:T(128)} %bitcast.39.here, s32[1]{0:T(128)} %bitcast.place, bf16[64,2048]{1,0:T(8,128)(2,1)} %copy-done.2, bf16[64,2048]{1,0:T(8,128)(2,1)} %collective-permute-done.21.pair_hbm, bf16[2048,256]{1,0:T(8,128)(2,1)} %gate_hbm.1, bf16[2048,256]{1,0:T(8,128)(2,1)} %up_hbm.1, ...), custom_call_target="tpu_custom_call" | custom-call | tf_op jit(solution)/shard_map/shared_mlp/pallas_call | solution.py:305
  90.1 4.3 %all-to-all-start.2 = ((bf16[8,16,2048]{2,1,0:T(8,128)(2,1)}), bf16[8,16,2048]{2,1,0:T(8,128)(2,1)S(1)}, u32[]{:S(2)}, u32[]{:S(2)}) async-start(bf16[8,16,2048]{2,1,0:T(8,128)(2,1)} %bitcast.117), calls=%async_computation.2 | async-start | bytes 1048576 | tf_op jit(solution)/shard_map/all_to_all | solution.py:555
  94.4 1.3 %fusion.53 = (bf16[64,2048]{1,0:T(8,128)(2,1)S(1)}, f32[64,2048]{1,0:T(8,128)S(1)}) fusion(bf16[64,2048]{1,0:T(8,128)(2,1)} %collective-permute-done.14, bf16[128,2048]{1,0:T(8,128)(2,1)S(1)} %bitcast.119, bf16[256,128]{1,0:T(8,128)(2,1)S(1)} %get-tuple-element.9), kind=kOutput, calls=%fused_computation.88 | convolution fusion | flops 69861376 | bytes 1638400 | tf_op jit(solution)/shard_map/dot_general | solution.py:568
  95.7 0.8 collective-permute-start.15
  96.5 0.8 collective-permute-start.16
  97.3 2.0 %collective-permute-start.17 = (bf16[16,2048]{1,0:T(8,128)(2,1)S(1)}, bf16[16,2048]{1,0:T(8,128)(2,1)S(1)}, u32[]{:S(2)}, u32[]{:S(2)}) collective-permute-start(bf16[16,2048]{1,0:T(8,128)(2,1)S(1)} %get-tuple-element.19), channel_id=1, source_target_pairs={{0,6},{1,7},{2,0},{3,1},{4,2},{5,3},{6,4},{7,5},{8,14},{9,15},{10,... | collective-permute-start | bytes 196616 | tf_op jit(solution)/shard_map/ppermute | solution.py:578
  99.2 3.9 %all-to-all-done.2 = bf16[8,16,2048]{2,1,0:T(8,128)(2,1)S(1)} async-done(((bf16[8,16,2048]{2,1,0:T(8,128)(2,1)}), bf16[8,16,2048]{2,1,0:T(8,128)(2,1)S(1)}, u32[]{:S(2)}, u32[]{:S(2)}) %all-to-all-start.2) | async-done | bytes 524320 | tf_op jit(solution)/shard_map/all_to_all | solution.py:555
  103.2 0.7 fusion.19
  (81 shorter events, 2.1 us)
Async XLA Ops:
  0.6 17.3 %copy-start = (bf16[2048,128]{1,0:T(8,128)(2,1)S(1)}, bf16[2048,128]{1,0:T(8,128)(2,1)}, u32[]{:S(2)}) copy-start(bf16[2048,128]{1,0:T(8,128)(2,1)} %param.23) | copy-start | bytes 1572868
  0.6 16.8 %copy-start.3 = (bf16[128,256]{1,0:T(8,128)(2,1)S(1)}, bf16[128,256]{1,0:T(8,128)(2,1)}, u32[]{:S(2)}) copy-start(bf16[128,256]{1,0:T(8,128)(2,1)} %refs_0_.1) | copy-start | bytes 196612
  0.7 13.7 %copy-start.7 = (bf16[2048,256]{1,0:T(8,128)(2,1)S(1)}, bf16[2048,256]{1,0:T(8,128)(2,1)}, u32[]{:S(2)}) copy-start(bf16[2048,256]{1,0:T(8,128)(2,1)} %up_hbm.1) | copy-start | bytes 3145732
  0.7 11.9 %collective-permute-start = (bf16[128,256]{1,0:T(8,128)(2,1)}, bf16[128,256]{1,0:T(8,128)(2,1)S(1)}, u32[]{:S(2)}, u32[]{:S(2)}) collective-permute-start(bf16[128,256]{1,0:T(8,128)(2,1)} %refs_0_.1), channel_id=1, source_target_pairs={{0,2},{1,3},{2,4},{3,5},{4,6},{5,7},{6,0},{7,1},{8,10},{9,11},{10,... | collective-permute-start | bytes 196616 | tf_op jit(solution)/shard_map/ppermute | solution.py:35
  2.4 10.2 %collective-permute-start.1 = (bf16[128,256]{1,0:T(8,128)(2,1)}, bf16[128,256]{1,0:T(8,128)(2,1)S(1)}, u32[]{:S(2)}, u32[]{:S(2)}) collective-permute-start(bf16[128,256]{1,0:T(8,128)(2,1)} %refs_0_.1), channel_id=1, source_target_pairs={{0,4},{1,5},{2,6},{3,7},{4,0},{5,1},{6,2},{7,3},{8,12},{9,13},{10,... | collective-permute-start | bytes 196616 | tf_op jit(solution)/shard_map/ppermute | solution.py:35
  5.3 7.8 %collective-permute-start.2 = (bf16[128,256]{1,0:T(8,128)(2,1)}, bf16[128,256]{1,0:T(8,128)(2,1)S(1)}, u32[]{:S(2)}, u32[]{:S(2)}) collective-permute-start(bf16[128,256]{1,0:T(8,128)(2,1)} %refs_0_.1), channel_id=1, source_target_pairs={{0,6},{1,7},{2,0},{3,1},{4,2},{5,3},{6,4},{7,5},{8,14},{9,15},{10,... | collective-permute-start | bytes 196616 | tf_op jit(solution)/shard_map/ppermute | solution.py:35
  6.7 7.7 %collective-permute-start.3 = (bf16[128,256]{1,0:T(8,128)(2,1)}, bf16[128,256]{1,0:T(8,128)(2,1)S(1)}, u32[]{:S(2)}, u32[]{:S(2)}) collective-permute-start(bf16[128,256]{1,0:T(8,128)(2,1)} %refs_0_.1), channel_id=1, source_target_pairs={{0,1},{1,0},{2,3},{3,2},{4,5},{5,4},{6,7},{7,6},{8,9},{9,8},{10,11... | collective-permute-start | bytes 196616 | tf_op jit(solution)/shard_map/ppermute | solution.py:37
  6.7 56.6 %collective-permute-start.22 = (bf16[2048,256]{1,0:T(8,128)(2,1)}, bf16[2048,256]{1,0:T(8,128)(2,1)}, u32[]{:S(2)}, u32[]{:S(2)}) collective-permute-start(bf16[2048,256]{1,0:T(8,128)(2,1)} %gate_hbm.1), channel_id=1, source_target_pairs={{0,97},{1,0},{2,99},{3,2},{4,101},{5,4},{6,103},{7,6},{8,105},{9,8... | collective-permute-start | bytes 3145736 | tf_op jit(solution)/shard_map/ppermute | solution.py:520
  11.9 6.1 %copy-start.13 = (f32[2048]{0:T(1024)S(1)}, f32[2048]{0:T(1024)}, u32[]{:S(2)}) copy-start(f32[2048]{0:T(1024)} %param.22) | copy-start | bytes 24580
  12.6 2.3 %collective-permute-start.4 = (bf16[128,256]{1,0:T(8,128)(2,1)S(1)}, bf16[128,256]{1,0:T(8,128)(2,1)S(1)}, u32[]{:S(2)}, u32[]{:S(2)}) collective-permute-start(bf16[128,256]{1,0:T(8,128)(2,1)S(1)} %collective-permute-done.refs_1_), channel_id=1, source_target_pairs={{0,1},{1,0},{2,3},{3,2},{4,5},{5,4},{6,7},{7,6},{8,9},{9,8},{10,11... | collective-permute-start | bytes 196616 | tf_op jit(solution)/shard_map/ppermute | solution.py:37
  12.6 4.8 %collective-permute-start.5 = (bf16[128,256]{1,0:T(8,128)(2,1)S(1)}, bf16[128,256]{1,0:T(8,128)(2,1)S(1)}, u32[]{:S(2)}, u32[]{:S(2)}) collective-permute-start(bf16[128,256]{1,0:T(8,128)(2,1)S(1)} %collective-permute-done.1.refs_2_), channel_id=1, source_target_pairs={{0,1},{1,0},{2,3},{3,2},{4,5},{5,4},{6,7},{7,6},{8,9},{9,8},{10,11... | collective-permute-start | bytes 196616 | tf_op jit(solution)/shard_map/ppermute | solution.py:37
  13.1 4.3 %collective-permute-start.6 = (bf16[128,256]{1,0:T(8,128)(2,1)S(1)}, bf16[128,256]{1,0:T(8,128)(2,1)S(1)}, u32[]{:S(2)}, u32[]{:S(2)}) collective-permute-start(bf16[128,256]{1,0:T(8,128)(2,1)S(1)} %collective-permute-done.2.refs_3_), channel_id=1, source_target_pairs={{0,1},{1,0},{2,3},{3,2},{4,5},{5,4},{6,7},{7,6},{8,9},{9,8},{10,11... | collective-permute-start | bytes 196616 | tf_op jit(solution)/shard_map/ppermute | solution.py:37
  14.4 49.0 %collective-permute-start.23 = (bf16[2048,256]{1,0:T(8,128)(2,1)S(1)}, bf16[2048,256]{1,0:T(8,128)(2,1)}, u32[]{:S(2)}, u32[]{:S(2)}) collective-permute-start(bf16[2048,256]{1,0:T(8,128)(2,1)S(1)} %copy-done.7), channel_id=1, source_target_pairs={{0,1},{1,96},{2,3},{3,98},{4,5},{5,100},{6,7},{7,102},{8,9},{9,104... | collective-permute-start | bytes 3145736 | tf_op jit(solution)/shard_map/ppermute | solution.py:520
  14.9 49.0 %collective-permute-start.24 = (bf16[256,2048]{1,0:T(8,128)(2,1)}, bf16[256,2048]{1,0:T(8,128)(2,1)}, u32[]{:S(2)}, u32[]{:S(2)}) collective-permute-start(bf16[256,2048]{1,0:T(8,128)(2,1)} %down_hbm.1), channel_id=1, source_target_pairs={{0,97},{1,0},{2,99},{3,2},{4,101},{5,4},{6,103},{7,6},{8,105},{9,8... | collective-permute-start | bytes 3145736 | tf_op jit(solution)/shard_map/ppermute | solution.py:520
  17.4 1.0 %copy-start.9 = (f32[2,8,64,16]{2,3,1,0:T(8,128)S(1)}, f32[2,8,64,16]{2,3,1,0:T(8,128)}, u32[]{:S(2)}) copy-start(f32[2,8,64,16]{2,3,1,0:T(8,128)} %param.28) | copy-start | bytes 196612
  17.7 1.4 %copy-start.10 = (f32[2,8,16,64]{3,2,1,0:T(8,128)S(1)}, f32[2,8,16,64]{3,2,1,0:T(8,128)}, u32[]{:S(2)}) copy-start(f32[2,8,16,64]{3,2,1,0:T(8,128)} %param.29) | copy-start | bytes 196612
  18.0 1.5 %copy-start.12 = (f32[128]{0:T(128)S(1)}, f32[128]{0:T(128)}, u32[]{:S(2)}) copy-start(f32[128]{0:T(128)} %param.30) | copy-start | bytes 1540
  19.5 13.1 %copy-start.5 = (s32[128,4]{0,1:T(4,128)S(1)}, s32[128,4]{0,1:T(4,128)}, u32[]{:S(2)}) copy-start(s32[128,4]{0,1:T(4,128)} %param.34) | copy-start | bytes 6148
  19.5 13.1 %copy-start.6 = (f32[128,4]{0,1:T(4,128)S(1)}, f32[128,4]{0,1:T(4,128)}, u32[]{:S(2)}) copy-start(f32[128,4]{0,1:T(4,128)} %param.35) | copy-start | bytes 6148
  19.5 13.4 %copy-start.4 = (f32[2048]{0:T(1024)S(1)}, f32[2048]{0:T(1024)}, u32[]{:S(2)}) copy-start(f32[2048]{0:T(1024)} %param.32) | copy-start | bytes 24580
  19.6 5.2 %collective-permute-start.7 = (bf16[128,128]{1,0:T(8,128)(2,1)S(1)}, bf16[128,128]{1,0:T(8,128)(2,1)S(1)}, u32[]{:S(2)}, u32[]{:S(2)}) collective-permute-start(bf16[128,128]{1,0:T(8,128)(2,1)S(1)} %fusion.27.refs_8_), channel_id=1, source_target_pairs={{0,2},{1,3},{2,4},{3,5},{4,6},{5,7},{6,0},{7,1},{8,10},{9,11},{10,... | collective-permute-start | bytes 98312 | tf_op jit(solution)/shard_map/ppermute | solution.py:35
  20.3 5.4 %collective-permute-start.8 = (bf16[128,128]{1,0:T(8,128)(2,1)S(1)}, bf16[128,128]{1,0:T(8,128)(2,1)S(1)}, u32[]{:S(2)}, u32[]{:S(2)}) collective-permute-start(bf16[128,128]{1,0:T(8,128)(2,1)S(1)} %fusion.27.refs_8_), channel_id=1, source_target_pairs={{0,4},{1,5},{2,6},{3,7},{4,0},{5,1},{6,2},{7,3},{8,12},{9,13},{10,... | collective-permute-start | bytes 98312 | tf_op jit(solution)/shard_map/ppermute | solution.py:35
  24.8 3.9 %collective-permute-start.9 = (bf16[128,128]{1,0:T(8,128)(2,1)S(1)}, bf16[128,128]{1,0:T(8,128)(2,1)S(1)}, u32[]{:S(2)}, u32[]{:S(2)}) collective-permute-start(bf16[128,128]{1,0:T(8,128)(2,1)S(1)} %fusion.27.refs_8_), channel_id=1, source_target_pairs={{0,6},{1,7},{2,0},{3,1},{4,2},{5,3},{6,4},{7,5},{8,14},{9,15},{10,... | collective-permute-start | bytes 98312 | tf_op jit(solution)/shard_map/ppermute | solution.py:35
  25.8 3.0 %collective-permute-start.10 = (bf16[128,128]{1,0:T(8,128)(2,1)S(1)}, bf16[128,128]{1,0:T(8,128)(2,1)S(1)}, u32[]{:S(2)}, u32[]{:S(2)}) collective-permute-start(bf16[128,128]{1,0:T(8,128)(2,1)S(1)} %fusion.27.refs_8_), channel_id=1, source_target_pairs={{0,1},{1,0},{2,3},{3,2},{4,5},{5,4},{6,7},{7,6},{8,9},{9,8},{10,11... | collective-permute-start | bytes 98312 | tf_op jit(solution)/shard_map/ppermute | solution.py:37
  28.7 1.2 %collective-permute-start.11 = (bf16[128,128]{1,0:T(8,128)(2,1)S(1)}, bf16[128,128]{1,0:T(8,128)(2,1)S(1)}, u32[]{:S(2)}, u32[]{:S(2)}) collective-permute-start(bf16[128,128]{1,0:T(8,128)(2,1)S(1)} %collective-permute-done.7.refs_9_), channel_id=1, source_target_pairs={{0,1},{1,0},{2,3},{3,2},{4,5},{5,4},{6,7},{7,6},{8,9},{9,8},{10,11... | collective-permute-start | bytes 98312 | tf_op jit(solution)/shard_map/ppermute | solution.py:37
  28.7 4.2 %collective-permute-start.12 = (bf16[128,128]{1,0:T(8,128)(2,1)S(1)}, bf16[128,128]{1,0:T(8,128)(2,1)S(1)}, u32[]{:S(2)}, u32[]{:S(2)}) collective-permute-start(bf16[128,128]{1,0:T(8,128)(2,1)S(1)} %collective-permute-done.8.refs_10_), channel_id=1, source_target_pairs={{0,1},{1,0},{2,3},{3,2},{4,5},{5,4},{6,7},{7,6},{8,9},{9,8},{10,11... | collective-permute-start | bytes 98312 | tf_op jit(solution)/shard_map/ppermute | solution.py:37
  29.9 3.0 %collective-permute-start.13 = (bf16[128,128]{1,0:T(8,128)(2,1)S(1)}, bf16[128,128]{1,0:T(8,128)(2,1)S(1)}, u32[]{:S(2)}, u32[]{:S(2)}) collective-permute-start(bf16[128,128]{1,0:T(8,128)(2,1)S(1)} %collective-permute-done.9.refs_11_), channel_id=1, source_target_pairs={{0,1},{1,0},{2,3},{3,2},{4,5},{5,4},{6,7},{7,6},{8,9},{9,8},{10,11... | collective-permute-start | bytes 98312 | tf_op jit(solution)/shard_map/ppermute | solution.py:37
  30.1 2.2 %copy-start.1 = (bf16[1024,2048]{1,0:T(8,128)(2,1)S(1)}, bf16[1024,2048]{1,0:T(8,128)(2,1)}, u32[]{:S(2)}) copy-start(bf16[1024,2048]{1,0:T(8,128)(2,1)} %weight_hbm.1) | copy-start | bytes 12582916
  51.9 22.1 %copy-start.11 = (bf16[2048]{0:T(1024)(128)(2,1)S(1)}, bf16[2048]{0:T(1024)(128)(2,1)}, u32[]{:S(2)}) copy-start(bf16[2048]{0:T(1024)(128)(2,1)} %param.33) | copy-start | bytes 12292
  56.1 23.2 %all-to-all-start.1 = ((bf16[16,8,2048]{2,1,0:T(8,128)(2,1)}), bf16[16,8,2048]{2,1,0:T(8,128)(2,1)S(1)}, u32[]{:S(2)}, u32[]{:S(2)}) async-start(bf16[16,8,2048]{2,1,0:T(8,128)(2,1)} %bitcast.112), calls=%async_computation.1 | async-start | bytes 1048576 | tf_op jit(solution)/shard_map/all_to_all | solution.py:547
  63.3 21.0 %collective-permute-start.25 = (bf16[2048,256]{1,0:T(8,128)(2,1)}, bf16[2048,256]{1,0:T(8,128)(2,1)}, u32[]{:S(2)}, u32[]{:S(2)}) collective-permute-start(bf16[2048,256]{1,0:T(8,128)(2,1)} %collective-permute-done.22.gate_far), channel_id=1, source_target_pairs={{0,1},{1,0},{2,3},{3,2},{4,5},{5,4},{6,7},{7,6},{8,9},{9,8},{10,11... | collective-permute-start | bytes 3145736 | tf_op jit(solution)/shard_map/ppermute | solution.py:521
  63.4 20.9 %collective-permute-start.26 = (bf16[2048,256]{1,0:T(8,128)(2,1)}, bf16[2048,256]{1,0:T(8,128)(2,1)S(1)}, u32[]{:S(2)}, u32[]{:S(2)}) collective-permute-start(bf16[2048,256]{1,0:T(8,128)(2,1)} %collective-permute-done.23.up_far), channel_id=1, source_target_pairs={{0,1},{1,0},{2,3},{3,2},{4,5},{5,4},{6,7},{7,6},{8,9},{9,8},{10,11... | collective-permute-start | bytes 3145736 | tf_op jit(solution)/shard_map/ppermute | solution.py:521
  63.9 20.4 %collective-permute-start.27 = (bf16[256,2048]{1,0:T(8,128)(2,1)}, bf16[256,2048]{1,0:T(8,128)(2,1)}, u32[]{:S(2)}, u32[]{:S(2)}) collective-permute-start(bf16[256,2048]{1,0:T(8,128)(2,1)} %collective-permute-done.24.down_far), channel_id=1, source_target_pairs={{0,1},{1,0},{2,3},{3,2},{4,5},{5,4},{6,7},{7,6},{8,9},{9,8},{10,11... | collective-permute-start | bytes 3145736 | tf_op jit(solution)/shard_map/ppermute | solution.py:521
  64.0 9.1 %collective-permute-start.18 = (bf16[16,2048]{1,0:T(8,128)(2,1)S(1)}, bf16[16,2048]{1,0:T(8,128)(2,1)S(1)}, u32[]{:S(2)}, u32[]{:S(2)}) collective-permute-start(bf16[16,2048]{1,0:T(8,128)(2,1)S(1)} %get-tuple-element.11.refs_0_), channel_id=1, source_target_pairs={{0,8},{8,16},{16,24},{24,0},{32,40},{40,48},{48,56},{56,32},{64,72... | collective-permute-start | bytes 196616 | tf_op jit(solution)/shard_map/ppermute | solution.py:539
  65.9 8.4 %collective-permute-start.19 = (bf16[16,2048]{1,0:T(8,128)(2,1)S(1)}, bf16[16,2048]{1,0:T(8,128)(2,1)S(1)}, u32[]{:S(2)}, u32[]{:S(2)}) collective-permute-start(bf16[16,2048]{1,0:T(8,128)(2,1)S(1)} %get-tuple-element.11.refs_0_), channel_id=1, source_target_pairs={{0,16},{8,24},{16,0},{24,8},{32,48},{40,56},{48,32},{56,40},{64,80... | collective-permute-start | bytes 196616 | tf_op jit(solution)/shard_map/ppermute | solution.py:539
  73.1 4.3 %collective-permute-start.20 = (bf16[16,2048]{1,0:T(8,128)(2,1)S(1)}, bf16[16,2048]{1,0:T(8,128)(2,1)S(1)}, u32[]{:S(2)}, u32[]{:S(2)}) collective-permute-start(bf16[16,2048]{1,0:T(8,128)(2,1)S(1)} %get-tuple-element.11.refs_0_), channel_id=1, source_target_pairs={{0,24},{8,0},{16,8},{24,16},{32,56},{40,32},{48,40},{56,48},{64,88... | collective-permute-start | bytes 196616 | tf_op jit(solution)/shard_map/ppermute | solution.py:539
  77.7 6.6 %copy-start.2 = (bf16[64,2048]{1,0:T(8,128)(2,1)}, bf16[64,2048]{1,0:T(8,128)(2,1)S(1)}, u32[]{:S(2)}) copy-start(bf16[64,2048]{1,0:T(8,128)(2,1)S(1)} %join_rows.1.line_hbm) | copy-start | bytes 786436
  77.7 6.6 %collective-permute-start.21 = (bf16[64,2048]{1,0:T(8,128)(2,1)S(1)}, bf16[64,2048]{1,0:T(8,128)(2,1)}, u32[]{:S(2)}, u32[]{:S(2)}) collective-permute-start(bf16[64,2048]{1,0:T(8,128)(2,1)S(1)} %join_rows.1.line_hbm), channel_id=1, source_target_pairs={{0,32},{8,40},{16,48},{24,56},{32,0},{40,8},{48,16},{56,24},{64,96... | collective-permute-start | bytes 786440 | tf_op jit(solution)/shard_map/ppermute | solution.py:541
  80.3 14.1 %collective-permute-start.14 = (bf16[64,2048]{1,0:T(8,128)(2,1)}, bf16[64,2048]{1,0:T(8,128)(2,1)}, u32[]{:S(2)}, u32[]{:S(2)}) collective-permute-start(bf16[64,2048]{1,0:T(8,128)(2,1)} %convolution_convert_fusion), channel_id=1, source_target_pairs={{0,1},{1,0},{2,3},{3,2},{4,5},{5,4},{6,7},{7,6},{8,9},{9,8},{10,11... | collective-permute-start | bytes 786440 | tf_op jit(solution)/shard_map/ppermute | solution.py:573
  84.3 1.0 copy-start.8
  90.1 13.0 %all-to-all-start.2 = ((bf16[8,16,2048]{2,1,0:T(8,128)(2,1)}), bf16[8,16,2048]{2,1,0:T(8,128)(2,1)S(1)}, u32[]{:S(2)}, u32[]{:S(2)}) async-start(bf16[8,16,2048]{2,1,0:T(8,128)(2,1)} %bitcast.117), calls=%async_computation.2 | async-start | bytes 1048576 | tf_op jit(solution)/shard_map/all_to_all | solution.py:555
  95.7 7.5 %collective-permute-start.15 = (bf16[16,2048]{1,0:T(8,128)(2,1)S(1)}, bf16[16,2048]{1,0:T(8,128)(2,1)S(1)}, u32[]{:S(2)}, u32[]{:S(2)}) collective-permute-start(bf16[16,2048]{1,0:T(8,128)(2,1)S(1)} %get-tuple-element.18), channel_id=1, source_target_pairs={{0,2},{1,3},{2,4},{3,5},{4,6},{5,7},{6,0},{7,1},{8,10},{9,11},{10,... | collective-permute-start | bytes 196616 | tf_op jit(solution)/shard_map/ppermute | solution.py:578
  96.5 6.7 %collective-permute-start.16 = (bf16[16,2048]{1,0:T(8,128)(2,1)S(1)}, bf16[16,2048]{1,0:T(8,128)(2,1)S(1)}, u32[]{:S(2)}, u32[]{:S(2)}) collective-permute-start(bf16[16,2048]{1,0:T(8,128)(2,1)S(1)} %get-tuple-element.20), channel_id=1, source_target_pairs={{0,4},{1,5},{2,6},{3,7},{4,0},{5,1},{6,2},{7,3},{8,12},{9,13},{10,... | collective-permute-start | bytes 196616 | tf_op jit(solution)/shard_map/ppermute | solution.py:578
  97.3 5.9 %collective-permute-start.17 = (bf16[16,2048]{1,0:T(8,128)(2,1)S(1)}, bf16[16,2048]{1,0:T(8,128)(2,1)S(1)}, u32[]{:S(2)}, u32[]{:S(2)}) collective-permute-start(bf16[16,2048]{1,0:T(8,128)(2,1)S(1)} %get-tuple-element.19), channel_id=1, source_target_pairs={{0,6},{1,7},{2,0},{3,1},{4,2},{5,3},{6,4},{7,5},{8,14},{9,15},{10,... | collective-permute-start | bytes 196616 | tf_op jit(solution)/shard_map/ppermute | solution.py:578
